TPU v7x, 512 devices: a whole 4x4x16 slice. The times are simulated.
512 devices in a mesh: sp: 256 (over z, y, x), tp: 2 (over core).
Axes of the slice: x: 4, y: 4, z: 16, core: 2. Of those that a mesh axis runs over, the one named last changes fastest.
Arguments:
- residual: bfloat16 [49152, 1024], P('sp', 'tp'), may hold values from -6 to 6
- query_first: bfloat16 [49152, 1024], P('sp', 'tp'), may hold values from -64 to 64
- key_first: bfloat16 [49152, 256], P('sp', 'tp'), may hold values from -20 to 20
- value_first: bfloat16 [49152, 256], P('sp', 'tp'), may hold values from -6 to 6
- documents: int32 [49152], P('sp'), may hold values from 0 to 53, as said below
- bias_first: float32 [16, 513], P('tp'), may hold values from -4 to 4
- out_first: bfloat16 [1024, 1024], P('tp'), may hold values from -0.75 to 0.75
- norm_gain: float32 [1024], replicated, may hold values from 0.1 to 1.9
- query_w: bfloat16 [1024, 1024], P(None, 'tp'), may hold values from -0.1875 to 0.1875
- key_w: bfloat16 [1024, 256], P(None, 'tp'), may hold values from -0.1875 to 0.1875
- value_w: bfloat16 [1024, 256], P(None, 'tp'), may hold values from -0.1875 to 0.1875
- bias_second: float32 [16, 513], P('tp'), may hold values from -4 to 4
- out_second: bfloat16 [1024, 1024], P('tp'), may hold values from -0.75 to 0.75
Outputs:
- layer_two: bfloat16 [49152, 1024], P('sp', 'tp')
Inputs may be any that keep to these rules, and one draw needn't show every extreme that they name: Document numbers start at 0, never fall, and rise by one at the first position of each document; there are exactly 54 documents, each of at least 896 positions.
All inputs are finite; a program needn't handle non-finite values.
Results may differ from a plain program's by a relative error of at most 0.017.
Values may be sent and summed in bfloat16 or wider, within the bound.
No kernel may reach another device: no remote copies, remote signals or barrier semaphores. Data moves between devices by JAX's collectives and lax.ppermute only.
A program may use at most 64 MiB of HBM per device.

v0:
```python
import jax
import jax.numpy as jnp
from jax import lax
from jax.sharding import PartitionSpec as P

HEAD_SIZE = 64
SEG = 64
PAST = 4
REL_CLIP = 256


eps = 1e-06


def from_behind(block, axis, distance):
    devices = range(lax.axis_size(axis))
    route = [(i - distance, i) for i in devices if i - distance in devices]
    return lax.ppermute(block, axis, route)


def joined_along(pieces, dim):
    shape = list(pieces.shape[1:])
    shape[dim] *= pieces.shape[0]
    return jnp.moveaxis(pieces, 0, dim).reshape(shape)


def sent_to_all(x, axis):
    length = lax.axis_size(axis)
    return lax.all_to_all(jnp.broadcast_to(x[None], (length, *x.shape)), axis, 0, 0, tiled=True)


def collect(x, axis, dim):
    return joined_along(sent_to_all(x, axis), dim)


def cut_along(x, dim, length):
    before, after = (x.shape[:dim], x.shape[dim + 1 :])
    return jnp.moveaxis(x.reshape(*before, length, -1, *after), dim, 0)


def sent_and_summed(x, axis, dim):
    length = lax.axis_size(axis)
    pieces = lax.all_to_all(cut_along(x, dim, length), axis, 0, 0, tiled=True)
    return jnp.sum(pieces.astype(jnp.float32), axis=0)


def bias_block(bias_table):
    span_rows = PAST * SEG
    band_rows = SEG * (PAST + 1)
    lowest = -(SEG - 1)
    highest = SEG - 1 + span_rows
    table_cols = bias_table.shape[1]
    left_count = max(0, -REL_CLIP - lowest)
    right_count = max(0, highest - REL_CLIP)
    first_col = max(0, lowest + REL_CLIP)
    last_col = min(table_cols, highest + REL_CLIP + 1)
    heads_local = bias_table.shape[0]
    pieces = []
    pieces.append(bias_table[:, first_col:last_col])
    pieces.append(jnp.broadcast_to(bias_table[:, table_cols - 1 :], (heads_local, right_count)))
    extended = jnp.concatenate(pieces, axis=1)[:, ::-1]
    length = extended.shape[1]
    rows = [
        extended[:, length - band_rows - query_row : length - query_row] for query_row in range(SEG)
    ]
    return jnp.stack(rows, axis=1)


def collect_prior(tok_rows, sender):
    span_rows = PAST * SEG
    hop_count = (span_rows + tok_rows - 1) // tok_rows
    arrived = []
    for distance in range(hop_count, 0, -1):
        needed = min(tok_rows, span_rows - (distance - 1) * tok_rows)
        arrived.append(sender(tok_rows - needed, distance))
    return arrived


def join_member(arrived, member):
    return jnp.concatenate([received[member] for received in arrived], axis=0)


def normalize(rows, norm_gain):
    rows_wide = rows.astype(jnp.float32)
    scale = lax.rsqrt(jnp.mean(rows_wide * rows_wide, axis=1, keepdims=True) + eps)
    return (rows_wide * scale * norm_gain).astype(jnp.bfloat16)


def make_bands(extended, segments):
    blocks = extended.reshape((segments + PAST, SEG) + extended.shape[1:])
    return jnp.concatenate([blocks[lag : lag + segments] for lag in range(PAST + 1)], axis=1)


def attend(queries, keys_ext, values_ext, parity_ext, valid_ext, parity_own, bias_table):
    tok_rows = queries.shape[0]
    segments = tok_rows // SEG
    band_rows = SEG * (PAST + 1)
    kv_local = keys_ext.shape[1] // HEAD_SIZE
    group_size = queries.shape[1] // HEAD_SIZE // kv_local
    key_bands = make_bands(keys_ext, segments).reshape(segments, band_rows, kv_local, HEAD_SIZE)
    value_bands = make_bands(values_ext, segments).reshape(segments, band_rows, kv_local, HEAD_SIZE)
    parity_bands = make_bands(parity_ext, segments)
    valid_bands = make_bands(valid_ext, segments)
    query_blocks = queries.reshape(segments, SEG, kv_local, group_size, HEAD_SIZE)
    logit_scores = jnp.einsum(
        "sqkgd,sbkd->skgqb", query_blocks, key_bands, preferred_element_type=jnp.float32
    )
    logit_scores = logit_scores * HEAD_SIZE ** (-0.5) + bias_block(bias_table).reshape(
        kv_local, group_size, SEG, band_rows
    )
    allowed = valid_bands[:, None, :] & (
        parity_bands[:, None, :] == parity_own.reshape(segments, SEG)[:, :, None]
    )
    logit_scores = jnp.where(allowed[:, None, None], logit_scores, -jnp.inf)
    largest = jnp.max(logit_scores, axis=-1, keepdims=True)
    softmax_weight = jnp.exp(logit_scores - largest)
    softmax_weight = (softmax_weight / jnp.sum(softmax_weight, axis=-1, keepdims=True)).astype(
        jnp.bfloat16
    )
    blended_output = jnp.einsum(
        "skgqb,sbkd->sqkgd", softmax_weight, value_bands, preferred_element_type=jnp.float32
    )
    return blended_output.astype(jnp.bfloat16).reshape(tok_rows, kv_local * group_size * HEAD_SIZE)


def body(
    residual,
    query_first,
    key_first,
    value_first,
    documents,
    bias_first,
    out_first,
    norm_gain,
    query_w,
    key_w,
    value_w,
    bias_second,
    out_second,
):
    tok_rows = residual.shape[0]
    span_rows = PAST * SEG
    offset = lax.axis_index("sp") * tok_rows
    positions = offset - span_rows + jnp.arange(span_rows + tok_rows, dtype=jnp.int32)
    valid_ext = positions >= 0
    parity_own = (documents % 2).astype(jnp.bfloat16)

    def send_first(first_row, distance):
        return from_behind(
            (key_first[first_row:], value_first[first_row:], parity_own[first_row:]), "sp", distance
        )

    arrived = collect_prior(tok_rows, send_first)
    prior_key = join_member(arrived, 0)
    prior_value = join_member(arrived, 1)
    parity_ext = jnp.concatenate([join_member(arrived, 2), parity_own], axis=0)
    mixed_one = attend(
        query_first,
        jnp.concatenate([prior_key, key_first], axis=0),
        jnp.concatenate([prior_value, value_first], axis=0),
        parity_ext,
        valid_ext,
        parity_own,
        bias_first,
    )
    partial_one = jnp.dot(mixed_one, out_first, preferred_element_type=jnp.float32)
    branch_sum = lax.psum_scatter(
        partial_one.astype(jnp.bfloat16), "tp", scatter_dimension=1, tiled=True
    ).astype(jnp.float32)
    layer_share = (residual.astype(jnp.float32) + branch_sum).astype(jnp.bfloat16)
    full_rows = collect(layer_share, "tp", 1)
    normed = normalize(full_rows, norm_gain)
    query_two = jnp.dot(normed, query_w, preferred_element_type=jnp.float32).astype(jnp.bfloat16)
    key_two = jnp.dot(normed, key_w, preferred_element_type=jnp.float32).astype(jnp.bfloat16)
    value_two = jnp.dot(normed, value_w, preferred_element_type=jnp.float32).astype(jnp.bfloat16)

    def send_keys(first_row, distance):
        return from_behind((key_two[first_row:], value_two[first_row:]), "sp", distance)

    arrived_two = collect_prior(tok_rows, send_keys)
    prior_key_two = join_member(arrived_two, 0)
    prior_value_two = join_member(arrived_two, 1)
    mixed_two = attend(
        query_two,
        jnp.concatenate([prior_key_two, key_two], axis=0),
        jnp.concatenate([prior_value_two, value_two], axis=0),
        parity_ext,
        valid_ext,
        parity_own,
        bias_second,
    )
    partial_two = jnp.dot(mixed_two, out_second, preferred_element_type=jnp.float32)
    branch_two = sent_and_summed(partial_two.astype(jnp.bfloat16), "tp", 1)
    return (layer_share.astype(jnp.float32) + branch_two).astype(jnp.bfloat16)


def solution(mesh):
    placed = (
        P("sp", "tp"),
        P("sp", "tp"),
        P("sp", "tp"),
        P("sp", "tp"),
        P("sp"),
        P("tp", None),
        P("tp", None),
        P(),
        P(None, "tp"),
        P(None, "tp"),
        P(None, "tp"),
        P("tp", None),
        P("tp", None),
    )
    return jax.shard_map(body, mesh=mesh, in_specs=placed, out_specs=P("sp", "tp"), check_vma=False)
```

profile of v0, /device:TPU:129, one launch (start us, length us, event | category | flops | bytes accessed | tf_op | source)
XLA Modules:
  0.0 165.6 jit_solution(11455431072425784902)
XLA Ops:
  6.5 1.3 fusion.170
  7.8 3.1 %collective-permute-start.3 = (bf16[192]{0:T(256)(128)(2,1)}, bf16[192]{0:T(256)(128)(2,1)S(1)}, u32[]{:S(2)}, u32[]{:S(2)}) collective-permute-start(bf16[192]{0:T(256)(128)(2,1)} %fusion.170), channel_id=1, source_target_pairs={{0,2},{2,4},{4,6},{6,8},{8,10},{10,12},{12,14},{14,16},{16,18},{18... | collective-permute-start | bytes 1160 | tf_op jit(solution)/shard_map/ppermute | solution.py:18
  10.9 1.2 slice.952
  12.1 4.3 %collective-permute-start.2 = (bf16[64]{0:T(256)(128)(2,1)}, bf16[64]{0:T(256)(128)(2,1)}, u32[]{:S(2)}, u32[]{:S(2)}) collective-permute-start(bf16[64]{0:T(256)(128)(2,1)} %slice.952), channel_id=1, source_target_pairs={{0,4},{2,6},{4,8},{6,10},{8,12},{10,14},{12,16},{14,18},{16,20},{1... | collective-permute-start | bytes 392 | tf_op jit(solution)/shard_map/ppermute | solution.py:18
  16.5 2.5 %collective-permute-start.5 = (bf16[192,128]{1,0:T(8,128)(2,1)}, bf16[192,128]{1,0:T(8,128)(2,1)S(1)}, u32[]{:S(2)}, u32[]{:S(2)}) collective-permute-start(bf16[192,128]{1,0:T(8,128)(2,1)} %param.15), channel_id=1, source_target_pairs={{0,2},{2,4},{4,6},{6,8},{8,10},{10,12},{12,14},{14,16},{16,18},{18... | collective-permute-start | bytes 147464 | tf_op jit(solution)/shard_map/ppermute | solution.py:18
  19.0 1.3 slice.958
  20.4 4.6 %collective-permute-start.4 = (bf16[64,128]{1,0:T(8,128)(2,1)}, bf16[64,128]{1,0:T(8,128)(2,1)}, u32[]{:S(2)}, u32[]{:S(2)}) collective-permute-start(bf16[64,128]{1,0:T(8,128)(2,1)} %slice.958), channel_id=1, source_target_pairs={{0,4},{2,6},{4,8},{6,10},{8,12},{10,14},{12,16},{14,18},{16,20},{1... | collective-permute-start | bytes 49160 | tf_op jit(solution)/shard_map/ppermute | solution.py:18
  25.0 2.8 %collective-permute-start.1 = (bf16[192,128]{1,0:T(8,128)(2,1)}, bf16[192,128]{1,0:T(8,128)(2,1)S(1)}, u32[]{:S(2)}, u32[]{:S(2)}) collective-permute-start(bf16[192,128]{1,0:T(8,128)(2,1)} %param.16), channel_id=1, source_target_pairs={{0,2},{2,4},{4,6},{6,8},{8,10},{10,12},{12,14},{14,16},{16,18},{18... | collective-permute-start | bytes 147464 | tf_op jit(solution)/shard_map/ppermute | solution.py:18
  28.6 0.8 slice_reduce_fusion.1
  30.2 0.8 slice_reduce_fusion
  32.8 0.9 concatenate.135
  33.7 1.3 slice.943
  35.0 0.9 concatenate.122
  75.2 1.3 stack.454
  76.6 3.6 %collective-permute-start = (bf16[64,128]{1,0:T(8,128)(2,1)}, bf16[64,128]{1,0:T(8,128)(2,1)S(1)}, u32[]{:S(2)}, u32[]{:S(2)}) collective-permute-start(bf16[64,128]{1,0:T(8,128)(2,1)} %slice.943), channel_id=1, source_target_pairs={{0,4},{2,6},{4,8},{6,10},{8,12},{10,14},{12,16},{14,18},{16,20},{1... | collective-permute-start | bytes 49160 | tf_op jit(solution)/shard_map/ppermute | solution.py:18
  83.7 3.3 %collective-permute-done = bf16[64,128]{1,0:T(8,128)(2,1)S(1)} collective-permute-done((bf16[64,128]{1,0:T(8,128)(2,1)}, bf16[64,128]{1,0:T(8,128)(2,1)S(1)}, u32[]{:S(2)}, u32[]{:S(2)}) %collective-permute-start) | collective-permute-done | bytes 16416 | tf_op jit(solution)/shard_map/ppermute | solution.py:18
  88.2 3.3 %fusion.187 = (f32[3,2,4,64]{3,2,1,0:T(4,128)S(1)}, f32[3,2,4,64,320]{4,3,2,1,0:T(8,128)}) fusion(f32[2,4,64,320]{3,2,1,0:T(8,128)S(1)} %bitcast.216, pred[3,64,320]{2,1,0:T(8,128)(4,1)} %compare_and_fusion, bf16[3,64,2,4,64]{4,3,2,1,0:T(4,128)(2,1)S(1)} %reshape.407, bf16[3,320,2,64]{1,3,2,0:T(8,128)(2,1)S(1)} %concatenate.136), kind=kOutput, calls=%fused_computation.331 | convolution fusion | flops 65372480 | bytes 3131392 | tf_op jit(solution)/shard_map/sub | solution.py:116
  91.7 2.6 %fusion.8 = bf16[3,64,2,4,64]{1,4,3,2,0:T(8,128)(2,1)S(1)} fusion(f32[3,2,4,64,320]{4,3,2,1,0:T(8,128)} %get-tuple-element.153, f32[3,2,4,64]{3,2,1,0:T(4,128)S(1)} %get-tuple-element.152, bf16[3,320,2,64]{1,3,2,0:T(8,128)(2,1)S(1)} %concatenate.123), kind=kOutput, calls=%fused_computation.16 | convolution fusion | flops 63995904 | bytes 2414592 | tf_op jit(solution)/shard_map/skgqb,sbkd->sqkgd/dot_general | solution.py:120
  94.9 1.1 convolution_convert_fusion.2
  112.4 1.3 stack.519
  113.7 2.0 %reduce-scatter.2.cloned.1.call-done = bf16[192,512]{1,0:T(8,128)(2,1)} async-done(((bf16[192,1024]{1,0:T(8,128)(2,1)}), bf16[192,512]{1,0:T(8,128)(2,1)}) %reduce-scatter.2.cloned.1.call-update) | async-done | bytes 196624 | tf_op jit(solution)/shard_map/reduce_scatter | solution.py:167
  115.7 1.0 add_convert_fusion.1
  116.7 5.0 %all_to_all.10 = bf16[2,192,512]{2,1,0:T(8,128)(2,1)S(1)} all-to-all(bf16[2,192,512]{2,1,0:T(8,128)(2,1)S(1)} %broadcast_in_dim.52), channel_id=1, replica_groups=mesh['sp'=256,'tp'=2] {'tp'}, dimensions={0} | all-to-all | bytes 786432 | tf_op jit(solution)/shard_map/all_to_all | solution.py:29
  122.9 1.9 %collective-permute-start.7 = (bf16[192,128]{1,0:T(8,128)(2,1)S(1)}, bf16[192,128]{1,0:T(8,128)(2,1)S(1)}, u32[]{:S(2)}, u32[]{:S(2)}) collective-permute-start(bf16[192,128]{1,0:T(8,128)(2,1)S(1)} %convolution_convert_fusion.6), channel_id=1, source_target_pairs={{0,2},{2,4},{4,6},{6,8},{8,10},{10,12},{12,14},{14,16},{16,18},{18... | collective-permute-start | bytes 147464 | tf_op jit(solution)/shard_map/ppermute | solution.py:18
  124.8 4.3 %collective-permute-start.6 = (bf16[64,128]{1,0:T(8,128)(2,1)S(1)}, bf16[64,128]{1,0:T(8,128)(2,1)S(1)}, u32[]{:S(2)}, u32[]{:S(2)}) collective-permute-start(bf16[64,128]{1,0:T(8,128)(2,1)S(1)} %slice.1356), channel_id=1, source_target_pairs={{0,4},{2,6},{4,8},{6,10},{8,12},{10,14},{12,16},{14,18},{16,20},{1... | collective-permute-start | bytes 49160 | tf_op jit(solution)/shard_map/ppermute | solution.py:18
  129.4 2.5 %collective-permute-start.9 = (bf16[192,128]{1,0:T(8,128)(2,1)S(1)}, bf16[192,128]{1,0:T(8,128)(2,1)S(1)}, u32[]{:S(2)}, u32[]{:S(2)}) collective-permute-start(bf16[192,128]{1,0:T(8,128)(2,1)S(1)} %convolution_convert_fusion.5), channel_id=1, source_target_pairs={{0,2},{2,4},{4,6},{6,8},{8,10},{10,12},{12,14},{14,16},{16,18},{18... | collective-permute-start | bytes 147464 | tf_op jit(solution)/shard_map/ppermute | solution.py:18
  132.6 4.8 %collective-permute-start.8 = (bf16[64,128]{1,0:T(8,128)(2,1)S(1)}, bf16[64,128]{1,0:T(8,128)(2,1)S(1)}, u32[]{:S(2)}, u32[]{:S(2)}) collective-permute-start(bf16[64,128]{1,0:T(8,128)(2,1)S(1)} %slice.1359), channel_id=1, source_target_pairs={{0,4},{2,6},{4,8},{6,10},{8,12},{10,14},{12,16},{14,18},{16,20},{1... | collective-permute-start | bytes 49160 | tf_op jit(solution)/shard_map/ppermute | solution.py:18
  138.8 4.0 %collective-permute-done.8 = bf16[64,128]{1,0:T(8,128)(2,1)S(1)} collective-permute-done((bf16[64,128]{1,0:T(8,128)(2,1)S(1)}, bf16[64,128]{1,0:T(8,128)(2,1)S(1)}, u32[]{:S(2)}, u32[]{:S(2)}) %collective-permute-start.8) | collective-permute-done | bytes 16416 | tf_op jit(solution)/shard_map/ppermute | solution.py:18
  143.8 0.9 concatenate.153
  144.7 3.4 %fusion.192 = (f32[3,2,4,64]{3,2,1,0:T(4,128)S(1)}, f32[3,2,4,64,320]{4,3,2,1,0:T(8,128)}) fusion(f32[2,4,64,320]{3,2,1,0:T(8,128)S(1)} %bitcast.215, pred[3,64,320]{2,1,0:T(8,128)(4,1)} %compare_and_fusion, bf16[3,64,2,4,64]{4,3,2,1,0:T(4,128)(2,1)S(1)} %reshape.409, bf16[3,320,2,64]{1,3,2,0:T(8,128)(2,1)} %concatenate.153), kind=kOutput, calls=%fused_computation.332 | convolution fusion | flops 65372480 | bytes 3131392 | tf_op jit(solution)/shard_map/sub | solution.py:116
  148.3 2.7 %fusion.9 = bf16[3,64,2,4,64]{1,4,3,2,0:T(8,128)(2,1)S(1)} fusion(f32[3,2,4,64,320]{4,3,2,1,0:T(8,128)} %get-tuple-element.155, f32[3,2,4,64]{3,2,1,0:T(4,128)S(1)} %get-tuple-element.154, bf16[3,320,2,64]{1,3,2,0:T(8,128)(2,1)S(1)} %concatenate.145), kind=kOutput, calls=%fused_computation.17 | convolution fusion | flops 63995904 | bytes 2414592 | tf_op jit(solution)/shard_map/skgqb,sbkd->sqkgd/dot_general | solution.py:120
  152.0 6.0 %all_to_all.11 = bf16[2,192,512]{2,1,0:T(8,128)(2,1)S(1)} all-to-all(bf16[2,192,512]{2,1,0:T(8,128)(2,1)S(1)} %bitcast.213), channel_id=1, replica_groups=mesh['sp'=256,'tp'=2] {'tp'}, dimensions={0} | all-to-all | bytes 786432 | tf_op jit(solution)/shard_map/all_to_all | solution.py:43
  (558 shorter events, 69.8 us)
Async XLA Ops:
  6.5 88.4 %copy-start = (bf16[512,1024]{1,0:T(8,128)(2,1)S(1)}, bf16[512,1024]{1,0:T(8,128)(2,1)}, u32[]{:S(2)}) copy-start(bf16[512,1024]{1,0:T(8,128)(2,1)} %param.19) | copy-start | bytes 3145732
  6.5 109.1 %reduce-scatter.2.cloned.1.call-start = ((), (), s32[]{:S(2)}) async-start(), calls=%async_computation.3 | async-start | bytes 589824 | tf_op jit(solution)/shard_map/reduce_scatter | solution.py:167
  7.8 68.7 %collective-permute-start.3 = (bf16[192]{0:T(256)(128)(2,1)}, bf16[192]{0:T(256)(128)(2,1)S(1)}, u32[]{:S(2)}, u32[]{:S(2)}) collective-permute-start(bf16[192]{0:T(256)(128)(2,1)} %fusion.170), channel_id=1, source_target_pairs={{0,2},{2,4},{4,6},{6,8},{8,10},{10,12},{12,14},{14,16},{16,18},{18... | collective-permute-start | bytes 1160 | tf_op jit(solution)/shard_map/ppermute | solution.py:18
  12.1 68.2 %collective-permute-start.2 = (bf16[64]{0:T(256)(128)(2,1)}, bf16[64]{0:T(256)(128)(2,1)}, u32[]{:S(2)}, u32[]{:S(2)}) collective-permute-start(bf16[64]{0:T(256)(128)(2,1)} %slice.952), channel_id=1, source_target_pairs={{0,4},{2,6},{4,8},{6,10},{8,12},{10,14},{12,16},{14,18},{16,20},{1... | collective-permute-start | bytes 392 | tf_op jit(solution)/shard_map/ppermute | solution.py:18
  16.5 65.5 %collective-permute-start.5 = (bf16[192,128]{1,0:T(8,128)(2,1)}, bf16[192,128]{1,0:T(8,128)(2,1)S(1)}, u32[]{:S(2)}, u32[]{:S(2)}) collective-permute-start(bf16[192,128]{1,0:T(8,128)(2,1)} %param.15), channel_id=1, source_target_pairs={{0,2},{2,4},{4,6},{6,8},{8,10},{10,12},{12,14},{14,16},{16,18},{18... | collective-permute-start | bytes 147464 | tf_op jit(solution)/shard_map/ppermute | solution.py:18
  20.4 61.6 %collective-permute-start.4 = (bf16[64,128]{1,0:T(8,128)(2,1)}, bf16[64,128]{1,0:T(8,128)(2,1)}, u32[]{:S(2)}, u32[]{:S(2)}) collective-permute-start(bf16[64,128]{1,0:T(8,128)(2,1)} %slice.958), channel_id=1, source_target_pairs={{0,4},{2,6},{4,8},{6,10},{8,12},{10,14},{12,16},{14,18},{16,20},{1... | collective-permute-start | bytes 49160 | tf_op jit(solution)/shard_map/ppermute | solution.py:18
  25.0 62.0 %collective-permute-start.1 = (bf16[192,128]{1,0:T(8,128)(2,1)}, bf16[192,128]{1,0:T(8,128)(2,1)S(1)}, u32[]{:S(2)}, u32[]{:S(2)}) collective-permute-start(bf16[192,128]{1,0:T(8,128)(2,1)} %param.16), channel_id=1, source_target_pairs={{0,2},{2,4},{4,6},{6,8},{8,10},{10,12},{12,14},{14,16},{16,18},{18... | collective-permute-start | bytes 147464 | tf_op jit(solution)/shard_map/ppermute | solution.py:18
  40.1 19.4 %copy-start.7 = (bf16[192,512]{1,0:T(8,128)(2,1)S(1)}, bf16[192,512]{1,0:T(8,128)(2,1)}, u32[]{:S(2)}) copy-start(bf16[192,512]{1,0:T(8,128)(2,1)} %param.14) | copy-start | bytes 589828
  57.4 25.4 %copy-start.3 = (bf16[192,128]{1,0:T(8,128)(2,1)S(1)}, bf16[192,128]{1,0:T(8,128)(2,1)}, u32[]{:S(2)}) copy-start(bf16[192,128]{1,0:T(8,128)(2,1)} %param.15) | copy-start | bytes 147460
  63.3 23.7 %copy-start.4 = (bf16[192,128]{1,0:T(8,128)(2,1)S(1)}, bf16[192,128]{1,0:T(8,128)(2,1)}, u32[]{:S(2)}) copy-start(bf16[192,128]{1,0:T(8,128)(2,1)} %param.16) | copy-start | bytes 147460
  76.6 10.4 %collective-permute-start = (bf16[64,128]{1,0:T(8,128)(2,1)}, bf16[64,128]{1,0:T(8,128)(2,1)S(1)}, u32[]{:S(2)}, u32[]{:S(2)}) collective-permute-start(bf16[64,128]{1,0:T(8,128)(2,1)} %slice.943), channel_id=1, source_target_pairs={{0,4},{2,6},{4,8},{6,10},{8,12},{10,14},{12,16},{14,18},{16,20},{1... | collective-permute-start | bytes 49160 | tf_op jit(solution)/shard_map/ppermute | solution.py:18
  96.1 16.1 %copy-start.9 = (f32[1,2,4,1,320]{4,3,2,1,0:T(1,128)S(1)}, f32[1,2,4,1,320]{4,3,2,1,0:T(1,128)}, u32[]{:S(2)}) copy-start(f32[1,2,4,1,320]{4,3,2,1,0:T(1,128)} %stack.637) | copy-start | bytes 30724
  96.1 16.2 %copy-start.10 = (f32[1,2,4,1,320]{4,3,2,1,0:T(1,128)S(1)}, f32[1,2,4,1,320]{4,3,2,1,0:T(1,128)}, u32[]{:S(2)}) copy-start(f32[1,2,4,1,320]{4,3,2,1,0:T(1,128)} %stack.585) | copy-start | bytes 30724
  96.1 16.2 %copy-start.11 = (f32[1,2,4,1,320]{4,3,2,1,0:T(1,128)S(1)}, f32[1,2,4,1,320]{4,3,2,1,0:T(1,128)}, u32[]{:S(2)}) copy-start(f32[1,2,4,1,320]{4,3,2,1,0:T(1,128)} %stack.586) | copy-start | bytes 30724
  96.1 16.2 %copy-start.12 = (f32[1,2,4,1,320]{4,3,2,1,0:T(1,128)S(1)}, f32[1,2,4,1,320]{4,3,2,1,0:T(1,128)}, u32[]{:S(2)}) copy-start(f32[1,2,4,1,320]{4,3,2,1,0:T(1,128)} %stack.587) | copy-start | bytes 30724
  96.1 16.2 %copy-start.13 = (f32[1,2,4,1,320]{4,3,2,1,0:T(1,128)S(1)}, f32[1,2,4,1,320]{4,3,2,1,0:T(1,128)}, u32[]{:S(2)}) copy-start(f32[1,2,4,1,320]{4,3,2,1,0:T(1,128)} %stack.588) | copy-start | bytes 30724
  96.1 16.2 %copy-start.14 = (f32[1,2,4,1,320]{4,3,2,1,0:T(1,128)S(1)}, f32[1,2,4,1,320]{4,3,2,1,0:T(1,128)}, u32[]{:S(2)}) copy-start(f32[1,2,4,1,320]{4,3,2,1,0:T(1,128)} %stack.589) | copy-start | bytes 30724
  96.1 16.2 %copy-start.15 = (f32[1,2,4,1,320]{4,3,2,1,0:T(1,128)S(1)}, f32[1,2,4,1,320]{4,3,2,1,0:T(1,128)}, u32[]{:S(2)}) copy-start(f32[1,2,4,1,320]{4,3,2,1,0:T(1,128)} %stack.590) | copy-start | bytes 30724
  96.1 16.2 %copy-start.16 = (f32[1,2,4,1,320]{4,3,2,1,0:T(1,128)S(1)}, f32[1,2,4,1,320]{4,3,2,1,0:T(1,128)}, u32[]{:S(2)}) copy-start(f32[1,2,4,1,320]{4,3,2,1,0:T(1,128)} %stack.591) | copy-start | bytes 30724
  96.1 16.2 %copy-start.17 = (f32[1,2,4,1,320]{4,3,2,1,0:T(1,128)S(1)}, f32[1,2,4,1,320]{4,3,2,1,0:T(1,128)}, u32[]{:S(2)}) copy-start(f32[1,2,4,1,320]{4,3,2,1,0:T(1,128)} %stack.592) | copy-start | bytes 30724
  96.1 16.2 %copy-start.18 = (f32[1,2,4,1,320]{4,3,2,1,0:T(1,128)S(1)}, f32[1,2,4,1,320]{4,3,2,1,0:T(1,128)}, u32[]{:S(2)}) copy-start(f32[1,2,4,1,320]{4,3,2,1,0:T(1,128)} %stack.593) | copy-start | bytes 30724
  96.2 16.2 %copy-start.19 = (f32[1,2,4,1,320]{4,3,2,1,0:T(1,128)S(1)}, f32[1,2,4,1,320]{4,3,2,1,0:T(1,128)}, u32[]{:S(2)}) copy-start(f32[1,2,4,1,320]{4,3,2,1,0:T(1,128)} %stack.594) | copy-start | bytes 30724
  96.2 16.2 %copy-start.20 = (f32[1,2,4,1,320]{4,3,2,1,0:T(1,128)S(1)}, f32[1,2,4,1,320]{4,3,2,1,0:T(1,128)}, u32[]{:S(2)}) copy-start(f32[1,2,4,1,320]{4,3,2,1,0:T(1,128)} %stack.595) | copy-start | bytes 30724
  96.2 16.2 %copy-start.21 = (f32[1,2,4,1,320]{4,3,2,1,0:T(1,128)S(1)}, f32[1,2,4,1,320]{4,3,2,1,0:T(1,128)}, u32[]{:S(2)}) copy-start(f32[1,2,4,1,320]{4,3,2,1,0:T(1,128)} %stack.596) | copy-start | bytes 30724
  96.2 16.2 %copy-start.22 = (f32[1,2,4,1,320]{4,3,2,1,0:T(1,128)S(1)}, f32[1,2,4,1,320]{4,3,2,1,0:T(1,128)}, u32[]{:S(2)}) copy-start(f32[1,2,4,1,320]{4,3,2,1,0:T(1,128)} %stack.597) | copy-start | bytes 30724
  96.2 16.2 %copy-start.23 = (f32[1,2,4,1,320]{4,3,2,1,0:T(1,128)S(1)}, f32[1,2,4,1,320]{4,3,2,1,0:T(1,128)}, u32[]{:S(2)}) copy-start(f32[1,2,4,1,320]{4,3,2,1,0:T(1,128)} %stack.598) | copy-start | bytes 30724
  96.2 16.2 %copy-start.24 = (f32[1,2,4,1,320]{4,3,2,1,0:T(1,128)S(1)}, f32[1,2,4,1,320]{4,3,2,1,0:T(1,128)}, u32[]{:S(2)}) copy-start(f32[1,2,4,1,320]{4,3,2,1,0:T(1,128)} %stack.599) | copy-start | bytes 30724
  99.8 15.8 %copy-start.8 = (bf16[192,512]{1,0:T(8,128)(2,1)S(1)}, bf16[192,512]{1,0:T(8,128)(2,1)}, u32[]{:S(2)}) copy-start(bf16[192,512]{1,0:T(8,128)(2,1)} %param.13) | copy-start | bytes 589828
  122.9 15.0 %collective-permute-start.7 = (bf16[192,128]{1,0:T(8,128)(2,1)S(1)}, bf16[192,128]{1,0:T(8,128)(2,1)S(1)}, u32[]{:S(2)}, u32[]{:S(2)}) collective-permute-start(bf16[192,128]{1,0:T(8,128)(2,1)S(1)} %convolution_convert_fusion.6), channel_id=1, source_target_pairs={{0,2},{2,4},{4,6},{6,8},{8,10},{10,12},{12,14},{14,16},{16,18},{18... | collective-permute-start | bytes 147464 | tf_op jit(solution)/shard_map/ppermute | solution.py:18
  124.8 13.0 %collective-permute-start.6 = (bf16[64,128]{1,0:T(8,128)(2,1)S(1)}, bf16[64,128]{1,0:T(8,128)(2,1)S(1)}, u32[]{:S(2)}, u32[]{:S(2)}) collective-permute-start(bf16[64,128]{1,0:T(8,128)(2,1)S(1)} %slice.1356), channel_id=1, source_target_pairs={{0,4},{2,6},{4,8},{6,10},{8,12},{10,14},{12,16},{14,18},{16,20},{1... | collective-permute-start | bytes 49160 | tf_op jit(solution)/shard_map/ppermute | solution.py:18
  129.4 13.5 %collective-permute-start.9 = (bf16[192,128]{1,0:T(8,128)(2,1)S(1)}, bf16[192,128]{1,0:T(8,128)(2,1)S(1)}, u32[]{:S(2)}, u32[]{:S(2)}) collective-permute-start(bf16[192,128]{1,0:T(8,128)(2,1)S(1)} %convolution_convert_fusion.5), channel_id=1, source_target_pairs={{0,2},{2,4},{4,6},{6,8},{8,10},{10,12},{12,14},{14,16},{16,18},{18... | collective-permute-start | bytes 147464 | tf_op jit(solution)/shard_map/ppermute | solution.py:18
  132.6 10.2 %collective-permute-start.8 = (bf16[64,128]{1,0:T(8,128)(2,1)S(1)}, bf16[64,128]{1,0:T(8,128)(2,1)S(1)}, u32[]{:S(2)}, u32[]{:S(2)}) collective-permute-start(bf16[64,128]{1,0:T(8,128)(2,1)S(1)} %slice.1359), channel_id=1, source_target_pairs={{0,4},{2,6},{4,8},{6,10},{8,12},{10,14},{12,16},{14,18},{16,20},{1... | collective-permute-start | bytes 49160 | tf_op jit(solution)/shard_map/ppermute | solution.py:18
  (8 other events, 72.6 us)
Sparse Core Ops, SparseCore 0:
  96.4 19.2 reduce-scatter.1
where the time goes:
time: 167 us; the launch traced here: 166 us
  local copies, waits for them, and re-layouts  72.2 us (43%)
  starting transfers between devices  34.6 us (21%)
  between operations  14.7 us (9%)
  matrix products  14.4 us (9%)
  blocking collectives  11 us (7%)
  other arithmetic  9.41 us (6%)
  waiting for transfers between devices  9.31 us (6%)
    unnamed x314, local copies, waits for them, and re-layouts  40 us
    ppermute x10, starting transfers between devices, from_behind(): return lax.ppermute(block, axis, route)  34.6 us
    another operation x130, local copies, waits for them, and re-layouts, bias_block(): return jnp.stack(rows, axis=1)  14.6 us
    concatenate x46, local copies, waits for them, and re-layouts, make_bands(): jnp.concatenate([blocks[lag:lag + segments] for lag in range(PAST + 1)],...  7.81 us
    ppermute x10, waiting for transfers between devices, from_behind(): return lax.ppermute(block, axis, route)  7.33 us
    sub x2, matrix products, attend(): softmax_weight = jnp.exp(logit_scores - largest)  6.7 us
    all_to_all x1, blocking collectives, sent_and_summed(): pieces = lax.all_to_all(cut_along(x, dim, length), axis, 0, 0, tiled=True)  6.04 us
    dot_general x2, matrix products, attend(): jnp.einsum('skgqb,sbkd->sqkgd', softmax_weight, value_bands, preferred_el...  5.33 us
  transfers between devices with their start and end apart: 11, of which 3 were waited for; matrix products, arithmetic and copies ran while one was open for 44% of the time, Pallas kernels for 0%

commit v1 on v0

v1 whole, which is shorter than its diff:
```python
import functools

import jax
import jax.numpy as jnp
from jax import lax
from jax.experimental import pallas as pl
from jax.experimental.pallas import tpu as pltpu
from jax.sharding import PartitionSpec as P

HEAD_SIZE = 64
SEG = 64
PAST = 4
EPS = 1e-06
BAND = SEG * (PAST + 1)
WIDE = 384
TILE = 128
NEG = -1e30
F32 = jnp.float32
BF16 = jnp.bfloat16

GROUP_HEADS = ((0, 2, 5, 7), (1, 3, 4, 6))


def whole():
    return pl.BlockSpec(memory_space=pltpu.VMEM)


def params(mib):
    return pltpu.CompilerParams(vmem_limit_bytes=mib * 1024 * 1024)


def shape(*dims, dtype=BF16):
    return jax.ShapeDtypeStruct(dims, dtype)


def cost(flops, transcendentals=0, nbytes=1 << 20):
    return pl.CostEstimate(flops=flops, bytes_accessed=nbytes, transcendentals=transcendentals)


def from_behind(block, distance):
    devices = range(lax.axis_size("sp"))
    route = [(i - distance, i) for i in devices if i - distance in devices]
    return lax.ppermute(block, "sp", route)


def pack_kernel(key_ref, value_ref, doc_ref, near_ref, far_ref, line):
    rows = key_ref.shape[0]
    near_ref[0:rows, 0:TILE] = key_ref[...]
    near_ref[0:rows, TILE : 2 * TILE] = value_ref[...]
    far_ref[0:SEG, 0:TILE] = key_ref[rows - SEG : rows, :]
    far_ref[0:SEG, TILE : 2 * TILE] = value_ref[rows - SEG : rows, :]
    line[...] = jnp.zeros_like(line)
    codes = (doc_ref[...] + 1).astype(F32)
    line[:, 0:rows] = jnp.broadcast_to(codes, (8, rows))
    flat = line[...]
    lanes = lax.broadcasted_iota(jnp.int32, flat.shape, 1)
    near = pltpu.roll(flat, SEG, 1)
    far = jnp.where(lanes < SEG, pltpu.roll(flat, 2 * TILE - (rows - SEG), 1), 0.0)
    near_ref[rows : rows + 16, :] = jnp.concatenate([near, near], axis=0).astype(BF16)
    far_ref[SEG : SEG + 16, :] = jnp.concatenate([far, far], axis=0).astype(BF16)


def fill_bias(table_ref, bias):
    table = table_ref[:, 0 : 4 * TILE]
    last = table_ref[:, 4 * TILE : 4 * TILE + 1]
    lanes = lax.broadcasted_iota(jnp.int32, table.shape, 1)
    moved = jnp.where(lanes < 448, pltpu.roll(table, 448, 1), jnp.broadcast_to(last, table.shape))
    mirror = 127 - lax.broadcasted_iota(jnp.int32, (8, TILE), 1)
    pieces = [
        jnp.take_along_axis(moved[:, TILE * t : TILE * (t + 1)], mirror, axis=1)
        for t in (3, 2, 1, 0)
    ]
    line = jnp.concatenate(pieces, axis=1)
    for group in range(2):
        for block, head in enumerate(GROUP_HEADS[group]):
            rows = jnp.broadcast_to(line[head : head + 1, :], (SEG, 4 * TILE))
            turned = pltpu.roll(rows, 449, 1, stride=1, stride_axis=0)
            bias[group, SEG * block : SEG * (block + 1), :] = turned[:, 0:WIDE]


def fill_band(src, row, dst, dst_swapped):
    count = src.shape[0]
    dst[row : row + count, :] = src
    for t in range(2):
        part = src[:, TILE * t : TILE * (t + 1)].astype(F32)
        dst_swapped[row : row + count, TILE * t : TILE * (t + 1)] = pltpu.roll(part, SEG, 1).astype(BF16)


def key_codes(doc_ref, near_code, far_code, line):
    rows = doc_ref.shape[1]
    line[...] = jnp.zeros_like(line)
    line[:, 0 : 2 * TILE] = near_code if far_code is None else near_code + far_code
    line[:, 2 * TILE : 2 * TILE + rows] = jnp.broadcast_to((doc_ref[...] + 1).astype(F32), (8, rows))
    return line[...]


def segment_mask(codes, segment):
    turned = codes if segment == 0 else pltpu.roll(codes, 512 - SEG * segment, 1)
    band = jnp.broadcast_to(turned[0:1, 0:WIDE], (SEG, WIDE))
    lanes = lax.broadcasted_iota(jnp.int32, (SEG, WIDE), 1)
    rows = lax.broadcasted_iota(jnp.int32, (SEG, WIDE), 0)
    own = jnp.sum(jnp.where(lanes == rows + PAST * SEG, band, 0.0), axis=1, keepdims=True)
    return jnp.where((band == own) & (lanes < BAND), 0.0, NEG)


def segment_attention(query, band, band_swapped, first_row, mask, bias):
    lanes = lax.broadcasted_iota(jnp.int32, (1, TILE), 1)
    scale = HEAD_SIZE ** (-0.5)
    low = jnp.where(lanes < HEAD_SIZE, scale, 0.0).astype(BF16)
    high = jnp.where(lanes < HEAD_SIZE, 0.0, scale).astype(BF16)
    results = []
    for group in range(2):
        source = band if group == 0 else band_swapped
        keys = source[first_row : first_row + WIDE, 0:TILE]
        values = source[first_row : first_row + WIDE, TILE : 2 * TILE]
        stacked = []
        for tile in range(4):
            even = (tile < 2) == (group == 0)
            stacked.append(query[:, TILE * tile : TILE * (tile + 1)] * (low if even else high))
        left = jnp.concatenate(stacked, axis=0)
        scores = lax.dot_general(left, keys, (((1,), (1,)), ((), ())), preferred_element_type=F32)
        weights = []
        shares = []
        for block in range(4):
            rows = slice(SEG * block, SEG * (block + 1))
            s = scores[rows] + bias[group, rows, :] + mask
            largest = jnp.max(s, axis=1, keepdims=True)
            e = jnp.exp(s - largest)
            shares.append(1.0 / jnp.sum(e, axis=1, keepdims=True))
            weights.append(e.astype(BF16))
        blended = jnp.dot(jnp.concatenate(weights, axis=0), values, preferred_element_type=F32)
        results.append([blended[SEG * b : SEG * (b + 1)] * shares[b] for b in range(4)])
    outs = []
    for tile in range(4):
        even, odd = (0, 1) if tile < 2 else (1, 0)
        outs.append(jnp.where(lanes < HEAD_SIZE, results[even][tile], results[odd][tile]))
    return jnp.concatenate(outs, axis=1)


def later_segments(query, own, near, codes, bias, band, band_swapped, mixed_ref):
    fill_band(near, SEG, band, band_swapped)
    fill_band(own, 4 * SEG, band, band_swapped)
    band[7 * SEG :, :] = jnp.zeros((SEG, 2 * TILE), BF16)
    band_swapped[7 * SEG :, :] = jnp.zeros((SEG, 2 * TILE), BF16)
    for segment in (1, 2):
        out = segment_attention(
            query[SEG * segment : SEG * (segment + 1), :],
            band,
            band_swapped,
            SEG * segment,
            segment_mask(codes, segment),
            bias,
        )
        mixed_ref[SEG * (segment - 1) : SEG * segment, :] = out.astype(BF16)


def first_segment(query, own, near, far, codes, bias, band, band_swapped):
    fill_band(far, 0, band, band_swapped)
    fill_band(near, SEG, band, band_swapped)
    fill_band(own, 4 * SEG, band, band_swapped)
    return segment_attention(query, band, band_swapped, 0, segment_mask(codes, 0), bias).astype(BF16)


def later_one_kernel(query_ref, key_ref, value_ref, doc_ref, near_ref, table_ref, mixed_ref, bias, band, swapped, line):
    rows = key_ref.shape[0]
    fill_bias(table_ref, bias)
    codes = key_codes(doc_ref, near_ref[rows : rows + 8, :].astype(F32), None, line)
    own = jnp.concatenate([key_ref[...], value_ref[...]], axis=1)
    later_segments(query_ref[...], own, near_ref[0:rows, :], codes, bias, band, swapped, mixed_ref)


def first_one_kernel(
    query_ref, key_ref, value_ref, doc_ref, near_ref, far_ref, table_ref, mixed_ref, weight_ref, residual_ref,
    out_ref, bias, band, swapped, line,
):
    rows = key_ref.shape[0]
    fill_bias(table_ref, bias)
    codes = key_codes(
        doc_ref, near_ref[rows : rows + 8, :].astype(F32), far_ref[SEG : SEG + 8, :].astype(F32), line
    )
    own = jnp.concatenate([key_ref[0:TILE, :], value_ref[0:TILE, :]], axis=1)
    head = first_segment(
        query_ref[0:SEG, :], own, near_ref[0:rows, :], far_ref[0:SEG, :], codes, bias, band, swapped
    )
    mixed = jnp.concatenate([head, mixed_ref[...]], axis=0)
    partial = jnp.dot(mixed, weight_ref[...], preferred_element_type=F32)
    mine = (lax.axis_index("tp") == 0).astype(F32)
    residual = residual_ref[...].astype(F32)
    half = residual.shape[1]
    out_ref[:, 0:half] = (partial[:, 0:half] + residual * mine).astype(BF16)
    out_ref[:, half:] = (partial[:, half:] + residual * (1.0 - mine)).astype(BF16)


def norm_kernel(both_ref, gain_ref, key_w_ref, value_w_ref, kv_ref, tail_ref, normed_ref, share_ref):
    layer = (both_ref[0].astype(F32) + both_ref[1].astype(F32)).astype(BF16)
    wide = layer.astype(F32)
    rows, channels = wide.shape
    scale = lax.rsqrt(jnp.mean(wide * wide, axis=1, keepdims=True) + EPS)
    normed = (wide * scale * gain_ref[...]).astype(BF16)
    keys = jnp.dot(normed, key_w_ref[...], preferred_element_type=F32).astype(BF16)
    values = jnp.dot(normed, value_w_ref[...], preferred_element_type=F32).astype(BF16)
    kv_ref[:, 0:TILE] = keys
    kv_ref[:, TILE : 2 * TILE] = values
    tail_ref[:, 0:TILE] = keys[rows - SEG :]
    tail_ref[:, TILE : 2 * TILE] = values[rows - SEG :]
    normed_ref[...] = normed
    half = channels // 2
    share_ref[...] = jnp.where(lax.axis_index("tp") == 0, wide[:, 0:half], wide[:, half:]).astype(BF16)


def later_two_kernel(
    normed_ref, weight_ref, kv_ref, doc_ref, near_ref, codes_ref, table_ref, mixed_ref, head_ref,
    bias, band, swapped, line,
):
    rows = kv_ref.shape[0]
    fill_bias(table_ref, bias)
    query = jnp.dot(normed_ref[...], weight_ref[...], preferred_element_type=F32).astype(BF16)
    head_ref[...] = query[0:SEG, :]
    codes = key_codes(doc_ref, codes_ref[rows : rows + 8, :].astype(F32), None, line)
    later_segments(query, kv_ref[...], near_ref[...], codes, bias, band, swapped, mixed_ref)


def first_two_kernel(
    head_ref, kv_ref, doc_ref, near_ref, far_ref, near_codes_ref, far_codes_ref, table_ref, mixed_ref, weight_ref,
    out_ref, bias, band, swapped, line,
):
    rows = kv_ref.shape[0]
    fill_bias(table_ref, bias)
    codes = key_codes(
        doc_ref, near_codes_ref[rows : rows + 8, :].astype(F32), far_codes_ref[SEG : SEG + 8, :].astype(F32), line
    )
    head = first_segment(
        head_ref[...], kv_ref[0:TILE, :], near_ref[...], far_ref[...], codes, bias, band, swapped
    )
    mixed = jnp.concatenate([head, mixed_ref[...]], axis=0)
    out_ref[...] = jnp.dot(mixed, weight_ref[...], preferred_element_type=F32).astype(BF16)


def last_kernel(both_ref, share_ref, out_ref):
    half = share_ref.shape[1]
    mine = pl.ds(pl.multiple_of(lax.axis_index("tp") * half, half), half)
    out_ref[...] = (
        share_ref[...].astype(F32) + both_ref[0, :, mine].astype(F32) + both_ref[1, :, mine].astype(F32)
    ).astype(BF16)


def call(kernel, outs, scratch, args, flops, mib=16):
    return pl.pallas_call(
        kernel,
        out_shape=outs,
        in_specs=[whole()] * len(args),
        out_specs=jax.tree.map(lambda _: whole(), outs),
        scratch_shapes=scratch,
        compiler_params=params(mib),
        cost_estimate=cost(flops),
    )(*args)


def body(
    residual,
    query_first,
    key_first,
    value_first,
    documents,
    bias_first,
    out_first,
    norm_gain,
    query_w,
    key_w,
    value_w,
    bias_second,
    out_second,
):
    rows, half = residual.shape
    width = query_first.shape[1]
    channels = out_first.shape[1]
    docs = documents.reshape(1, rows)
    gain = norm_gain.reshape(1, channels)
    attention_scratch = [
        pltpu.VMEM((2, 4 * SEG, WIDE), F32),
        pltpu.VMEM((8 * SEG, 2 * TILE), BF16),
        pltpu.VMEM((8 * SEG, 2 * TILE), BF16),
        pltpu.VMEM((8, 4 * TILE), F32),
    ]
    near_send, far_send = call(
        pack_kernel,
        (shape(rows + 16, 2 * TILE), shape(SEG + 16, 2 * TILE)),
        [pltpu.VMEM((8, 2 * TILE), F32)],
        (key_first, value_first, docs),
        1 << 20,
    )
    near_one = from_behind(near_send, 1)
    far_one = from_behind(far_send, 2)
    later_one = call(
        later_one_kernel,
        shape(rows - SEG, width),
        attention_scratch,
        (query_first, key_first, value_first, docs, near_one, bias_first),
        1 << 31,
    )
    sent_one = call(
        first_one_kernel,
        shape(rows, channels),
        attention_scratch,
        (query_first, key_first, value_first, docs, near_one, far_one, bias_first, later_one, out_first, residual),
        1 << 30,
    )
    both_one = lax.all_gather(sent_one, "tp", axis=0)
    kv_two, tail_two, normed, share = call(
        norm_kernel,
        (shape(rows, 2 * TILE), shape(SEG, 2 * TILE), shape(rows, channels), shape(rows, half)),
        [],
        (both_one, gain, key_w, value_w),
        1 << 30,
    )
    near_two = from_behind(kv_two, 1)
    far_two = from_behind(tail_two, 2)
    later_two, head_two = call(
        later_two_kernel,
        (shape(rows - SEG, width), shape(SEG, width)),
        attention_scratch,
        (normed, query_w, kv_two, docs, near_two, near_one, bias_second),
        1 << 31,
    )
    sent_two = call(
        first_two_kernel,
        shape(rows, channels),
        attention_scratch,
        (head_two, kv_two, docs, near_two, far_two, near_one, far_one, bias_second, later_two, out_second),
        1 << 30,
    )
    both_two = lax.all_gather(sent_two, "tp", axis=0)
    return call(last_kernel, shape(rows, half), [], (both_two, share), 1 << 20)


def solution(mesh):
    placed = (
        P("sp", "tp"),
        P("sp", "tp"),
        P("sp", "tp"),
        P("sp", "tp"),
        P("sp"),
        P("tp", None),
        P("tp", None),
        P(),
        P(None, "tp"),
        P(None, "tp"),
        P(None, "tp"),
        P("tp", None),
        P("tp", None),
    )
    return jax.shard_map(body, mesh=mesh, in_specs=placed, out_specs=P("sp", "tp"), check_vma=False)
```

time: 167 us -> 42.9 us (0.26)
  local copies, waits for them, and re-layouts: 72.2 us -> 3.25 us
  starting transfers between devices: 34.6 us -> 12.6 us
  between operations: 14.7 us -> 0.15 us
  matrix products: 14.4 us -> 0 us
  other arithmetic: 9.41 us -> 0 us
  Pallas kernels: 0 us -> 8.86 us
  blocking collectives: 11 us -> 7.62 us
    unnamed x314 -> x26, local copies, waits for them, and re-layouts: 40 us -> 3.25 us
    ppermute x10 -> x4, starting transfers between devices: 34.6 us -> 12.6 us  [from_behind(): return lax.ppermute(block, 'sp', route)]
    another operation x130 -> x0, local copies, waits for them, and re-layouts: 14.6 us -> none  [bias_block(): return jnp.stack(rows, axis=1)]
    all_to_all x2 -> x0, blocking collectives: 11 us -> none  [the longest x1 6.04 us: sent_and_summed(): pieces = lax.all_to_all(cut_along(x, dim, length), axis, 0, 0, tiled=True)]
    pallas_call x0 -> x7, Pallas kernels: none -> 8.86 us  [call(): pl.pallas_call(kernel, out_shape=outs, in_specs=[whole()] * len(args), ou...]
    concatenate x49 -> x0, local copies, waits for them, and re-layouts: 8.57 us -> none  [the longest x46 7.81 us: make_bands(): jnp.concatenate([blocks[lag:lag + segments] for lag in range(PAST + 1)],...]
    dot_general x7 -> x0, matrix products: 7.72 us -> none  [the longest x2 5.33 us: attend(): jnp.einsum('skgqb,sbkd->sqkgd', softmax_weight, value_bands, preferred_el...]
    all_gather x0 -> x2, blocking collectives: none -> 7.62 us  [the longest x1 3.81 us: body(): both_one = lax.all_gather(sent_one, 'tp', axis=0)]
  transfers between devices with their start and end apart: 11 -> 4, of which waited for: 3 -> 3; matrix products, arithmetic and copies ran while one was open for 44% -> 0% of each run, Pallas kernels for 0% -> 10%
where the time goes in v1:
time: 42.9 us; the launch traced here: 42.5 us
  starting transfers between devices  12.6 us (29%)
  waiting for transfers between devices  9.97 us (23%)
  Pallas kernels  8.86 us (21%)
  blocking collectives  7.62 us (18%)
  local copies, waits for them, and re-layouts  3.25 us (8%)
    ppermute x4, starting transfers between devices, from_behind(): return lax.ppermute(block, 'sp', route)  12.6 us
    ppermute x4, waiting for transfers between devices, from_behind(): return lax.ppermute(block, 'sp', route)  9.97 us
    pallas_call x7, Pallas kernels, call(): pl.pallas_call(kernel, out_shape=outs, in_specs=[whole()] * len(args), ou...  8.86 us
    all_gather x1, blocking collectives, body(): both_one = lax.all_gather(sent_one, 'tp', axis=0)  3.81 us
    all_gather x1, blocking collectives, body(): both_two = lax.all_gather(sent_two, 'tp', axis=0)  3.81 us
    unnamed x26, local copies, waits for them, and re-layouts  3.25 us
  transfers between devices with their start and end apart: 4, of which 3 were waited for; matrix products, arithmetic and copies ran while one was open for 0% of the time, Pallas kernels for 10%

profile of v1, /device:TPU:129, one launch (start us, length us, event | category | flops | bytes accessed | tf_op | source)
XLA Modules:
  0.0 42.5 jit_solution(14226572970086462341)
XLA Ops:
  0.0 0.7 %copy-done.2 = s32[192]{0:T(256)S(1)} copy-done((s32[192]{0:T(256)S(1)}, s32[192]{0:T(256)}, u32[]{:S(2)}) %copy-start.2) | copy-done | bytes 792
  0.7 0.8 %copy-done = bf16[192,128]{1,0:T(8,128)(2,1)S(1)} copy-done((bf16[192,128]{1,0:T(8,128)(2,1)S(1)}, bf16[192,128]{1,0:T(8,128)(2,1)}, u32[]{:S(2)}) %copy-start) | copy-done | bytes 49176
  1.5 0.8 %copy-done.1 = bf16[192,128]{1,0:T(8,128)(2,1)S(1)} copy-done((bf16[192,128]{1,0:T(8,128)(2,1)S(1)}, bf16[192,128]{1,0:T(8,128)(2,1)}, u32[]{:S(2)}) %copy-start.1) | copy-done | bytes 49176
  2.3 0.1 shard_map.127
  2.4 3.1 %collective-permute-start = (bf16[208,256]{1,0:T(8,128)(2,1)S(1)}, bf16[208,256]{1,0:T(8,128)(2,1)S(1)}, u32[]{:S(2)}, u32[]{:S(2)}) collective-permute-start(bf16[208,256]{1,0:T(8,128)(2,1)S(1)} %get-tuple-element.13), channel_id=1, source_target_pairs={{0,2},{2,4},{4,6},{6,8},{8,10},{10,12},{12,14},{14,16},{16,18},{18... | collective-permute-start | bytes 319496 | tf_op jit(solution)/shard_map/ppermute | solution.py:43
  5.5 0.0 copy-start.3
  5.5 4.5 %collective-permute-start.1 = (bf16[80,256]{1,0:T(8,128)(2,1)S(1)}, bf16[80,256]{1,0:T(8,128)(2,1)S(1)}, u32[]{:S(2)}, u32[]{:S(2)}) collective-permute-start(bf16[80,256]{1,0:T(8,128)(2,1)S(1)} %get-tuple-element.14), channel_id=1, source_target_pairs={{0,4},{2,6},{4,8},{6,10},{8,12},{10,14},{12,16},{14,18},{16,20},{1... | collective-permute-start | bytes 122888 | tf_op jit(solution)/shard_map/ppermute | solution.py:43
  10.0 3.5 %collective-permute-done.near_ref.codes_ref.near_codes_ref = bf16[208,256]{1,0:T(8,128)(2,1)S(1)} collective-permute-done((bf16[208,256]{1,0:T(8,128)(2,1)S(1)}, bf16[208,256]{1,0:T(8,128)(2,1)S(1)}, u32[]{:S(2)}, u32[]{:S(2)}) %collective-permute-start) | collective-permute-done | bytes 106528 | tf_op jit(solution)/shard_map/ppermute | solution.py:43
  13.5 0.0 copy-done.10
  13.5 0.9 %copy-done.8 = bf16[192,512]{1,0:T(8,128)(2,1)S(1)} copy-done((bf16[192,512]{1,0:T(8,128)(2,1)S(1)}, bf16[192,512]{1,0:T(8,128)(2,1)}, u32[]{:S(2)}) %copy-start.8) | copy-done | bytes 196632
  14.5 2.0 %shard_map.128.mixed_ref = bf16[128,512]{1,0:T(8,128)(2,1)S(1)} custom-call(bf16[192,512]{1,0:T(8,128)(2,1)S(1)} %copy-done.8, bf16[192,128]{1,0:T(8,128)(2,1)S(1)} %copy-done, bf16[192,128]{1,0:T(8,128)(2,1)S(1)} %copy-done.1, s32[1,192]{1,0:T(1,128)S(1)} %bitcast.7, bf16[208,256]{1,0:T(8,128)(2,1)S(1)} %collective-permute-done.near_ref.codes_ref.near_codes_ref, ...), custom_call_target="tpu_custom_call" | custom-call | flops 2147483648 | bytes 1048576 | tf_op jit(solution)/shard_map/pallas_call | solution.py:248
  16.5 0.0 collective-permute-done.1.far_ref.far_codes_ref
  16.5 0.0 copy-done.3
  16.5 0.0 copy-done.9
  16.5 1.7 %shard_map.129 = bf16[192,1024]{1,0:T(8,128)(2,1)S(1)} custom-call(bf16[192,512]{1,0:T(8,128)(2,1)S(1)} %copy-done.8, bf16[192,128]{1,0:T(8,128)(2,1)S(1)} %copy-done, bf16[192,128]{1,0:T(8,128)(2,1)S(1)} %copy-done.1, s32[1,192]{1,0:T(1,128)S(1)} %bitcast.8, bf16[208,256]{1,0:T(8,128)(2,1)S(1)} %collective-permute-done.near_ref.codes_ref.near_codes_ref, ...), custom_call_target="tpu_custom_call" | custom-call | flops 1073741824 | bytes 1048576 | tf_op jit(solution)/shard_map/pallas_call | solution.py:248
  18.2 0.0 copy-start.6
  18.2 0.0 copy-start.7
  18.3 0.0 copy-start.12
  18.3 3.8 %all-gather = bf16[384,1024]{1,0:T(8,128)(2,1)S(1)} all-gather(bf16[192,1024]{1,0:T(8,128)(2,1)S(1)} %shard_map.129), channel_id=2, replica_groups=mesh['sp'=256,'tp'=2] {'tp'}, dimensions={0}, use_global_device_ids=true | all-gather | bytes 1179648 | tf_op jit(solution)/shard_map/all_gather | solution.py:308
  22.1 0.0 copy-done.6
  22.1 0.0 copy-done.12
  22.1 0.0 copy-start.11
  22.1 0.6 %shard_map.130 = (bf16[192,256]{1,0:T(8,128)(2,1)S(1)}, bf16[64,256]{1,0:T(8,128)(2,1)S(1)}, bf16[192,1024]{1,0:T(8,128)(2,1)S(1)}, bf16[192,512]{1,0:T(8,128)(2,1)S(1)}) custom-call(bf16[2,192,1024]{2,1,0:T(8,128)(2,1)S(1)} %bitcast.5, f32[1,1024]{1,0:T(1,128)S(1)} %bitcast.11, bf16[1024,128]{1,0:T(8,128)(2,1)S(1)} %copy-done.6, bf16[1024,128]{1,0:T(8,128)(2,1)S(1)} %copy-done.7), custom_call_target="tpu_custom_call" | custom-call | flops 1073741824 | bytes 1048576 | tf_op jit(solution)/shard_map/pallas_call | solution.py:248
  22.7 3.1 %collective-permute-start.2 = (bf16[192,256]{1,0:T(8,128)(2,1)S(1)}, bf16[192,256]{1,0:T(8,128)(2,1)S(1)}, u32[]{:S(2)}, u32[]{:S(2)}) collective-permute-start(bf16[192,256]{1,0:T(8,128)(2,1)S(1)} %get-tuple-element.16.kv_ref), channel_id=1, source_target_pairs={{0,2},{2,4},{4,6},{6,8},{8,10},{10,12},{12,14},{14,16},{16,18},{18... | collective-permute-start | bytes 294920 | tf_op jit(solution)/shard_map/ppermute | solution.py:43
  25.8 1.9 %collective-permute-start.3 = (bf16[64,256]{1,0:T(8,128)(2,1)S(1)}, bf16[64,256]{1,0:T(8,128)(2,1)S(1)}, u32[]{:S(2)}, u32[]{:S(2)}) collective-permute-start(bf16[64,256]{1,0:T(8,128)(2,1)S(1)} %get-tuple-element.18), channel_id=1, source_target_pairs={{0,4},{2,6},{4,8},{6,10},{8,12},{10,14},{12,16},{14,18},{16,20},{1... | collective-permute-start | bytes 98312 | tf_op jit(solution)/shard_map/ppermute | solution.py:43
  27.7 6.2 %collective-permute-done.2.near_ref = bf16[192,256]{1,0:T(8,128)(2,1)S(1)} collective-permute-done((bf16[192,256]{1,0:T(8,128)(2,1)S(1)}, bf16[192,256]{1,0:T(8,128)(2,1)S(1)}, u32[]{:S(2)}, u32[]{:S(2)}) %collective-permute-start.2) | collective-permute-done | bytes 98336 | tf_op jit(solution)/shard_map/ppermute | solution.py:43
  34.0 2.0 %shard_map.131 = (bf16[128,512]{1,0:T(8,128)(2,1)S(1)}, bf16[64,512]{1,0:T(8,128)(2,1)S(1)}) custom-call(bf16[192,1024]{1,0:T(8,128)(2,1)S(1)} %get-tuple-element.15.normed_ref, bf16[1024,512]{1,0:T(8,128)(2,1)S(1)} %copy-done.4, bf16[192,256]{1,0:T(8,128)(2,1)S(1)} %get-tuple-element.16.kv_ref, s32[1,192]{1,0:T(1,128)S(1)} %bitcast.9, ...), custom_call_target="tpu_custom_call" | custom-call | flops 2147483648 | bytes 1048576 | tf_op jit(solution)/shard_map/pallas_call | solution.py:248
  36.0 0.2 collective-permute-done.3.far_ref
  36.2 0.0 copy-done.5
  36.2 1.7 %shard_map.132 = bf16[192,1024]{1,0:T(8,128)(2,1)S(1)} custom-call(bf16[64,512]{1,0:T(8,128)(2,1)S(1)} %get-tuple-element.17.head_ref, bf16[192,256]{1,0:T(8,128)(2,1)S(1)} %get-tuple-element.16.kv_ref, s32[1,192]{1,0:T(1,128)S(1)} %bitcast.10, bf16[192,256]{1,0:T(8,128)(2,1)S(1)} %collective-permute-done.2.near_ref, ...), custom_call_target="tpu_custom_call" | custom-call | flops 1073741824 | bytes 1048576 | tf_op jit(solution)/shard_map/pallas_call | solution.py:248
  37.9 3.8 %all-gather.1 = bf16[384,1024]{1,0:T(8,128)(2,1)S(1)} all-gather(bf16[192,1024]{1,0:T(8,128)(2,1)S(1)} %shard_map.132), channel_id=3, replica_groups=mesh['sp'=256,'tp'=2] {'tp'}, dimensions={0}, use_global_device_ids=true | all-gather | bytes 1179648 | tf_op jit(solution)/shard_map/all_gather | solution.py:332
  41.7 0.8 %shard_map.133 = bf16[192,512]{1,0:T(8,128)(2,1)} custom-call(bf16[2,192,1024]{2,1,0:T(8,128)(2,1)S(1)} %bitcast.4, bf16[192,512]{1,0:T(8,128)(2,1)S(1)} %get-tuple-element.20.share_ref), custom_call_target="tpu_custom_call" | custom-call | flops 1048576 | bytes 1048576 | tf_op jit(solution)/shard_map/pallas_call | solution.py:248
  (11 shorter events, 0.0 us)
Async XLA Ops:
  0.0 0.7 %copy-start.2 = (s32[192]{0:T(256)S(1)}, s32[192]{0:T(256)}, u32[]{:S(2)}) copy-start(s32[192]{0:T(256)} %param.17) | copy-start | bytes 2308
  0.7 0.8 %copy-start = (bf16[192,128]{1,0:T(8,128)(2,1)S(1)}, bf16[192,128]{1,0:T(8,128)(2,1)}, u32[]{:S(2)}) copy-start(bf16[192,128]{1,0:T(8,128)(2,1)} %key_ref.5) | copy-start | bytes 147460
  1.5 0.8 %copy-start.1 = (bf16[192,128]{1,0:T(8,128)(2,1)S(1)}, bf16[192,128]{1,0:T(8,128)(2,1)}, u32[]{:S(2)}) copy-start(bf16[192,128]{1,0:T(8,128)(2,1)} %value_ref.5) | copy-start | bytes 147460
  2.3 11.3 %copy-start.10 = (f32[8,513]{1,0:T(8,128)S(1)}, f32[8,513]{1,0:T(8,128)}, u32[]{:S(2)}) copy-start(f32[8,513]{1,0:T(8,128)} %table_ref.5) | copy-start | bytes 49252
  2.4 11.2 %collective-permute-start = (bf16[208,256]{1,0:T(8,128)(2,1)S(1)}, bf16[208,256]{1,0:T(8,128)(2,1)S(1)}, u32[]{:S(2)}, u32[]{:S(2)}) collective-permute-start(bf16[208,256]{1,0:T(8,128)(2,1)S(1)} %get-tuple-element.13), channel_id=1, source_target_pairs={{0,2},{2,4},{4,6},{6,8},{8,10},{10,12},{12,14},{14,16},{16,18},{18... | collective-permute-start | bytes 319496 | tf_op jit(solution)/shard_map/ppermute | solution.py:43
  5.5 11.0 %copy-start.3 = (bf16[512,1024]{1,0:T(8,128)(2,1)S(1)}, bf16[512,1024]{1,0:T(8,128)(2,1)}, u32[]{:S(2)}) copy-start(bf16[512,1024]{1,0:T(8,128)(2,1)} %weight_ref.3) | copy-start | bytes 3145732
  5.5 11.0 %collective-permute-start.1 = (bf16[80,256]{1,0:T(8,128)(2,1)S(1)}, bf16[80,256]{1,0:T(8,128)(2,1)S(1)}, u32[]{:S(2)}, u32[]{:S(2)}) collective-permute-start(bf16[80,256]{1,0:T(8,128)(2,1)S(1)} %get-tuple-element.14), channel_id=1, source_target_pairs={{0,4},{2,6},{4,8},{6,10},{8,12},{10,14},{12,16},{14,18},{16,20},{1... | collective-permute-start | bytes 122888 | tf_op jit(solution)/shard_map/ppermute | solution.py:43
  13.5 0.9 %copy-start.8 = (bf16[192,512]{1,0:T(8,128)(2,1)S(1)}, bf16[192,512]{1,0:T(8,128)(2,1)}, u32[]{:S(2)}) copy-start(bf16[192,512]{1,0:T(8,128)(2,1)} %query_ref.3) | copy-start | bytes 589828
  14.5 2.1 %copy-start.9 = (bf16[192,512]{1,0:T(8,128)(2,1)S(1)}, bf16[192,512]{1,0:T(8,128)(2,1)}, u32[]{:S(2)}) copy-start(bf16[192,512]{1,0:T(8,128)(2,1)} %residual_ref.1) | copy-start | bytes 589828
  18.2 3.8 %copy-start.6 = (bf16[1024,128]{1,0:T(8,128)(2,1)S(1)}, bf16[1024,128]{1,0:T(8,128)(2,1)}, u32[]{:S(2)}) copy-start(bf16[1024,128]{1,0:T(8,128)(2,1)} %key_w_ref.1) | copy-start | bytes 786436
  18.2 3.8 %copy-start.7 = (bf16[1024,128]{1,0:T(8,128)(2,1)S(1)}, bf16[1024,128]{1,0:T(8,128)(2,1)}, u32[]{:S(2)}) copy-start(bf16[1024,128]{1,0:T(8,128)(2,1)} %value_w_ref.1) | copy-start | bytes 786436
  18.3 3.8 %copy-start.12 = (f32[1024]{0:T(1024)S(1)}, f32[1024]{0:T(1024)}, u32[]{:S(2)}) copy-start(f32[1024]{0:T(1024)} %param.20) | copy-start | bytes 12292
  22.1 11.9 %copy-start.4 = (bf16[1024,512]{1,0:T(8,128)(2,1)S(1)}, bf16[1024,512]{1,0:T(8,128)(2,1)}, u32[]{:S(2)}) copy-start(bf16[1024,512]{1,0:T(8,128)(2,1)} %weight_ref.4) | copy-start | bytes 3145732
  22.1 11.9 %copy-start.11 = (f32[8,513]{1,0:T(8,128)S(1)}, f32[8,513]{1,0:T(8,128)}, u32[]{:S(2)}) copy-start(f32[8,513]{1,0:T(8,128)} %table_ref.7) | copy-start | bytes 49252
  22.7 11.3 %collective-permute-start.2 = (bf16[192,256]{1,0:T(8,128)(2,1)S(1)}, bf16[192,256]{1,0:T(8,128)(2,1)S(1)}, u32[]{:S(2)}, u32[]{:S(2)}) collective-permute-start(bf16[192,256]{1,0:T(8,128)(2,1)S(1)} %get-tuple-element.16.kv_ref), channel_id=1, source_target_pairs={{0,2},{2,4},{4,6},{6,8},{8,10},{10,12},{12,14},{14,16},{16,18},{18... | collective-permute-start | bytes 294920 | tf_op jit(solution)/shard_map/ppermute | solution.py:43
  25.8 10.4 %collective-permute-start.3 = (bf16[64,256]{1,0:T(8,128)(2,1)S(1)}, bf16[64,256]{1,0:T(8,128)(2,1)S(1)}, u32[]{:S(2)}, u32[]{:S(2)}) collective-permute-start(bf16[64,256]{1,0:T(8,128)(2,1)S(1)} %get-tuple-element.18), channel_id=1, source_target_pairs={{0,4},{2,6},{4,8},{6,10},{8,12},{10,14},{12,16},{14,18},{16,20},{1... | collective-permute-start | bytes 98312 | tf_op jit(solution)/shard_map/ppermute | solution.py:43
  34.0 2.2 %copy-start.5 = (bf16[512,1024]{1,0:T(8,128)(2,1)S(1)}, bf16[512,1024]{1,0:T(8,128)(2,1)}, u32[]{:S(2)}) copy-start(bf16[512,1024]{1,0:T(8,128)(2,1)} %weight_ref.5) | copy-start | bytes 3145732

commit v2 on v1

v2 whole, which is shorter than its diff:
```python
import jax
import jax.numpy as jnp
from jax import lax
from jax.experimental import pallas as pl
from jax.experimental.pallas import tpu as pltpu
from jax.sharding import PartitionSpec as P


HEAD_SIZE = 64
SEG = 64
EPS = 1e-06
TILE = 128
NEG = -1e30
F32 = jnp.float32
BF16 = jnp.bfloat16

GROUP_HEADS = ((0, 2, 5, 7), (1, 3, 4, 6))


def whole():
    return pl.BlockSpec(memory_space=pltpu.VMEM)


def params(mib):
    return pltpu.CompilerParams(vmem_limit_bytes=mib * 1024 * 1024)


def shape(*dims, dtype=BF16):
    return jax.ShapeDtypeStruct(dims, dtype)


def cost(flops, transcendentals=0, nbytes=1 << 20):
    return pl.CostEstimate(flops=flops, bytes_accessed=nbytes, transcendentals=transcendentals)


def from_behind(block, distance):
    devices = range(lax.axis_size("sp"))
    route = [(i - distance, i) for i in devices if i - distance in devices]
    return lax.ppermute(block, "sp", route)


def pack_kernel(key_hbm, value_hbm, doc_hbm, query_hbm, near_ref, far_ref, query_ref, line, docs, sems):
    rows = key_hbm.shape[0]
    copies = [
        (doc_hbm, docs),
        (key_hbm, near_ref.at[0:rows, 0:TILE]),
        (value_hbm, near_ref.at[0:rows, TILE : 2 * TILE]),
        (key_hbm.at[rows - SEG : rows, :], far_ref.at[0:SEG, 0:TILE]),
        (value_hbm.at[rows - SEG : rows, :], far_ref.at[0:SEG, TILE : 2 * TILE]),
        (query_hbm, query_ref),
    ]
    copies = [pltpu.make_async_copy(a, b, sems.at[i]) for i, (a, b) in enumerate(copies)]
    for copy in copies:
        copy.start()
    line[...] = jnp.zeros_like(line)
    copies[0].wait()
    codes = (docs[...] + 1).astype(F32)
    line[:, 0:rows] = jnp.broadcast_to(codes, (8, rows))
    flat = line[...]
    lanes = lax.broadcasted_iota(jnp.int32, flat.shape, 1)
    near = pltpu.roll(flat, SEG, 1)
    far = jnp.where(lanes < SEG, pltpu.roll(flat, 2 * TILE - (rows - SEG), 1), 0.0)
    near_ref[rows : rows + 16, :] = jnp.concatenate([near, near], axis=0).astype(BF16)
    far_ref[SEG : SEG + 16, :] = jnp.concatenate([far, far], axis=0).astype(BF16)
    for copy in copies[1:]:
        copy.wait()


def fill_bias(table_ref, halo_bias, own_bias):
    table = table_ref[:, 0 : 4 * TILE]
    last = table_ref[:, 4 * TILE : 4 * TILE + 1]
    lanes = lax.broadcasted_iota(jnp.int32, table.shape, 1)
    moved = jnp.where(lanes < 448, pltpu.roll(table, 448, 1), jnp.broadcast_to(last, table.shape))
    mirror = 127 - lax.broadcasted_iota(jnp.int32, (8, TILE), 1)
    pieces = [
        jnp.take_along_axis(moved[:, TILE * t : TILE * (t + 1)], mirror, axis=1)
        for t in (3, 2, 1, 0)
    ]
    line = jnp.concatenate(pieces, axis=1)
    for group in range(2):
        for block, head in enumerate(GROUP_HEADS[group]):
            rows = jnp.broadcast_to(line[head : head + 1, :], (SEG, 4 * TILE))
            spot = slice(SEG * block, SEG * (block + 1))
            for odd in range(2):
                turned = pltpu.roll(rows, 449 if odd == 0 else 1, 1, stride=1, stride_axis=0)
                halo_bias[odd, group, spot, :] = turned[:, 0 : 2 * TILE]
                if odd == 0:
                    own_bias[group, spot, 0 : 2 * TILE] = turned[:, TILE : 3 * TILE]
                else:
                    own_bias[group, spot, 2 * TILE : 3 * TILE] = turned[:, 2 * TILE : 3 * TILE]


def swap_halves(part):
    tiles = [
        pltpu.roll(part[:, TILE * t : TILE * (t + 1)].astype(F32), SEG, 1).astype(BF16) for t in range(2)
    ]
    return jnp.concatenate(tiles, axis=1)


def query_code(own_codes, segment):
    lanes = lax.broadcasted_iota(jnp.int32, (SEG, 2 * TILE), 1)
    rows = lax.broadcasted_iota(jnp.int32, (SEG, 2 * TILE), 0)
    spread = jnp.broadcast_to(own_codes[0:1, :], (SEG, 2 * TILE))
    return jnp.sum(jnp.where(lanes == rows + SEG * segment, spread, 0.0), axis=1, keepdims=True)


def code_mask(codes, mine, low, high):
    lanes = lax.broadcasted_iota(jnp.int32, (SEG, codes.shape[1]), 1)
    agree = (jnp.broadcast_to(codes, (SEG, codes.shape[1])) == mine) & (lanes >= low) & (lanes < high)
    return jnp.where(agree, 0.0, NEG)


def half_scales():
    lanes = lax.broadcasted_iota(jnp.int32, (1, TILE), 1)
    scale = HEAD_SIZE ** (-0.5)
    low = jnp.where(lanes < HEAD_SIZE, scale, 0.0).astype(BF16)
    high = jnp.where(lanes < HEAD_SIZE, 0.0, scale).astype(BF16)
    return low, high


def stacked_queries(query, group):
    low, high = half_scales()
    return jnp.concatenate(
        [
            query[:, TILE * t : TILE * (t + 1)] * (low if (t < 2) == (group == 0) else high)
            for t in range(4)
        ],
        axis=0,
    )


def own_part(query, own, codes, own_bias, band, swapped, partial_ref, top_ref, total_ref):
    rows = own.shape[0]
    band[0:rows, :] = own
    band[rows:, :] = jnp.zeros((2 * TILE - rows, 2 * TILE), BF16)
    swapped[0:rows, :] = swap_halves(own)
    swapped[rows:, :] = jnp.zeros((2 * TILE - rows, 2 * TILE), BF16)
    for segment in range(3):
        width = 2 * TILE if segment == 2 else TILE
        first = (TILE, 2 * TILE, 0)[segment]
        mask = code_mask(codes[0:1, 0:width], query_code(codes, segment), 0, SEG * (segment + 1))
        for group in range(2):
            source = band if group == 0 else swapped
            left = stacked_queries(query[SEG * segment : SEG * (segment + 1), :], group)
            scores = lax.dot_general(
                left, source[0:width, 0:TILE], (((1,), (1,)), ((), ())), preferred_element_type=F32
            )
            base = 4 * SEG * (2 * segment + group)
            weights = []
            for block in range(4):
                spot = slice(SEG * block, SEG * (block + 1))
                s = scores[spot] + own_bias[group, spot, first : first + width] + mask
                top = jnp.max(s, axis=1, keepdims=True)
                e = jnp.exp(s - top)
                place = slice(base + SEG * block, base + SEG * (block + 1))
                top_ref[place, :] = jnp.broadcast_to(top, (SEG, TILE))
                total_ref[place, :] = jnp.broadcast_to(jnp.sum(e, axis=1, keepdims=True), (SEG, TILE))
                weights.append(e.astype(BF16))
            partial_ref[base : base + 4 * SEG, :] = jnp.dot(
                jnp.concatenate(weights, axis=0), source[0:width, TILE : 2 * TILE], preferred_element_type=F32
            )


def near_part(query_ref, near, codes, own_codes, halo_bias, partial_ref, top_ref, total_ref, band, swapped, mixed, heads_out):
    for target, rows in ((band, near), (swapped, swap_halves(near))):
        target[0:SEG, :] = jnp.zeros((SEG, 2 * TILE), BF16)
        target[SEG:, :] = rows
    lanes = lax.broadcasted_iota(jnp.int32, (1, TILE), 1)
    head_partial, head_top, head_total = heads_out
    for segment in range(3):
        start = TILE if segment == 2 else 0
        width = 2 * TILE - start
        mask = code_mask(codes[0:1, start:], query_code(own_codes, segment), 0 if segment == 2 else SEG, width)
        results = []
        for group in range(2):
            source = band if group == 0 else swapped
            left = stacked_queries(query_ref[SEG * segment : SEG * (segment + 1), :], group)
            scores = lax.dot_general(
                left, source[start:, 0:TILE], (((1,), (1,)), ((), ())), preferred_element_type=F32
            )
            base = 4 * SEG * (2 * segment + group)
            weights = []
            olds = []
            shares = []
            for block in range(4):
                spot = slice(SEG * block, SEG * (block + 1))
                place = slice(base + SEG * block, base + SEG * (block + 1))
                s = scores[spot] + halo_bias[segment % 2, group, spot, 0:width] + mask
                old_top = top_ref[place, :]
                top = jnp.maximum(jnp.max(s, axis=1, keepdims=True), old_top)
                e = jnp.exp(s - jnp.concatenate([top] * (width // TILE), axis=1))
                old = jnp.exp(old_top - top)
                total = total_ref[place, :] * old + jnp.sum(e, axis=1, keepdims=True)
                weights.append(e.astype(BF16))
                if segment == 0:
                    head_top[place, :] = top
                    head_total[place, :] = total
                    olds.append(old)
                else:
                    share = 1.0 / total
                    shares.append(share)
                    olds.append(old * share)
            blended = jnp.dot(
                jnp.concatenate(weights, axis=0), source[start:, TILE : 2 * TILE], preferred_element_type=F32
            )
            for block in range(4):
                place = slice(base + SEG * block, base + SEG * (block + 1))
                fresh = blended[SEG * block : SEG * (block + 1)]
                before = partial_ref[place, :] * olds[block]
                if segment == 0:
                    head_partial[place, :] = fresh + before
                else:
                    results.append(fresh * shares[block] + before)
        if segment:
            store_heads(mixed, SEG * (segment - 1), results, lanes)


def store_heads(mixed, row, results, lanes):
    for tile in range(4):
        even, odd = (0, 4) if tile < 2 else (4, 0)
        mixed[row : row + SEG, TILE * tile : TILE * (tile + 1)] = jnp.where(
            lanes < HEAD_SIZE, results[even + tile], results[odd + tile]
        ).astype(BF16)


def far_part(query, far, codes, own_codes, halo_bias, partial_ref, top_ref, total_ref, mixed):
    lanes = lax.broadcasted_iota(jnp.int32, (1, TILE), 1)
    mask = code_mask(codes[0:1, 0:SEG], query_code(own_codes, 0), 0, SEG)
    sides = (far, swap_halves(far))
    results = []
    for group in range(2):
        left = stacked_queries(query, group)
        scores = lax.dot_general(
            left, sides[group][:, 0:TILE], (((1,), (1,)), ((), ())), preferred_element_type=F32
        )
        base = 4 * SEG * group
        weights = []
        olds = []
        shares = []
        for block in range(4):
            spot = slice(SEG * block, SEG * (block + 1))
            place = slice(base + SEG * block, base + SEG * (block + 1))
            s = scores[spot] + halo_bias[0, group, spot, 0:SEG] + mask
            old_top = top_ref[place, :]
            top = jnp.maximum(jnp.max(s, axis=1, keepdims=True), old_top)
            e = jnp.exp(s - top[:, 0:SEG])
            old = jnp.exp(old_top - top)
            share = 1.0 / (total_ref[place, :] * old + jnp.sum(e, axis=1, keepdims=True))
            shares.append(share)
            olds.append(old * share)
            weights.append(e.astype(BF16))
        blended = jnp.dot(
            jnp.concatenate(weights, axis=0), sides[group][:, TILE : 2 * TILE], preferred_element_type=F32
        )
        for block in range(4):
            place = slice(base + SEG * block, base + SEG * (block + 1))
            results.append(
                blended[SEG * block : SEG * (block + 1)] * shares[block] + partial_ref[place, :] * olds[block]
            )
    store_heads(mixed, 0, results, lanes)


def codes_of(packed_ref, row, turn):
    codes = packed_ref[row : row + 16, :].astype(F32)[0:8]
    return pltpu.roll(codes, turn, 1) if turn else codes


def before_one_kernel(query_ref, packed_ref, table_ref, halo_bias, partial_ref, top_ref, total_ref, own_bias, band, swapped):
    rows = query_ref.shape[0]
    fill_bias(table_ref, halo_bias, own_bias)
    own_codes = codes_of(packed_ref, rows, 2 * TILE - SEG)
    own_part(
        query_ref[...], packed_ref[0:rows, :], own_codes, own_bias, band, swapped, partial_ref, top_ref, total_ref
    )


def before_two_kernel(
    normed_ref, weight_ref, kv_ref, packed_ref, table_ref, query_ref, halo_bias, partial_ref, top_ref, total_ref,
    own_bias, band, swapped,
):
    rows = kv_ref.shape[0]
    query = jnp.dot(normed_ref[...], weight_ref[...], preferred_element_type=F32).astype(BF16)
    query_ref[...] = query
    fill_bias(table_ref, halo_bias, own_bias)
    own_codes = codes_of(packed_ref, rows, 2 * TILE - SEG)
    own_part(query, kv_ref[...], own_codes, own_bias, band, swapped, partial_ref, top_ref, total_ref)


def with_residual(partial, residual):
    mine = (lax.axis_index("tp") == 0).astype(F32)
    wide = residual.astype(F32)
    half = wide.shape[1]
    return (partial[:, 0:half] + wide * mine).astype(BF16), (partial[:, half:] + wide * (1.0 - mine)).astype(BF16)


def near_one_kernel(
    query_ref, near_ref, packed_ref, halo_bias, partial_ref, top_ref, total_ref, weight_ref, residual_ref,
    out_ref, head_partial, head_top, head_total, band, swapped, mixed,
):
    rows = query_ref.shape[0]
    near_part(
        query_ref, near_ref[0:rows, :], codes_of(near_ref, rows, 0), codes_of(packed_ref, rows, 2 * TILE - SEG),
        halo_bias, partial_ref, top_ref, total_ref, band, swapped, mixed, (head_partial, head_top, head_total),
    )
    partial = jnp.dot(mixed[...], weight_ref[...], preferred_element_type=F32)
    half = residual_ref.shape[1]
    out_ref[:, 0:half], out_ref[:, half:] = with_residual(partial, residual_ref[SEG:, :])


def near_two_kernel(
    query_ref, near_ref, near_codes_ref, packed_ref, halo_bias, partial_ref, top_ref, total_ref, weight_ref,
    out_ref, head_partial, head_top, head_total, band, swapped, mixed,
):
    rows = query_ref.shape[0]
    near_part(
        query_ref, near_ref[...], codes_of(near_codes_ref, rows, 0), codes_of(packed_ref, rows, 2 * TILE - SEG),
        halo_bias, partial_ref, top_ref, total_ref, band, swapped, mixed, (head_partial, head_top, head_total),
    )
    out_ref[...] = jnp.dot(mixed[...], weight_ref[...], preferred_element_type=F32).astype(BF16)


def far_one_kernel(
    query_ref, far_ref, packed_ref, halo_bias, rest_ref, partial_ref, top_ref, total_ref, weight_ref, residual_ref,
    out_ref, mixed,
):
    rows = query_ref.shape[0]
    out_ref[SEG:, :] = rest_ref[...]
    far_part(
        query_ref[0:SEG, :], far_ref[0:SEG, :], codes_of(far_ref, SEG, 0), codes_of(packed_ref, rows, 2 * TILE - SEG),
        halo_bias, partial_ref, top_ref, total_ref, mixed,
    )
    partial = jnp.dot(mixed[...], weight_ref[...], preferred_element_type=F32)
    half = residual_ref.shape[1]
    out_ref[0:SEG, 0:half], out_ref[0:SEG, half:] = with_residual(partial, residual_ref[0:SEG, :])


def far_two_kernel(
    query_ref, far_ref, far_codes_ref, packed_ref, halo_bias, rest_ref, partial_ref, top_ref, total_ref, weight_ref,
    out_ref, mixed,
):
    rows = query_ref.shape[0]
    out_ref[SEG:, :] = rest_ref[...]
    far_part(
        query_ref[0:SEG, :], far_ref[...], codes_of(far_codes_ref, SEG, 0), codes_of(packed_ref, rows, 2 * TILE - SEG),
        halo_bias, partial_ref, top_ref, total_ref, mixed,
    )
    out_ref[0:SEG, :] = jnp.dot(mixed[...], weight_ref[...], preferred_element_type=F32).astype(BF16)


def norm_kernel(both_ref, gain_ref, key_w_ref, value_w_ref, kv_ref, tail_ref, normed_ref, share_ref):
    layer = (both_ref[0].astype(F32) + both_ref[1].astype(F32)).astype(BF16)
    wide = layer.astype(F32)
    rows, channels = wide.shape
    scale = lax.rsqrt(jnp.mean(wide * wide, axis=1, keepdims=True) + EPS)
    normed = (wide * scale * gain_ref[...]).astype(BF16)
    keys = jnp.dot(normed, key_w_ref[...], preferred_element_type=F32).astype(BF16)
    values = jnp.dot(normed, value_w_ref[...], preferred_element_type=F32).astype(BF16)
    kv_ref[:, 0:TILE] = keys
    kv_ref[:, TILE : 2 * TILE] = values
    tail_ref[:, 0:TILE] = keys[rows - SEG :]
    tail_ref[:, TILE : 2 * TILE] = values[rows - SEG :]
    normed_ref[...] = normed
    half = channels // 2
    share_ref[...] = jnp.where(lax.axis_index("tp") == 0, wide[:, 0:half], wide[:, half:]).astype(BF16)


def last_kernel(both_ref, share_ref, out_ref):
    half = share_ref.shape[1]
    mine = pl.ds(pl.multiple_of(lax.axis_index("tp") * half, half), half)
    out_ref[...] = (
        share_ref[...].astype(F32) + both_ref[0, :, mine].astype(F32) + both_ref[1, :, mine].astype(F32)
    ).astype(BF16)


def call(kernel, outs, scratch, args, flops, mib=16, spaces=None):
    return pl.pallas_call(
        kernel,
        out_shape=outs,
        in_specs=[whole()] * len(args) if spaces is None else [pl.BlockSpec(memory_space=s) for s in spaces],
        out_specs=jax.tree.map(lambda _: whole(), outs),
        scratch_shapes=scratch,
        compiler_params=params(mib),
        cost_estimate=cost(flops),
    )(*args)


def body(
    residual,
    query_first,
    key_first,
    value_first,
    documents,
    bias_first,
    out_first,
    norm_gain,
    query_w,
    key_w,
    value_w,
    bias_second,
    out_second,
):
    rows, half = residual.shape
    width = query_first.shape[1]
    channels = out_first.shape[1]
    docs = documents.reshape(1, rows)
    gain = norm_gain.reshape(1, channels)
    bands = [pltpu.VMEM((2 * TILE, 2 * TILE), BF16), pltpu.VMEM((2 * TILE, 2 * TILE), BF16)]
    before_scratch = [pltpu.VMEM((2, 4 * SEG, 3 * TILE), F32), *bands]
    near_scratch = [*bands, pltpu.VMEM((rows - SEG, width), BF16)]
    far_scratch = [pltpu.VMEM((SEG, width), BF16)]
    stats = shape(24 * SEG, TILE, dtype=F32)
    head_stats = shape(8 * SEG, TILE, dtype=F32)
    near_shapes = (shape(rows - SEG, channels), head_stats, head_stats, head_stats)
    own_shapes = (shape(2, 2, 4 * SEG, 2 * TILE, dtype=F32), stats, stats, stats)
    packed, far_send, query_one = call(
        pack_kernel,
        (shape(rows + 16, 2 * TILE), shape(SEG + 16, 2 * TILE), shape(rows, width)),
        [pltpu.VMEM((8, 2 * TILE), F32), pltpu.VMEM((1, rows), jnp.int32), pltpu.SemaphoreType.DMA((6,))],
        tuple(pltpu.with_memory_space_constraint(x, pltpu.HBM) for x in (key_first, value_first, docs, query_first)),
        1 << 20,
        spaces=[pltpu.HBM] * 4,
    )
    near_one = from_behind(packed, 1)
    far_one = from_behind(far_send, 2)
    own_one = call(
        before_one_kernel, own_shapes, before_scratch, (query_one, packed, bias_first), 1 << 31
    )
    rest_one = call(
        near_one_kernel,
        near_shapes,
        near_scratch,
        (query_one, near_one, packed, *own_one, out_first, residual),
        1 << 31,
    )
    sent_one = call(
        far_one_kernel,
        shape(rows, channels),
        far_scratch,
        (query_one, far_one, packed, own_one[0], *rest_one, out_first, residual),
        1 << 31,
    )
    both_one = lax.all_gather(sent_one, "tp", axis=0)
    kv_two, tail_two, normed, share = call(
        norm_kernel,
        (shape(rows, 2 * TILE), shape(SEG, 2 * TILE), shape(rows, channels), shape(rows, half)),
        [],
        (both_one, gain, key_w, value_w),
        1 << 30,
    )
    near_two = from_behind(kv_two, 1)
    far_two = from_behind(tail_two, 2)
    query_two, *own_two = call(
        before_two_kernel,
        (shape(rows, width), *own_shapes),
        before_scratch,
        (normed, query_w, kv_two, packed, bias_second),
        1 << 31,
    )
    rest_two = call(
        near_two_kernel,
        near_shapes,
        near_scratch,
        (query_two, near_two, near_one, packed, *own_two, out_second),
        1 << 31,
    )
    sent_two = call(
        far_two_kernel,
        shape(rows, channels),
        far_scratch,
        (query_two, far_two, far_one, packed, own_two[0], *rest_two, out_second),
        1 << 31,
    )
    both_two = lax.all_gather(sent_two, "tp", axis=0)
    return call(last_kernel, shape(rows, half), [], (both_two, share), 1 << 20)


def solution(mesh):
    placed = (
        P("sp", "tp"),
        P("sp", "tp"),
        P("sp", "tp"),
        P("sp", "tp"),
        P("sp"),
        P("tp", None),
        P("tp", None),
        P(),
        P(None, "tp"),
        P(None, "tp"),
        P(None, "tp"),
        P("tp", None),
        P("tp", None),
    )
    return jax.shard_map(body, mesh=mesh, in_specs=placed, out_specs=P("sp", "tp"), check_vma=False)
```

time: 42.9 us -> 43.9 us (1.023)
  the two profiles are of different devices: /device:TPU:129 before, /device:TPU:257 now
where the time goes in v2:
time: 43.9 us; the launch traced here: 43.6 us
  waiting for transfers between devices  14.5 us (33%)
  Pallas kernels  10.7 us (24%)
  starting transfers between devices  10.7 us (24%)
  blocking collectives  7.46 us (17%)
    ppermute x4, waiting for transfers between devices, from_behind(): return lax.ppermute(block, 'sp', route)  14.5 us
    ppermute x4, starting transfers between devices, from_behind(): return lax.ppermute(block, 'sp', route)  10.7 us
    pallas_call x9, Pallas kernels, call(): pl.pallas_call(kernel, out_shape=outs, in_specs=[whole()] * len(args) if...  10.7 us
    all_gather x1, blocking collectives, body(): both_one = lax.all_gather(sent_one, 'tp', axis=0)  4.23 us
    all_gather x1, blocking collectives, body(): both_two = lax.all_gather(sent_two, 'tp', axis=0)  3.24 us
  transfers between devices with their start and end apart: 4, of which 2 were waited for; matrix products, arithmetic and copies ran while one was open for 0% of the time, Pallas kernels for 15%

profile of v2, /device:TPU:257, one launch (start us, length us, event | category | flops | bytes accessed | tf_op | source)
XLA Modules:
  0.0 43.6 jit_solution(8535405900821731086)
XLA Ops:
  0.0 1.1 %shard_map.127 = (bf16[208,256]{1,0:T(8,128)(2,1)S(1)}, bf16[80,256]{1,0:T(8,128)(2,1)S(1)}, bf16[192,512]{1,0:T(8,128)(2,1)S(1)}) custom-call(bf16[192,128]{1,0:T(8,128)(2,1)} %key_hbm.1, bf16[192,128]{1,0:T(8,128)(2,1)} %value_hbm.1, s32[1,192]{1,0:T(1,128)} %bitcast.7, bf16[192,512]{1,0:T(8,128)(2,1)} %query_hbm.1), custom_call_target="tpu_custom_call" | custom-call | flops 1048576 | bytes 1048576 | tf_op jit(solution)/shard_map/pallas_call | solution.py:376
  1.1 4.7 %collective-permute-start = (bf16[80,256]{1,0:T(8,128)(2,1)S(1)}, bf16[80,256]{1,0:T(8,128)(2,1)S(1)}, u32[]{:S(2)}, u32[]{:S(2)}) collective-permute-start(bf16[80,256]{1,0:T(8,128)(2,1)S(1)} %get-tuple-element.30), channel_id=1, source_target_pairs={{0,4},{2,6},{4,8},{6,10},{8,12},{10,14},{12,16},{14,18},{16,20},{1... | collective-permute-start | bytes 122888 | tf_op jit(solution)/shard_map/ppermute | solution.py:39
  5.8 2.2 %collective-permute-start.1 = (bf16[208,256]{1,0:T(8,128)(2,1)S(1)}, bf16[208,256]{1,0:T(8,128)(2,1)S(1)}, u32[]{:S(2)}, u32[]{:S(2)}) collective-permute-start(bf16[208,256]{1,0:T(8,128)(2,1)S(1)} %get-tuple-element.31.packed_ref), channel_id=1, source_target_pairs={{0,2},{2,4},{4,6},{6,8},{8,10},{10,12},{12,14},{14,16},{16,18},{18... | collective-permute-start | bytes 319496 | tf_op jit(solution)/shard_map/ppermute | solution.py:39
  8.0 0.0 copy-done.6
  8.0 0.0 copy-start
  8.0 0.0 copy-start.5
  8.0 1.9 %shard_map.128 = (f32[2,2,256,256]{3,2,1,0:T(8,128)S(1)}, f32[1536,128]{1,0:T(8,128)S(1)}, f32[1536,128]{1,0:T(8,128)S(1)}, f32[1536,128]{1,0:T(8,128)S(1)}) custom-call(bf16[192,512]{1,0:T(8,128)(2,1)S(1)} %get-tuple-element.29.query_ref, bf16[208,256]{1,0:T(8,128)(2,1)S(1)} %get-tuple-element.31.packed_ref, f32[8,513]{1,0:T(8,128)S(1)} %copy-done.6), custom_call_target="tpu_custom_call" | custom-call | flops 2147483648 | bytes 1048576 | tf_op jit(solution)/shard_map/pallas_call | solution.py:376
  9.9 6.7 %collective-permute-done.1.near_ref.near_codes_ref = bf16[208,256]{1,0:T(8,128)(2,1)S(1)} collective-permute-done((bf16[208,256]{1,0:T(8,128)(2,1)S(1)}, bf16[208,256]{1,0:T(8,128)(2,1)S(1)}, u32[]{:S(2)}, u32[]{:S(2)}) %collective-permute-start.1) | collective-permute-done | bytes 106528 | tf_op jit(solution)/shard_map/ppermute | solution.py:39
  16.6 0.0 copy-done
  16.6 0.0 copy-done.5
  16.7 1.5 %shard_map.129 = (bf16[128,1024]{1,0:T(8,128)(2,1)S(1)}, f32[512,128]{1,0:T(8,128)S(1)}, f32[512,128]{1,0:T(8,128)S(1)}, f32[512,128]{1,0:T(8,128)S(1)}) custom-call(bf16[192,512]{1,0:T(8,128)(2,1)S(1)} %get-tuple-element.29.query_ref, bf16[208,256]{1,0:T(8,128)(2,1)S(1)} %collective-permute-done.1.near_ref.near_codes_ref, ...), custom_call_target="tpu_custom_call" | custom-call | flops 2147483648 | bytes 1048576 | tf_op jit(solution)/shard_map/pallas_call | solution.py:376
  18.1 0.0 collective-permute-done.far_ref.far_codes_ref
  18.1 1.0 %shard_map.130 = bf16[192,1024]{1,0:T(8,128)(2,1)S(1)} custom-call(bf16[192,512]{1,0:T(8,128)(2,1)S(1)} %get-tuple-element.29.query_ref, bf16[80,256]{1,0:T(8,128)(2,1)S(1)} %collective-permute-done.far_ref.far_codes_ref, bf16[208,256]{1,0:T(8,128)(2,1)S(1)} %get-tuple-element.31.packed_ref, f32[2,2,256,256]{3,2,1,0:T(8,128)S(1)} %get-tuple-element.32.halo_bias, ...), custom_call_target="tpu_custom_call" | custom-call | flops 2147483648 | bytes 1048576 | tf_op jit(solution)/shard_map/pallas_call | solution.py:376
  19.1 0.0 copy-start.3
  19.1 0.0 copy-start.4
  19.1 0.0 copy-start.8
  19.1 4.2 %all-gather = bf16[384,1024]{1,0:T(8,128)(2,1)S(1)} all-gather(bf16[192,1024]{1,0:T(8,128)(2,1)S(1)} %shard_map.130), channel_id=2, replica_groups=mesh['sp'=256,'tp'=2] {'tp'}, dimensions={0}, use_global_device_ids=true | all-gather | bytes 1179648 | tf_op jit(solution)/shard_map/all_gather | solution.py:442
  23.4 0.0 copy-done.3
  23.4 0.0 copy-start.7
  23.4 0.6 %shard_map.131 = (bf16[192,256]{1,0:T(8,128)(2,1)S(1)}, bf16[64,256]{1,0:T(8,128)(2,1)S(1)}, bf16[192,1024]{1,0:T(8,128)(2,1)S(1)}, bf16[192,512]{1,0:T(8,128)(2,1)S(1)}) custom-call(bf16[2,192,1024]{2,1,0:T(8,128)(2,1)S(1)} %bitcast.5, f32[1,1024]{1,0:T(1,128)S(1)} %bitcast.6, bf16[1024,128]{1,0:T(8,128)(2,1)S(1)} %copy-done.3, bf16[1024,128]{1,0:T(8,128)(2,1)S(1)} %copy-done.4), custom_call_target="tpu_custom_call" | custom-call | flops 1073741824 | bytes 1048576 | tf_op jit(solution)/shard_map/pallas_call | solution.py:376
  24.0 1.9 %collective-permute-start.2 = (bf16[64,256]{1,0:T(8,128)(2,1)S(1)}, bf16[64,256]{1,0:T(8,128)(2,1)S(1)}, u32[]{:S(2)}, u32[]{:S(2)}) collective-permute-start(bf16[64,256]{1,0:T(8,128)(2,1)S(1)} %get-tuple-element.43), channel_id=1, source_target_pairs={{0,4},{2,6},{4,8},{6,10},{8,12},{10,14},{12,16},{14,18},{16,20},{1... | collective-permute-start | bytes 98312 | tf_op jit(solution)/shard_map/ppermute | solution.py:39
  25.9 1.9 %collective-permute-start.3 = (bf16[192,256]{1,0:T(8,128)(2,1)S(1)}, bf16[192,256]{1,0:T(8,128)(2,1)S(1)}, u32[]{:S(2)}, u32[]{:S(2)}) collective-permute-start(bf16[192,256]{1,0:T(8,128)(2,1)S(1)} %get-tuple-element.41.kv_ref), channel_id=1, source_target_pairs={{0,2},{2,4},{4,6},{6,8},{8,10},{10,12},{12,14},{14,16},{16,18},{18... | collective-permute-start | bytes 294920 | tf_op jit(solution)/shard_map/ppermute | solution.py:39
  27.8 0.0 copy-done.1
  27.8 0.0 copy-done.7
  27.9 0.0 copy-start.2
  27.9 1.5 %shard_map.132 = (bf16[192,512]{1,0:T(8,128)(2,1)S(1)}, f32[2,2,256,256]{3,2,1,0:T(8,128)S(1)}, f32[1536,128]{1,0:T(8,128)S(1)}, f32[1536,128]{1,0:T(8,128)S(1)}, f32[1536,128]{1,0:T(8,128)S(1)}) custom-call(bf16[192,1024]{1,0:T(8,128)(2,1)S(1)} %get-tuple-element.40.normed_ref, bf16[1024,512]{1,0:T(8,128)(2,1)S(1)} %copy-done.1, ...), custom_call_target="tpu_custom_call" | custom-call | flops 2147483648 | bytes 1048576 | tf_op jit(solution)/shard_map/pallas_call | solution.py:376
  29.4 7.8 %collective-permute-done.3.near_ref = bf16[192,256]{1,0:T(8,128)(2,1)S(1)} collective-permute-done((bf16[192,256]{1,0:T(8,128)(2,1)S(1)}, bf16[192,256]{1,0:T(8,128)(2,1)S(1)}, u32[]{:S(2)}, u32[]{:S(2)}) %collective-permute-start.3) | collective-permute-done | bytes 98336 | tf_op jit(solution)/shard_map/ppermute | solution.py:39
  37.2 1.5 %shard_map.133 = (bf16[128,1024]{1,0:T(8,128)(2,1)S(1)}, f32[512,128]{1,0:T(8,128)S(1)}, f32[512,128]{1,0:T(8,128)S(1)}, f32[512,128]{1,0:T(8,128)S(1)}) custom-call(bf16[192,512]{1,0:T(8,128)(2,1)S(1)} %get-tuple-element.42.query_ref, bf16[192,256]{1,0:T(8,128)(2,1)S(1)} %collective-permute-done.3.near_ref, ...), custom_call_target="tpu_custom_call" | custom-call | flops 2147483648 | bytes 1048576 | tf_op jit(solution)/shard_map/pallas_call | solution.py:376
  38.7 0.0 collective-permute-done.2.far_ref
  38.7 0.9 %shard_map.134 = bf16[192,1024]{1,0:T(8,128)(2,1)S(1)} custom-call(bf16[192,512]{1,0:T(8,128)(2,1)S(1)} %get-tuple-element.42.query_ref, bf16[64,256]{1,0:T(8,128)(2,1)S(1)} %collective-permute-done.2.far_ref, bf16[80,256]{1,0:T(8,128)(2,1)S(1)} %collective-permute-done.far_ref.far_codes_ref, bf16[208,256]{1,0:T(8,128)(2,1)S(1)} %get-tuple-element.31.packed_ref, ...), custom_call_target="tpu_custom_call" | custom-call | flops 2147483648 | bytes 1048576 | tf_op jit(solution)/shard_map/pallas_call | solution.py:376
  39.7 3.2 %all-gather.1 = bf16[384,1024]{1,0:T(8,128)(2,1)S(1)} all-gather(bf16[192,1024]{1,0:T(8,128)(2,1)S(1)} %shard_map.134), channel_id=3, replica_groups=mesh['sp'=256,'tp'=2] {'tp'}, dimensions={0}, use_global_device_ids=true | all-gather | bytes 1179648 | tf_op jit(solution)/shard_map/all_gather | solution.py:473
  42.9 0.8 %shard_map.135 = bf16[192,512]{1,0:T(8,128)(2,1)} custom-call(bf16[2,192,1024]{2,1,0:T(8,128)(2,1)S(1)} %bitcast.4, bf16[192,512]{1,0:T(8,128)(2,1)S(1)} %get-tuple-element.52.share_ref), custom_call_target="tpu_custom_call" | custom-call | flops 1048576 | bytes 1048576 | tf_op jit(solution)/shard_map/pallas_call | solution.py:376
  (5 shorter events, 0.0 us)
Async XLA Ops:
  0.0 8.0 %copy-start.6 = (f32[8,513]{1,0:T(8,128)S(1)}, f32[8,513]{1,0:T(8,128)}, u32[]{:S(2)}) copy-start(f32[8,513]{1,0:T(8,128)} %table_ref.2) | copy-start | bytes 49252
  1.1 17.0 %collective-permute-start = (bf16[80,256]{1,0:T(8,128)(2,1)S(1)}, bf16[80,256]{1,0:T(8,128)(2,1)S(1)}, u32[]{:S(2)}, u32[]{:S(2)}) collective-permute-start(bf16[80,256]{1,0:T(8,128)(2,1)S(1)} %get-tuple-element.30), channel_id=1, source_target_pairs={{0,4},{2,6},{4,8},{6,10},{8,12},{10,14},{12,16},{14,18},{16,20},{1... | collective-permute-start | bytes 122888 | tf_op jit(solution)/shard_map/ppermute | solution.py:39
  5.8 10.9 %collective-permute-start.1 = (bf16[208,256]{1,0:T(8,128)(2,1)S(1)}, bf16[208,256]{1,0:T(8,128)(2,1)S(1)}, u32[]{:S(2)}, u32[]{:S(2)}) collective-permute-start(bf16[208,256]{1,0:T(8,128)(2,1)S(1)} %get-tuple-element.31.packed_ref), channel_id=1, source_target_pairs={{0,2},{2,4},{4,6},{6,8},{8,10},{10,12},{12,14},{14,16},{16,18},{18... | collective-permute-start | bytes 319496 | tf_op jit(solution)/shard_map/ppermute | solution.py:39
  8.0 8.6 %copy-start = (bf16[512,1024]{1,0:T(8,128)(2,1)S(1)}, bf16[512,1024]{1,0:T(8,128)(2,1)}, u32[]{:S(2)}) copy-start(bf16[512,1024]{1,0:T(8,128)(2,1)} %weight_ref.6) | copy-start | bytes 3145732
  8.0 8.6 %copy-start.5 = (bf16[192,512]{1,0:T(8,128)(2,1)S(1)}, bf16[192,512]{1,0:T(8,128)(2,1)}, u32[]{:S(2)}) copy-start(bf16[192,512]{1,0:T(8,128)(2,1)} %residual_ref.3) | copy-start | bytes 589828
  19.1 4.3 %copy-start.3 = (bf16[1024,128]{1,0:T(8,128)(2,1)S(1)}, bf16[1024,128]{1,0:T(8,128)(2,1)}, u32[]{:S(2)}) copy-start(bf16[1024,128]{1,0:T(8,128)(2,1)} %key_w_ref.1) | copy-start | bytes 786436
  19.1 4.3 %copy-start.4 = (bf16[1024,128]{1,0:T(8,128)(2,1)S(1)}, bf16[1024,128]{1,0:T(8,128)(2,1)}, u32[]{:S(2)}) copy-start(bf16[1024,128]{1,0:T(8,128)(2,1)} %value_w_ref.1) | copy-start | bytes 786436
  19.1 4.2 %copy-start.8 = (f32[1024]{0:T(1024)S(1)}, f32[1024]{0:T(1024)}, u32[]{:S(2)}) copy-start(f32[1024]{0:T(1024)} %param.20) | copy-start | bytes 12292
  23.4 4.5 %copy-start.1 = (bf16[1024,512]{1,0:T(8,128)(2,1)S(1)}, bf16[1024,512]{1,0:T(8,128)(2,1)}, u32[]{:S(2)}) copy-start(bf16[1024,512]{1,0:T(8,128)(2,1)} %weight_ref.7) | copy-start | bytes 3145732
  23.4 4.5 %copy-start.7 = (f32[8,513]{1,0:T(8,128)S(1)}, f32[8,513]{1,0:T(8,128)}, u32[]{:S(2)}) copy-start(f32[8,513]{1,0:T(8,128)} %table_ref.3) | copy-start | bytes 49252
  24.0 14.7 %collective-permute-start.2 = (bf16[64,256]{1,0:T(8,128)(2,1)S(1)}, bf16[64,256]{1,0:T(8,128)(2,1)S(1)}, u32[]{:S(2)}, u32[]{:S(2)}) collective-permute-start(bf16[64,256]{1,0:T(8,128)(2,1)S(1)} %get-tuple-element.43), channel_id=1, source_target_pairs={{0,4},{2,6},{4,8},{6,10},{8,12},{10,14},{12,16},{14,18},{16,20},{1... | collective-permute-start | bytes 98312 | tf_op jit(solution)/shard_map/ppermute | solution.py:39
  25.9 11.3 %collective-permute-start.3 = (bf16[192,256]{1,0:T(8,128)(2,1)S(1)}, bf16[192,256]{1,0:T(8,128)(2,1)S(1)}, u32[]{:S(2)}, u32[]{:S(2)}) collective-permute-start(bf16[192,256]{1,0:T(8,128)(2,1)S(1)} %get-tuple-element.41.kv_ref), channel_id=1, source_target_pairs={{0,2},{2,4},{4,6},{6,8},{8,10},{10,12},{12,14},{14,16},{16,18},{18... | collective-permute-start | bytes 294920 | tf_op jit(solution)/shard_map/ppermute | solution.py:39
  27.9 9.3 %copy-start.2 = (bf16[512,1024]{1,0:T(8,128)(2,1)S(1)}, bf16[512,1024]{1,0:T(8,128)(2,1)}, u32[]{:S(2)}) copy-start(bf16[512,1024]{1,0:T(8,128)(2,1)} %weight_ref.9) | copy-start | bytes 3145732

commit v3 on v2

--- a/solution.py
+++ b/solution.py
@@ -39,15 +39,17 @@
     return lax.ppermute(block, "sp", route)
 
 
-def pack_kernel(key_hbm, value_hbm, doc_hbm, query_hbm, near_ref, far_ref, query_ref, line, docs, sems):
+def pack_kernel(key_hbm, value_hbm, doc_hbm, near_ref, far_ref, line, docs, sems):
     rows = key_hbm.shape[0]
     copies = [
         (doc_hbm, docs),
-        (key_hbm, near_ref.at[0:rows, 0:TILE]),
-        (value_hbm, near_ref.at[0:rows, TILE : 2 * TILE]),
+        *(
+            (source.at[first : first + rows // 2, :], near_ref.at[first : first + rows // 2, lane : lane + TILE])
+            for first in (0, rows // 2)
+            for source, lane in ((key_hbm, 0), (value_hbm, TILE))
+        ),
         (key_hbm.at[rows - SEG : rows, :], far_ref.at[0:SEG, 0:TILE]),
         (value_hbm.at[rows - SEG : rows, :], far_ref.at[0:SEG, TILE : 2 * TILE]),
-        (query_hbm, query_ref),
     ]
     copies = [pltpu.make_async_copy(a, b, sems.at[i]) for i, (a, b) in enumerate(copies)]
     for copy in copies:
@@ -166,15 +168,21 @@
         target[0:SEG, :] = jnp.zeros((SEG, 2 * TILE), BF16)
         target[SEG:, :] = rows
     lanes = lax.broadcasted_iota(jnp.int32, (1, TILE), 1)
-    head_partial, head_top, head_total = heads_out
+    head_partial, head_top, head_total, head_left, head_code = heads_out
     for segment in range(3):
         start = TILE if segment == 2 else 0
         width = 2 * TILE - start
-        mask = code_mask(codes[0:1, start:], query_code(own_codes, segment), 0 if segment == 2 else SEG, width)
+        mine = query_code(own_codes, segment)
+        if segment == 0:
+            head_code[...] = jnp.broadcast_to(mine, (SEG, TILE))
+        mask = code_mask(codes[0:1, start:], mine, 0 if segment == 2 else SEG, width)
         results = []
         for group in range(2):
             source = band if group == 0 else swapped
             left = stacked_queries(query_ref[SEG * segment : SEG * (segment + 1), :], group)
+            if segment == 0:
+                turned = pltpu.roll(left.astype(F32), SEG, 1).astype(BF16) if group else left
+                head_left[4 * SEG * group : 4 * SEG * (group + 1), :] = turned
             scores = lax.dot_general(
                 left, source[start:, 0:TILE], (((1,), (1,)), ((), ())), preferred_element_type=F32
             )
@@ -223,40 +231,36 @@
         ).astype(BF16)
 
 
-def far_part(query, far, codes, own_codes, halo_bias, partial_ref, top_ref, total_ref, mixed):
+def far_part(far, codes, halo_bias, partial_ref, top_ref, total_ref, left_ref, code_ref, mixed):
     lanes = lax.broadcasted_iota(jnp.int32, (1, TILE), 1)
-    mask = code_mask(codes[0:1, 0:SEG], query_code(own_codes, 0), 0, SEG)
-    sides = (far, swap_halves(far))
+    scores = lax.dot_general(
+        left_ref[...], far[:, 0:TILE], (((1,), (1,)), ((), ())), preferred_element_type=F32
+    )
+    values = far[:, TILE : 2 * TILE]
+    both = jnp.concatenate([values, pltpu.roll(values.astype(F32), SEG, 1).astype(BF16)], axis=1)
+    agree = jnp.broadcast_to(codes[0:1, 0:SEG], (SEG, SEG)) == code_ref[:, 0:SEG]
+    mask = jnp.where(agree, 0.0, NEG)
+    weights = []
+    olds = []
+    shares = []
+    for block in range(8):
+        spot = slice(SEG * (block % 4), SEG * (block % 4 + 1))
+        place = slice(SEG * block, SEG * (block + 1))
+        s = scores[place] + halo_bias[0, block // 4, spot, 0:SEG] + mask
+        old_top = top_ref[place, :]
+        top = jnp.maximum(jnp.max(s, axis=1, keepdims=True), old_top)
+        e = jnp.exp(s - top[:, 0:SEG])
+        old = jnp.exp(old_top - top)
+        share = 1.0 / (total_ref[place, :] * old + jnp.sum(e, axis=1, keepdims=True))
+        shares.append(share)
+        olds.append(old * share)
+        weights.append(e.astype(BF16))
+    blended = jnp.dot(jnp.concatenate(weights, axis=0), both, preferred_element_type=F32)
     results = []
-    for group in range(2):
-        left = stacked_queries(query, group)
-        scores = lax.dot_general(
-            left, sides[group][:, 0:TILE], (((1,), (1,)), ((), ())), preferred_element_type=F32
-        )
-        base = 4 * SEG * group
-        weights = []
-        olds = []
-        shares = []
-        for block in range(4):
-            spot = slice(SEG * block, SEG * (block + 1))
-            place = slice(base + SEG * block, base + SEG * (block + 1))
-            s = scores[spot] + halo_bias[0, group, spot, 0:SEG] + mask
-            old_top = top_ref[place, :]
-            top = jnp.maximum(jnp.max(s, axis=1, keepdims=True), old_top)
-            e = jnp.exp(s - top[:, 0:SEG])
-            old = jnp.exp(old_top - top)
-            share = 1.0 / (total_ref[place, :] * old + jnp.sum(e, axis=1, keepdims=True))
-            shares.append(share)
-            olds.append(old * share)
-            weights.append(e.astype(BF16))
-        blended = jnp.dot(
-            jnp.concatenate(weights, axis=0), sides[group][:, TILE : 2 * TILE], preferred_element_type=F32
-        )
-        for block in range(4):
-            place = slice(base + SEG * block, base + SEG * (block + 1))
-            results.append(
-                blended[SEG * block : SEG * (block + 1)] * shares[block] + partial_ref[place, :] * olds[block]
-            )
+    for block in range(8):
+        place = slice(SEG * block, SEG * (block + 1))
+        side = slice(TILE * (block // 4), TILE * (block // 4 + 1))
+        results.append(blended[place, side] * shares[block] + partial_ref[place, :] * olds[block])
     store_heads(mixed, 0, results, lanes)
 
 
@@ -265,10 +269,15 @@
     return pltpu.roll(codes, turn, 1) if turn else codes
 
 
-def before_one_kernel(query_ref, packed_ref, table_ref, halo_bias, partial_ref, top_ref, total_ref, own_bias, band, swapped):
+def before_one_kernel(
+    query_hbm, packed_ref, table_ref, query_ref, halo_bias, partial_ref, top_ref, total_ref, own_bias, band, swapped, sem
+):
     rows = query_ref.shape[0]
+    copy = pltpu.make_async_copy(query_hbm, query_ref, sem)
+    copy.start()
     fill_bias(table_ref, halo_bias, own_bias)
     own_codes = codes_of(packed_ref, rows, 2 * TILE - SEG)
+    copy.wait()
     own_part(
         query_ref[...], packed_ref[0:rows, :], own_codes, own_bias, band, swapped, partial_ref, top_ref, total_ref
     )
@@ -295,12 +304,13 @@
 
 def near_one_kernel(
     query_ref, near_ref, packed_ref, halo_bias, partial_ref, top_ref, total_ref, weight_ref, residual_ref,
-    out_ref, head_partial, head_top, head_total, band, swapped, mixed,
+    out_ref, head_partial, head_top, head_total, head_left, head_code, band, swapped, mixed,
 ):
     rows = query_ref.shape[0]
     near_part(
         query_ref, near_ref[0:rows, :], codes_of(near_ref, rows, 0), codes_of(packed_ref, rows, 2 * TILE - SEG),
-        halo_bias, partial_ref, top_ref, total_ref, band, swapped, mixed, (head_partial, head_top, head_total),
+        halo_bias, partial_ref, top_ref, total_ref, band, swapped, mixed,
+        (head_partial, head_top, head_total, head_left, head_code),
     )
     partial = jnp.dot(mixed[...], weight_ref[...], preferred_element_type=F32)
     half = residual_ref.shape[1]
@@ -309,25 +319,24 @@
 
 def near_two_kernel(
     query_ref, near_ref, near_codes_ref, packed_ref, halo_bias, partial_ref, top_ref, total_ref, weight_ref,
-    out_ref, head_partial, head_top, head_total, band, swapped, mixed,
+    out_ref, head_partial, head_top, head_total, head_left, head_code, band, swapped, mixed,
 ):
     rows = query_ref.shape[0]
     near_part(
         query_ref, near_ref[...], codes_of(near_codes_ref, rows, 0), codes_of(packed_ref, rows, 2 * TILE - SEG),
-        halo_bias, partial_ref, top_ref, total_ref, band, swapped, mixed, (head_partial, head_top, head_total),
+        halo_bias, partial_ref, top_ref, total_ref, band, swapped, mixed,
+        (head_partial, head_top, head_total, head_left, head_code),
     )
     out_ref[...] = jnp.dot(mixed[...], weight_ref[...], preferred_element_type=F32).astype(BF16)
 
 
 def far_one_kernel(
-    query_ref, far_ref, packed_ref, halo_bias, rest_ref, partial_ref, top_ref, total_ref, weight_ref, residual_ref,
+    far_ref, halo_bias, rest_ref, partial_ref, top_ref, total_ref, left_ref, code_ref, weight_ref, residual_ref,
     out_ref, mixed,
 ):
-    rows = query_ref.shape[0]
     out_ref[SEG:, :] = rest_ref[...]
     far_part(
-        query_ref[0:SEG, :], far_ref[0:SEG, :], codes_of(far_ref, SEG, 0), codes_of(packed_ref, rows, 2 * TILE - SEG),
-        halo_bias, partial_ref, top_ref, total_ref, mixed,
+        far_ref[0:SEG, :], codes_of(far_ref, SEG, 0), halo_bias, partial_ref, top_ref, total_ref, left_ref, code_ref, mixed
     )
     partial = jnp.dot(mixed[...], weight_ref[...], preferred_element_type=F32)
     half = residual_ref.shape[1]
@@ -335,16 +344,20 @@
 
 
 def far_two_kernel(
-    query_ref, far_ref, far_codes_ref, packed_ref, halo_bias, rest_ref, partial_ref, top_ref, total_ref, weight_ref,
-    out_ref, mixed,
-):
-    rows = query_ref.shape[0]
-    out_ref[SEG:, :] = rest_ref[...]
+    far_ref, far_codes_ref, halo_bias, rest_ref, partial_ref, top_ref, total_ref, left_ref, code_ref, weight_ref,
+    mine_ref, theirs_ref, mixed,
+):
+    half = mine_ref.shape[1]
+    first = lax.axis_index("tp") == 0
+    rest = rest_ref[...]
+    mine_ref[SEG:, :] = jnp.where(first, rest[:, 0:half], rest[:, half:])
+    theirs_ref[SEG:, :] = jnp.where(first, rest[:, half:], rest[:, 0:half])
     far_part(
-        query_ref[0:SEG, :], far_ref[...], codes_of(far_codes_ref, SEG, 0), codes_of(packed_ref, rows, 2 * TILE - SEG),
-        halo_bias, partial_ref, top_ref, total_ref, mixed,
-    )
-    out_ref[0:SEG, :] = jnp.dot(mixed[...], weight_ref[...], preferred_element_type=F32).astype(BF16)
+        far_ref[...], codes_of(far_codes_ref, SEG, 0), halo_bias, partial_ref, top_ref, total_ref, left_ref, code_ref, mixed
+    )
+    partial = jnp.dot(mixed[...], weight_ref[...], preferred_element_type=F32).astype(BF16)
+    mine_ref[0:SEG, :] = jnp.where(first, partial[:, 0:half], partial[:, half:])
+    theirs_ref[0:SEG, :] = jnp.where(first, partial[:, half:], partial[:, 0:half])
 
 
 def norm_kernel(both_ref, gain_ref, key_w_ref, value_w_ref, kv_ref, tail_ref, normed_ref, share_ref):
@@ -364,20 +377,29 @@
     share_ref[...] = jnp.where(lax.axis_index("tp") == 0, wide[:, 0:half], wide[:, half:]).astype(BF16)
 
 
-def last_kernel(both_ref, share_ref, out_ref):
-    half = share_ref.shape[1]
-    mine = pl.ds(pl.multiple_of(lax.axis_index("tp") * half, half), half)
-    out_ref[...] = (
-        share_ref[...].astype(F32) + both_ref[0, :, mine].astype(F32) + both_ref[1, :, mine].astype(F32)
-    ).astype(BF16)
-
-
-def call(kernel, outs, scratch, args, flops, mib=16, spaces=None):
+def last_kernel(both_ref, mine_ref, share_ref, out_hbm, out, sems):
+    first = lax.axis_index("tp") == 0
+    copies = []
+    parts = sems.shape[0]
+    rows = out.shape[0] // parts
+    for part in range(parts):
+        spot = slice(rows * part, rows * (part + 1))
+        theirs = jnp.where(first, both_ref[1, spot, :], both_ref[0, spot, :])
+        out[spot, :] = (
+            share_ref[spot, :].astype(F32) + mine_ref[spot, :].astype(F32) + theirs.astype(F32)
+        ).astype(BF16)
+        copies.append(pltpu.make_async_copy(out.at[spot, :], out_hbm.at[spot, :], sems.at[part]))
+        copies[-1].start()
+    for copy in copies:
+        copy.wait()
+
+
+def call(kernel, outs, scratch, args, flops, mib=16, spaces=None, out_space=pltpu.VMEM):
     return pl.pallas_call(
         kernel,
         out_shape=outs,
         in_specs=[whole()] * len(args) if spaces is None else [pl.BlockSpec(memory_space=s) for s in spaces],
-        out_specs=jax.tree.map(lambda _: whole(), outs),
+        out_specs=jax.tree.map(lambda _: pl.BlockSpec(memory_space=out_space), outs),
         scratch_shapes=scratch,
         compiler_params=params(mib),
         cost_estimate=cost(flops),
@@ -410,20 +432,32 @@
     far_scratch = [pltpu.VMEM((SEG, width), BF16)]
     stats = shape(24 * SEG, TILE, dtype=F32)
     head_stats = shape(8 * SEG, TILE, dtype=F32)
-    near_shapes = (shape(rows - SEG, channels), head_stats, head_stats, head_stats)
+    near_shapes = (
+        shape(rows - SEG, channels),
+        head_stats,
+        head_stats,
+        head_stats,
+        shape(8 * SEG, TILE),
+        shape(SEG, TILE, dtype=F32),
+    )
     own_shapes = (shape(2, 2, 4 * SEG, 2 * TILE, dtype=F32), stats, stats, stats)
-    packed, far_send, query_one = call(
+    packed, far_send = call(
         pack_kernel,
-        (shape(rows + 16, 2 * TILE), shape(SEG + 16, 2 * TILE), shape(rows, width)),
-        [pltpu.VMEM((8, 2 * TILE), F32), pltpu.VMEM((1, rows), jnp.int32), pltpu.SemaphoreType.DMA((6,))],
-        tuple(pltpu.with_memory_space_constraint(x, pltpu.HBM) for x in (key_first, value_first, docs, query_first)),
+        (shape(rows + 16, 2 * TILE), shape(SEG + 16, 2 * TILE)),
+        [pltpu.VMEM((8, 2 * TILE), F32), pltpu.VMEM((1, rows), jnp.int32), pltpu.SemaphoreType.DMA((7,))],
+        tuple(pltpu.with_memory_space_constraint(x, pltpu.HBM) for x in (key_first, value_first, docs)),
         1 << 20,
-        spaces=[pltpu.HBM] * 4,
+        spaces=[pltpu.HBM] * 3,
     )
     near_one = from_behind(packed, 1)
     far_one = from_behind(far_send, 2)
-    own_one = call(
-        before_one_kernel, own_shapes, before_scratch, (query_one, packed, bias_first), 1 << 31
+    query_one, *own_one = call(
+        before_one_kernel,
+        (shape(rows, width), *own_shapes),
+        [*before_scratch, pltpu.SemaphoreType.DMA],
+        (pltpu.with_memory_space_constraint(query_first, pltpu.HBM), packed, bias_first),
+        1 << 31,
+        spaces=[pltpu.HBM, pltpu.VMEM, pltpu.VMEM],
     )
     rest_one = call(
         near_one_kernel,
@@ -436,7 +470,7 @@
         far_one_kernel,
         shape(rows, channels),
         far_scratch,
-        (query_one, far_one, packed, own_one[0], *rest_one, out_first, residual),
+        (far_one, own_one[0], *rest_one, out_first, residual),
         1 << 31,
     )
     both_one = lax.all_gather(sent_one, "tp", axis=0)
@@ -463,15 +497,22 @@
         (query_two, near_two, near_one, packed, *own_two, out_second),
         1 << 31,
     )
-    sent_two = call(
+    mine_two, sent_two = call(
         far_two_kernel,
-        shape(rows, channels),
+        (shape(rows, half), shape(rows, half)),
         far_scratch,
-        (query_two, far_two, far_one, packed, own_two[0], *rest_two, out_second),
+        (far_two, far_one, own_two[0], *rest_two, out_second),
         1 << 31,
     )
     both_two = lax.all_gather(sent_two, "tp", axis=0)
-    return call(last_kernel, shape(rows, half), [], (both_two, share), 1 << 20)
+    return call(
+        last_kernel,
+        shape(rows, half),
+        [pltpu.VMEM((rows, half), BF16), pltpu.SemaphoreType.DMA((4,))],
+        (both_two, mine_two, share),
+        1 << 20,
+        out_space=pltpu.HBM,
+    )
 
 
 def solution(mesh):

time: 43.9 us -> 43.3 us (0.986)
  waiting for transfers between devices: 14.5 us -> 14 us
    ppermute x4, waiting for transfers between devices: 14.5 us -> 14 us  [from_behind(): return lax.ppermute(block, 'sp', route)]
  transfers between devices with their start and end apart: 4 -> 4, of which waited for: 2 -> 2; matrix products, arithmetic and copies ran while one was open for 0% -> 0% of each run, Pallas kernels for 15% -> 16%
where the time goes in v3:
time: 43.3 us; the launch traced here: 43 us
  waiting for transfers between devices  14 us (32%)
  starting transfers between devices  10.8 us (25%)
  Pallas kernels  10.7 us (25%)
  blocking collectives  7.18 us (17%)
    ppermute x4, waiting for transfers between devices, from_behind(): return lax.ppermute(block, 'sp', route)  14 us
    ppermute x4, starting transfers between devices, from_behind(): return lax.ppermute(block, 'sp', route)  10.8 us
    pallas_call x9, Pallas kernels, call(): pl.pallas_call(kernel, out_shape=outs, in_specs=[whole()] * len(args) if...  10.7 us
    all_gather x1, blocking collectives, body(): both_one = lax.all_gather(sent_one, 'tp', axis=0)  4.23 us
    all_gather x1, blocking collectives, body(): both_two = lax.all_gather(sent_two, 'tp', axis=0)  2.95 us
  transfers between devices with their start and end apart: 4, of which 2 were waited for; matrix products, arithmetic and copies ran while one was open for 0% of the time, Pallas kernels for 16%

profile of v3, /device:TPU:257, one launch (start us, length us, event | category | flops | bytes accessed | tf_op | source)
XLA Modules:
  0.0 43.0 jit_solution(15371463611237052157)
XLA Ops:
  0.0 0.9 %shard_map.127 = (bf16[208,256]{1,0:T(8,128)(2,1)S(1)}, bf16[80,256]{1,0:T(8,128)(2,1)S(1)}) custom-call(bf16[192,128]{1,0:T(8,128)(2,1)} %key_hbm.1, bf16[192,128]{1,0:T(8,128)(2,1)} %value_hbm.1, s32[1,192]{1,0:T(1,128)} %bitcast.7), custom_call_target="tpu_custom_call" | custom-call | flops 1048576 | bytes 1048576 | tf_op jit(solution)/shard_map/pallas_call | solution.py:398
  0.9 4.7 %collective-permute-start = (bf16[80,256]{1,0:T(8,128)(2,1)S(1)}, bf16[80,256]{1,0:T(8,128)(2,1)S(1)}, u32[]{:S(2)}, u32[]{:S(2)}) collective-permute-start(bf16[80,256]{1,0:T(8,128)(2,1)S(1)} %get-tuple-element.35), channel_id=1, source_target_pairs={{0,4},{2,6},{4,8},{6,10},{8,12},{10,14},{12,16},{14,18},{16,20},{1... | collective-permute-start | bytes 122888 | tf_op jit(solution)/shard_map/ppermute | solution.py:39
  5.6 0.0 copy-start
  5.6 0.0 copy-start.5
  5.6 2.4 %collective-permute-start.1 = (bf16[208,256]{1,0:T(8,128)(2,1)S(1)}, bf16[208,256]{1,0:T(8,128)(2,1)S(1)}, u32[]{:S(2)}, u32[]{:S(2)}) collective-permute-start(bf16[208,256]{1,0:T(8,128)(2,1)S(1)} %get-tuple-element.36.packed_ref), channel_id=1, source_target_pairs={{0,2},{2,4},{4,6},{6,8},{8,10},{10,12},{12,14},{14,16},{16,18},{18... | collective-permute-start | bytes 319496 | tf_op jit(solution)/shard_map/ppermute | solution.py:39
  7.9 0.0 copy-done.6
  8.0 2.5 %shard_map.128 = (bf16[192,512]{1,0:T(8,128)(2,1)S(1)}, f32[2,2,256,256]{3,2,1,0:T(8,128)S(1)}, f32[1536,128]{1,0:T(8,128)S(1)}, f32[1536,128]{1,0:T(8,128)S(1)}, f32[1536,128]{1,0:T(8,128)S(1)}) custom-call(bf16[192,512]{1,0:T(8,128)(2,1)} %query_hbm.1, bf16[208,256]{1,0:T(8,128)(2,1)S(1)} %get-tuple-element.36.packed_ref, f32[8,513]{1,0:T(8,128)S(1)} %copy-done.6), custom_call_target="tpu_custom_call" | custom-call | flops 2147483648 | bytes 1048576 | tf_op jit(solution)/shard_map/pallas_call | solution.py:398
  10.4 6.2 %collective-permute-done.1.near_ref.near_codes_ref = bf16[208,256]{1,0:T(8,128)(2,1)S(1)} collective-permute-done((bf16[208,256]{1,0:T(8,128)(2,1)S(1)}, bf16[208,256]{1,0:T(8,128)(2,1)S(1)}, u32[]{:S(2)}, u32[]{:S(2)}) %collective-permute-start.1) | collective-permute-done | bytes 106528 | tf_op jit(solution)/shard_map/ppermute | solution.py:39
  16.6 0.0 copy-done
  16.6 0.0 copy-done.5
  16.6 1.5 %shard_map.129 = (bf16[128,1024]{1,0:T(8,128)(2,1)S(1)}, f32[512,128]{1,0:T(8,128)S(1)}, f32[512,128]{1,0:T(8,128)S(1)}, f32[512,128]{1,0:T(8,128)S(1)}, bf16[51...) custom-call(bf16[192,512]{1,0:T(8,128)(2,1)S(1)} %get-tuple-element.38.query_ref, ...), custom_call_target="tpu_custom_call" | custom-call | flops 2147483648 | bytes 1048576 | tf_op jit(solution)/shard_map/pallas_call | solution.py:398
  18.1 0.0 collective-permute-done.far_ref.far_codes_ref
  18.1 0.8 %shard_map.130 = bf16[192,1024]{1,0:T(8,128)(2,1)S(1)} custom-call(bf16[80,256]{1,0:T(8,128)(2,1)S(1)} %collective-permute-done.far_ref.far_codes_ref, f32[2,2,256,256]{3,2,1,0:T(8,128)S(1)} %get-tuple-element.37.halo_bias, bf16[128,1024]{1,0:T(8,128)(2,1)S(1)} %get-tuple-element.42.rest_ref, f32[512,128]{1,0:T(8,128)S(1)} %get-tuple-element.43.partial_ref, ...), custom_call_target="tpu_custom_call" | custom-call | flops 2147483648 | bytes 1048576 | tf_op jit(solution)/shard_map/pallas_call | solution.py:398
  18.9 0.0 copy-start.3
  18.9 0.0 copy-start.4
  18.9 0.0 copy-start.8
  18.9 4.2 %all-gather = bf16[384,1024]{1,0:T(8,128)(2,1)S(1)} all-gather(bf16[192,1024]{1,0:T(8,128)(2,1)S(1)} %shard_map.130), channel_id=2, replica_groups=mesh['sp'=256,'tp'=2] {'tp'}, dimensions={0}, use_global_device_ids=true | all-gather | bytes 1179648 | tf_op jit(solution)/shard_map/all_gather | solution.py:476
  23.1 0.0 copy-done.3
  23.1 0.0 copy-done.4
  23.1 0.0 copy-done.8
  23.2 0.0 copy-start.7
  23.2 0.6 %shard_map.131 = (bf16[192,256]{1,0:T(8,128)(2,1)S(1)}, bf16[64,256]{1,0:T(8,128)(2,1)S(1)}, bf16[192,1024]{1,0:T(8,128)(2,1)S(1)}, bf16[192,512]{1,0:T(8,128)(2,1)S(1)}) custom-call(bf16[2,192,1024]{2,1,0:T(8,128)(2,1)S(1)} %bitcast.5, f32[1,1024]{1,0:T(1,128)S(1)} %bitcast.6, bf16[1024,128]{1,0:T(8,128)(2,1)S(1)} %copy-done.3, bf16[1024,128]{1,0:T(8,128)(2,1)S(1)} %copy-done.4), custom_call_target="tpu_custom_call" | custom-call | flops 1073741824 | bytes 1048576 | tf_op jit(solution)/shard_map/pallas_call | solution.py:398
  23.8 1.9 %collective-permute-start.2 = (bf16[64,256]{1,0:T(8,128)(2,1)S(1)}, bf16[64,256]{1,0:T(8,128)(2,1)S(1)}, u32[]{:S(2)}, u32[]{:S(2)}) collective-permute-start(bf16[64,256]{1,0:T(8,128)(2,1)S(1)} %get-tuple-element.48), channel_id=1, source_target_pairs={{0,4},{2,6},{4,8},{6,10},{8,12},{10,14},{12,16},{14,18},{16,20},{1... | collective-permute-start | bytes 98312 | tf_op jit(solution)/shard_map/ppermute | solution.py:39
  25.7 1.9 %collective-permute-start.3 = (bf16[192,256]{1,0:T(8,128)(2,1)S(1)}, bf16[192,256]{1,0:T(8,128)(2,1)S(1)}, u32[]{:S(2)}, u32[]{:S(2)}) collective-permute-start(bf16[192,256]{1,0:T(8,128)(2,1)S(1)} %get-tuple-element.50.kv_ref), channel_id=1, source_target_pairs={{0,2},{2,4},{4,6},{6,8},{8,10},{10,12},{12,14},{14,16},{16,18},{18... | collective-permute-start | bytes 294920 | tf_op jit(solution)/shard_map/ppermute | solution.py:39
  27.6 0.0 copy-start.2
  27.6 1.5 %shard_map.132 = (bf16[192,512]{1,0:T(8,128)(2,1)S(1)}, f32[2,2,256,256]{3,2,1,0:T(8,128)S(1)}, f32[1536,128]{1,0:T(8,128)S(1)}, f32[1536,128]{1,0:T(8,128)S(1)}, f32[1536,128]{1,0:T(8,128)S(1)}) custom-call(bf16[192,1024]{1,0:T(8,128)(2,1)S(1)} %get-tuple-element.49.normed_ref, bf16[1024,512]{1,0:T(8,128)(2,1)S(1)} %copy-done.1, ...), custom_call_target="tpu_custom_call" | custom-call | flops 2147483648 | bytes 1048576 | tf_op jit(solution)/shard_map/pallas_call | solution.py:398
  29.2 7.8 %collective-permute-done.3.near_ref = bf16[192,256]{1,0:T(8,128)(2,1)S(1)} collective-permute-done((bf16[192,256]{1,0:T(8,128)(2,1)S(1)}, bf16[192,256]{1,0:T(8,128)(2,1)S(1)}, u32[]{:S(2)}, u32[]{:S(2)}) %collective-permute-start.3) | collective-permute-done | bytes 98336 | tf_op jit(solution)/shard_map/ppermute | solution.py:39
  37.0 1.5 %shard_map.133 = (bf16[128,1024]{1,0:T(8,128)(2,1)S(1)}, f32[512,128]{1,0:T(8,128)S(1)}, f32[512,128]{1,0:T(8,128)S(1)}, f32[512,128]{1,0:T(8,128)S(1)}, bf16[51...) custom-call(bf16[192,512]{1,0:T(8,128)(2,1)S(1)} %get-tuple-element.52.query_ref, ...), custom_call_target="tpu_custom_call" | custom-call | flops 2147483648 | bytes 1048576 | tf_op jit(solution)/shard_map/pallas_call | solution.py:398
  38.5 0.0 collective-permute-done.2.far_ref
  38.5 0.8 %shard_map.134 = (bf16[192,512]{1,0:T(8,128)(2,1)S(1)}, bf16[192,512]{1,0:T(8,128)(2,1)S(1)}) custom-call(bf16[64,256]{1,0:T(8,128)(2,1)S(1)} %collective-permute-done.2.far_ref, bf16[80,256]{1,0:T(8,128)(2,1)S(1)} %collective-permute-done.far_ref.far_codes_ref, f32[2,2,256,256]{3,2,1,0:T(8,128)S(1)} %get-tuple-element.51.halo_bias, ...), custom_call_target="tpu_custom_call" | custom-call | flops 2147483648 | bytes 1048576 | tf_op jit(solution)/shard_map/pallas_call | solution.py:398
  39.3 3.0 %all-gather.1 = bf16[384,512]{1,0:T(8,128)(2,1)S(1)} all-gather(bf16[192,512]{1,0:T(8,128)(2,1)S(1)} %get-tuple-element.62), channel_id=3, replica_groups=mesh['sp'=256,'tp'=2] {'tp'}, dimensions={0}, use_global_device_ids=true | all-gather | bytes 589824 | tf_op jit(solution)/shard_map/all_gather | solution.py:507
  42.2 0.7 %shard_map.135 = bf16[192,512]{1,0:T(8,128)(2,1)} custom-call(bf16[2,192,512]{2,1,0:T(8,128)(2,1)S(1)} %bitcast.4, bf16[192,512]{1,0:T(8,128)(2,1)S(1)} %get-tuple-element.63.mine_ref, bf16[192,512]{1,0:T(8,128)(2,1)S(1)} %get-tuple-element.64.share_ref), custom_call_target="tpu_custom_call" | custom-call | flops 1048576 | bytes 1048576 | tf_op jit(solution)/shard_map/pallas_call | solution.py:398
  (5 shorter events, 0.0 us)
Async XLA Ops:
  0.0 7.9 %copy-start.6 = (f32[8,513]{1,0:T(8,128)S(1)}, f32[8,513]{1,0:T(8,128)}, u32[]{:S(2)}) copy-start(f32[8,513]{1,0:T(8,128)} %table_ref.2) | copy-start | bytes 49252
  0.9 17.2 %collective-permute-start = (bf16[80,256]{1,0:T(8,128)(2,1)S(1)}, bf16[80,256]{1,0:T(8,128)(2,1)S(1)}, u32[]{:S(2)}, u32[]{:S(2)}) collective-permute-start(bf16[80,256]{1,0:T(8,128)(2,1)S(1)} %get-tuple-element.35), channel_id=1, source_target_pairs={{0,4},{2,6},{4,8},{6,10},{8,12},{10,14},{12,16},{14,18},{16,20},{1... | collective-permute-start | bytes 122888 | tf_op jit(solution)/shard_map/ppermute | solution.py:39
  5.6 11.0 %copy-start = (bf16[512,1024]{1,0:T(8,128)(2,1)S(1)}, bf16[512,1024]{1,0:T(8,128)(2,1)}, u32[]{:S(2)}) copy-start(bf16[512,1024]{1,0:T(8,128)(2,1)} %weight_ref.6) | copy-start | bytes 3145732
  5.6 11.0 %copy-start.5 = (bf16[192,512]{1,0:T(8,128)(2,1)S(1)}, bf16[192,512]{1,0:T(8,128)(2,1)}, u32[]{:S(2)}) copy-start(bf16[192,512]{1,0:T(8,128)(2,1)} %residual_ref.3) | copy-start | bytes 589828
  5.6 11.0 %collective-permute-start.1 = (bf16[208,256]{1,0:T(8,128)(2,1)S(1)}, bf16[208,256]{1,0:T(8,128)(2,1)S(1)}, u32[]{:S(2)}, u32[]{:S(2)}) collective-permute-start(bf16[208,256]{1,0:T(8,128)(2,1)S(1)} %get-tuple-element.36.packed_ref), channel_id=1, source_target_pairs={{0,2},{2,4},{4,6},{6,8},{8,10},{10,12},{12,14},{14,16},{16,18},{18... | collective-permute-start | bytes 319496 | tf_op jit(solution)/shard_map/ppermute | solution.py:39
  18.9 4.3 %copy-start.3 = (bf16[1024,128]{1,0:T(8,128)(2,1)S(1)}, bf16[1024,128]{1,0:T(8,128)(2,1)}, u32[]{:S(2)}) copy-start(bf16[1024,128]{1,0:T(8,128)(2,1)} %key_w_ref.1) | copy-start | bytes 786436
  18.9 4.3 %copy-start.4 = (bf16[1024,128]{1,0:T(8,128)(2,1)S(1)}, bf16[1024,128]{1,0:T(8,128)(2,1)}, u32[]{:S(2)}) copy-start(bf16[1024,128]{1,0:T(8,128)(2,1)} %value_w_ref.1) | copy-start | bytes 786436
  18.9 4.3 %copy-start.8 = (f32[1024]{0:T(1024)S(1)}, f32[1024]{0:T(1024)}, u32[]{:S(2)}) copy-start(f32[1024]{0:T(1024)} %param.20) | copy-start | bytes 12292
  23.1 4.5 %copy-start.1 = (bf16[1024,512]{1,0:T(8,128)(2,1)S(1)}, bf16[1024,512]{1,0:T(8,128)(2,1)}, u32[]{:S(2)}) copy-start(bf16[1024,512]{1,0:T(8,128)(2,1)} %weight_ref.7) | copy-start | bytes 3145732
  23.2 4.5 %copy-start.7 = (f32[8,513]{1,0:T(8,128)S(1)}, f32[8,513]{1,0:T(8,128)}, u32[]{:S(2)}) copy-start(f32[8,513]{1,0:T(8,128)} %table_ref.3) | copy-start | bytes 49252
  23.8 14.7 %collective-permute-start.2 = (bf16[64,256]{1,0:T(8,128)(2,1)S(1)}, bf16[64,256]{1,0:T(8,128)(2,1)S(1)}, u32[]{:S(2)}, u32[]{:S(2)}) collective-permute-start(bf16[64,256]{1,0:T(8,128)(2,1)S(1)} %get-tuple-element.48), channel_id=1, source_target_pairs={{0,4},{2,6},{4,8},{6,10},{8,12},{10,14},{12,16},{14,18},{16,20},{1... | collective-permute-start | bytes 98312 | tf_op jit(solution)/shard_map/ppermute | solution.py:39
  25.7 11.3 %collective-permute-start.3 = (bf16[192,256]{1,0:T(8,128)(2,1)S(1)}, bf16[192,256]{1,0:T(8,128)(2,1)S(1)}, u32[]{:S(2)}, u32[]{:S(2)}) collective-permute-start(bf16[192,256]{1,0:T(8,128)(2,1)S(1)} %get-tuple-element.50.kv_ref), channel_id=1, source_target_pairs={{0,2},{2,4},{4,6},{6,8},{8,10},{10,12},{12,14},{14,16},{16,18},{18... | collective-permute-start | bytes 294920 | tf_op jit(solution)/shard_map/ppermute | solution.py:39
  27.6 9.4 %copy-start.2 = (bf16[512,1024]{1,0:T(8,128)(2,1)S(1)}, bf16[512,1024]{1,0:T(8,128)(2,1)}, u32[]{:S(2)}) copy-start(bf16[512,1024]{1,0:T(8,128)(2,1)} %weight_ref.9) | copy-start | bytes 3145732

commit v4 on v3

--- a/solution.py
+++ b/solution.py
@@ -33,9 +33,13 @@
     return pl.CostEstimate(flops=flops, bytes_accessed=nbytes, transcendentals=transcendentals)
 
 
-def from_behind(block, distance):
+def from_behind(block, distance, across=False):
     devices = range(lax.axis_size("sp"))
     route = [(i - distance, i) for i in devices if i - distance in devices]
+    if across:
+        return lax.ppermute(
+            block, ("sp", "tp"), [(2 * a + core, 2 * b + 1 - core) for a, b in route for core in range(2)]
+        )
     return lax.ppermute(block, "sp", route)
 
 
@@ -270,17 +274,26 @@
 
 
 def before_one_kernel(
-    query_hbm, packed_ref, table_ref, query_ref, halo_bias, partial_ref, top_ref, total_ref, own_bias, band, swapped, sem
+    query_hbm, key_w_hbm, value_w_hbm, packed_ref, table_ref, query_ref, weight_ref, halo_bias, partial_ref, top_ref,
+    total_ref, own_bias, band, swapped, sems,
 ):
     rows = query_ref.shape[0]
-    copy = pltpu.make_async_copy(query_hbm, query_ref, sem)
+    copy = pltpu.make_async_copy(query_hbm, query_ref, sems.at[0])
     copy.start()
+    weight_copies = [
+        pltpu.make_async_copy(key_w_hbm, weight_ref.at[:, 0:TILE], sems.at[1]),
+        pltpu.make_async_copy(value_w_hbm, weight_ref.at[:, TILE : 2 * TILE], sems.at[2]),
+    ]
+    for weight_copy in weight_copies:
+        weight_copy.start()
     fill_bias(table_ref, halo_bias, own_bias)
     own_codes = codes_of(packed_ref, rows, 2 * TILE - SEG)
     copy.wait()
     own_part(
         query_ref[...], packed_ref[0:rows, :], own_codes, own_bias, band, swapped, partial_ref, top_ref, total_ref
     )
+    for weight_copy in weight_copies:
+        weight_copy.wait()
 
 
 def before_two_kernel(
@@ -360,21 +373,19 @@
     theirs_ref[0:SEG, :] = jnp.where(first, partial[:, half:], partial[:, 0:half])
 
 
-def norm_kernel(both_ref, gain_ref, key_w_ref, value_w_ref, kv_ref, tail_ref, normed_ref, share_ref):
-    layer = (both_ref[0].astype(F32) + both_ref[1].astype(F32)).astype(BF16)
+def norm_kernel(both_ref, gain_ref, weight_ref, other_weight_ref, kv_ref, send_ref, tail_ref, normed_ref, share_ref):
+    layer = both_ref[0] + both_ref[1]
     wide = layer.astype(F32)
     rows, channels = wide.shape
     scale = lax.rsqrt(jnp.mean(wide * wide, axis=1, keepdims=True) + EPS)
     normed = (wide * scale * gain_ref[...]).astype(BF16)
-    keys = jnp.dot(normed, key_w_ref[...], preferred_element_type=F32).astype(BF16)
-    values = jnp.dot(normed, value_w_ref[...], preferred_element_type=F32).astype(BF16)
-    kv_ref[:, 0:TILE] = keys
-    kv_ref[:, TILE : 2 * TILE] = values
-    tail_ref[:, 0:TILE] = keys[rows - SEG :]
-    tail_ref[:, TILE : 2 * TILE] = values[rows - SEG :]
+    send = jnp.dot(normed, other_weight_ref[...], preferred_element_type=F32).astype(BF16)
+    send_ref[...] = send
+    tail_ref[...] = send[rows - SEG :]
+    kv_ref[...] = jnp.dot(normed, weight_ref[...], preferred_element_type=F32).astype(BF16)
     normed_ref[...] = normed
     half = channels // 2
-    share_ref[...] = jnp.where(lax.axis_index("tp") == 0, wide[:, 0:half], wide[:, half:]).astype(BF16)
+    share_ref[...] = jnp.where(lax.axis_index("tp") == 0, layer[:, 0:half], layer[:, half:])
 
 
 def last_kernel(both_ref, mine_ref, share_ref, out_hbm, out, sems):
@@ -451,14 +462,19 @@
     )
     near_one = from_behind(packed, 1)
     far_one = from_behind(far_send, 2)
-    query_one, *own_one = call(
+    query_one, weights, *own_one = call(
         before_one_kernel,
-        (shape(rows, width), *own_shapes),
-        [*before_scratch, pltpu.SemaphoreType.DMA],
-        (pltpu.with_memory_space_constraint(query_first, pltpu.HBM), packed, bias_first),
+        (shape(rows, width), shape(channels, 2 * TILE), *own_shapes),
+        [*before_scratch, pltpu.SemaphoreType.DMA((3,))],
+        (
+            *(pltpu.with_memory_space_constraint(x, pltpu.HBM) for x in (query_first, key_w, value_w)),
+            packed,
+            bias_first,
+        ),
         1 << 31,
-        spaces=[pltpu.HBM, pltpu.VMEM, pltpu.VMEM],
-    )
+        spaces=[pltpu.HBM] * 3 + [pltpu.VMEM] * 2,
+    )
+    other_weights = lax.ppermute(weights, "tp", [(0, 1), (1, 0)])
     rest_one = call(
         near_one_kernel,
         near_shapes,
@@ -474,15 +490,21 @@
         1 << 31,
     )
     both_one = lax.all_gather(sent_one, "tp", axis=0)
-    kv_two, tail_two, normed, share = call(
+    kv_two, send_two, tail_two, normed, share = call(
         norm_kernel,
-        (shape(rows, 2 * TILE), shape(SEG, 2 * TILE), shape(rows, channels), shape(rows, half)),
+        (
+            shape(rows, 2 * TILE),
+            shape(rows, 2 * TILE),
+            shape(SEG, 2 * TILE),
+            shape(rows, channels),
+            shape(rows, half),
+        ),
         [],
-        (both_one, gain, key_w, value_w),
+        (both_one, gain, weights, other_weights),
         1 << 30,
     )
-    near_two = from_behind(kv_two, 1)
-    far_two = from_behind(tail_two, 2)
+    near_two = from_behind(send_two, 1, across=True)
+    far_two = from_behind(tail_two, 2, across=True)
     query_two, *own_two = call(
         before_two_kernel,
         (shape(rows, width), *own_shapes),

time: 43.3 us -> 43 us (level)
  starting transfers between devices: 10.8 us -> 14 us
  waiting for transfers between devices: 14 us -> 12 us
  blocking collectives: 7.18 us -> 6.19 us
    ppermute x4 -> x2, waiting for transfers between devices: 14 us -> 3.38 us  [from_behind(): return lax.ppermute(block, 'sp', route)]
    ppermute x0 -> x3, waiting for transfers between devices: none -> 8.61 us  [the longest x2 8.6 us: from_behind(): lax.ppermute(block, ('sp', 'tp'), [(2 * a + core, 2 * b + 1 - core) for a...]
    ppermute x0 -> x3, starting transfers between devices: none -> 6.99 us  [the longest x2 3.84 us: from_behind(): lax.ppermute(block, ('sp', 'tp'), [(2 * a + core, 2 * b + 1 - core) for a...]
    ppermute x4 -> x2, starting transfers between devices: 10.8 us -> 7 us  [from_behind(): return lax.ppermute(block, 'sp', route)]
    all_gather x1, blocking collectives: 2.95 us -> 2.09 us  [body(): both_two = lax.all_gather(sent_two, 'tp', axis=0)]
    pallas_call x9, Pallas kernels: 10.7 us -> 10.3 us  [call(): pl.pallas_call(kernel, out_shape=outs, in_specs=[whole()] * len(args) if...]
  transfers between devices with their start and end apart: 4 -> 5, of which waited for: 2 -> 2; matrix products, arithmetic and copies ran while one was open for 0% -> 0% of each run, Pallas kernels for 16% -> 17%
where the time goes in v4:
time: 43 us; the launch traced here: 42.7 us
  starting transfers between devices  14 us (33%)
  waiting for transfers between devices  12 us (28%)
  Pallas kernels  10.3 us (24%)
  blocking collectives  6.19 us (14%)
    pallas_call x9, Pallas kernels, call(): pl.pallas_call(kernel, out_shape=outs, in_specs=[whole()] * len(args) if...  10.3 us
    ppermute x2, waiting for transfers between devices, from_behind(): lax.ppermute(block, ('sp', 'tp'), [(2 * a + core, 2 * b + 1 - core) for a...  8.6 us
    ppermute x2, starting transfers between devices, from_behind(): return lax.ppermute(block, 'sp', route)  7 us
    all_gather x1, blocking collectives, body(): both_one = lax.all_gather(sent_one, 'tp', axis=0)  4.1 us
    ppermute x2, starting transfers between devices, from_behind(): lax.ppermute(block, ('sp', 'tp'), [(2 * a + core, 2 * b + 1 - core) for a...  3.84 us
    ppermute x2, waiting for transfers between devices, from_behind(): return lax.ppermute(block, 'sp', route)  3.38 us
    ppermute x1, starting transfers between devices, body(): other_weights = lax.ppermute(weights, 'tp', [(0, 1), (1, 0)])  3.15 us
    all_gather x1, blocking collectives, body(): both_two = lax.all_gather(sent_two, 'tp', axis=0)  2.09 us
  transfers between devices with their start and end apart: 5, of which 2 were waited for; matrix products, arithmetic and copies ran while one was open for 0% of the time, Pallas kernels for 17%

profile of v4, /device:TPU:257, one launch (start us, length us, event | category | flops | bytes accessed | tf_op | source)
XLA Modules:
  0.0 42.7 jit_solution(18094000588852253194)
XLA Ops:
  0.0 0.9 %shard_map.127 = (bf16[208,256]{1,0:T(8,128)(2,1)S(1)}, bf16[80,256]{1,0:T(8,128)(2,1)S(1)}) custom-call(bf16[192,128]{1,0:T(8,128)(2,1)} %key_hbm.1, bf16[192,128]{1,0:T(8,128)(2,1)} %value_hbm.1, s32[1,192]{1,0:T(1,128)} %bitcast.7), custom_call_target="tpu_custom_call" | custom-call | flops 1048576 | bytes 1048576 | tf_op jit(solution)/shard_map/pallas_call | solution.py:409
  0.9 4.7 %collective-permute-start = (bf16[80,256]{1,0:T(8,128)(2,1)S(1)}, bf16[80,256]{1,0:T(8,128)(2,1)S(1)}, u32[]{:S(2)}, u32[]{:S(2)}) collective-permute-start(bf16[80,256]{1,0:T(8,128)(2,1)S(1)} %get-tuple-element.37), channel_id=1, source_target_pairs={{0,4},{2,6},{4,8},{6,10},{8,12},{10,14},{12,16},{14,18},{16,20},{1... | collective-permute-start | bytes 122888 | tf_op jit(solution)/shard_map/ppermute | solution.py:43
  5.6 0.0 copy-start
  5.6 0.0 copy-start.3
  5.6 2.4 %collective-permute-start.1 = (bf16[208,256]{1,0:T(8,128)(2,1)S(1)}, bf16[208,256]{1,0:T(8,128)(2,1)S(1)}, u32[]{:S(2)}, u32[]{:S(2)}) collective-permute-start(bf16[208,256]{1,0:T(8,128)(2,1)S(1)} %get-tuple-element.38.packed_ref), channel_id=1, source_target_pairs={{0,2},{2,4},{4,6},{6,8},{8,10},{10,12},{12,14},{14,16},{16,18},{18... | collective-permute-start | bytes 319496 | tf_op jit(solution)/shard_map/ppermute | solution.py:43
  7.9 0.0 copy-done.4
  8.0 2.1 %shard_map.128 = (bf16[192,512]{1,0:T(8,128)(2,1)S(1)}, bf16[1024,256]{1,0:T(8,128)(2,1)S(1)}, f32[2,2,256,256]{3,2,1,0:T(8,128)S(1)}, f32[1536,128]{1,0:T(8,128...) custom-call(bf16[192,512]{1,0:T(8,128)(2,1)} %query_hbm.1, bf16[1024,128]{1,0:T(8,128)(2,1)} %key_w_hbm.1, ...), custom_call_target="tpu_custom_call" | custom-call | flops 2147483648 | bytes 1048576 | tf_op jit(solution)/shard_map/pallas_call | solution.py:409
  10.1 3.1 %collective-permute-start.2 = (bf16[1024,256]{1,0:T(8,128)(2,1)S(1)}, bf16[1024,256]{1,0:T(8,128)(2,1)S(1)}, u32[]{:S(2)}, u32[]{:S(2)}) collective-permute-start(bf16[1024,256]{1,0:T(8,128)(2,1)S(1)} %get-tuple-element.50.weight_ref), channel_id=1, source_target_pairs={{0,1},{1,0},{2,3},{3,2},{4,5},{5,4},{6,7},{7,6},{8,9},{9,8},{10,11... | collective-permute-start | bytes 1572872 | tf_op jit(solution)/shard_map/ppermute | solution.py:477
  13.2 3.4 %collective-permute-done.1.near_ref.near_codes_ref = bf16[208,256]{1,0:T(8,128)(2,1)S(1)} collective-permute-done((bf16[208,256]{1,0:T(8,128)(2,1)S(1)}, bf16[208,256]{1,0:T(8,128)(2,1)S(1)}, u32[]{:S(2)}, u32[]{:S(2)}) %collective-permute-start.1) | collective-permute-done | bytes 106528 | tf_op jit(solution)/shard_map/ppermute | solution.py:43
  16.6 0.0 copy-done
  16.6 0.0 copy-done.3
  16.6 1.5 %shard_map.129 = (bf16[128,1024]{1,0:T(8,128)(2,1)S(1)}, f32[512,128]{1,0:T(8,128)S(1)}, f32[512,128]{1,0:T(8,128)S(1)}, f32[512,128]{1,0:T(8,128)S(1)}, bf16[51...) custom-call(bf16[192,512]{1,0:T(8,128)(2,1)S(1)} %get-tuple-element.40.query_ref, ...), custom_call_target="tpu_custom_call" | custom-call | flops 2147483648 | bytes 1048576 | tf_op jit(solution)/shard_map/pallas_call | solution.py:409
  18.1 0.0 collective-permute-done.far_ref.far_codes_ref
  18.1 0.8 %shard_map.130 = bf16[192,1024]{1,0:T(8,128)(2,1)S(1)} custom-call(bf16[80,256]{1,0:T(8,128)(2,1)S(1)} %collective-permute-done.far_ref.far_codes_ref, f32[2,2,256,256]{3,2,1,0:T(8,128)S(1)} %get-tuple-element.39.halo_bias, bf16[128,1024]{1,0:T(8,128)(2,1)S(1)} %get-tuple-element.44.rest_ref, f32[512,128]{1,0:T(8,128)S(1)} %get-tuple-element.45.partial_ref, ...), custom_call_target="tpu_custom_call" | custom-call | flops 2147483648 | bytes 1048576 | tf_op jit(solution)/shard_map/pallas_call | solution.py:409
  18.9 0.0 copy-start.6
  18.9 4.1 %all-gather = bf16[384,1024]{1,0:T(8,128)(2,1)S(1)} all-gather(bf16[192,1024]{1,0:T(8,128)(2,1)S(1)} %shard_map.130), channel_id=2, replica_groups=mesh['sp'=256,'tp'=2] {'tp'}, dimensions={0}, use_global_device_ids=true | all-gather | bytes 1179648 | tf_op jit(solution)/shard_map/all_gather | solution.py:492
  23.0 0.0 collective-permute-done.2.other_weight_ref
  23.0 0.0 copy-done.6
  23.0 0.5 %shard_map.131 = (bf16[192,256]{1,0:T(8,128)(2,1)S(1)}, bf16[192,256]{1,0:T(8,128)(2,1)S(1)}, bf16[64,256]{1,0:T(8,128)(2,1)S(1)}, bf16[192,1024]{1,0:T(8,128)(2,1)S(1)}, bf16[192,512]{1,0:T(8,128)(2,1)S(1)}) custom-call(bf16[2,192,1024]{2,1,0:T(8,128)(2,1)S(1)} %bitcast.5, f32[1,1024]{1,0:T(1,128)S(1)} %bitcast.6, ...), custom_call_target="tpu_custom_call" | custom-call | flops 1073741824 | bytes 1048576 | tf_op jit(solution)/shard_map/pallas_call | solution.py:409
  23.5 1.9 %collective-permute-start.3 = (bf16[64,256]{1,0:T(8,128)(2,1)S(1)}, bf16[64,256]{1,0:T(8,128)(2,1)S(1)}, u32[]{:S(2)}, u32[]{:S(2)}) collective-permute-start(bf16[64,256]{1,0:T(8,128)(2,1)S(1)} %get-tuple-element.51), channel_id=1, source_target_pairs={{0,5},{1,4},{2,7},{3,6},{4,9},{5,8},{6,11},{7,10},{8,13},{9,12},{1... | collective-permute-start | bytes 98312 | tf_op jit(solution)/shard_map/ppermute | solution.py:40
  25.5 1.9 %collective-permute-start.4 = (bf16[192,256]{1,0:T(8,128)(2,1)S(1)}, bf16[192,256]{1,0:T(8,128)(2,1)S(1)}, u32[]{:S(2)}, u32[]{:S(2)}) collective-permute-start(bf16[192,256]{1,0:T(8,128)(2,1)S(1)} %get-tuple-element.56), channel_id=1, source_target_pairs={{0,3},{1,2},{2,5},{3,4},{4,7},{5,6},{6,9},{7,8},{8,11},{9,10},{10,... | collective-permute-start | bytes 294920 | tf_op jit(solution)/shard_map/ppermute | solution.py:40
  27.4 0.0 copy-done.1
  27.4 0.0 copy-done.5
  27.4 0.0 copy-start.2
  27.4 1.5 %shard_map.132 = (bf16[192,512]{1,0:T(8,128)(2,1)S(1)}, f32[2,2,256,256]{3,2,1,0:T(8,128)S(1)}, f32[1536,128]{1,0:T(8,128)S(1)}, f32[1536,128]{1,0:T(8,128)S(1)}, f32[1536,128]{1,0:T(8,128)S(1)}) custom-call(bf16[192,1024]{1,0:T(8,128)(2,1)S(1)} %get-tuple-element.52.normed_ref, bf16[1024,512]{1,0:T(8,128)(2,1)S(1)} %copy-done.1, ...), custom_call_target="tpu_custom_call" | custom-call | flops 2147483648 | bytes 1048576 | tf_op jit(solution)/shard_map/pallas_call | solution.py:409
  29.0 8.6 %collective-permute-done.4.near_ref = bf16[192,256]{1,0:T(8,128)(2,1)S(1)} collective-permute-done((bf16[192,256]{1,0:T(8,128)(2,1)S(1)}, bf16[192,256]{1,0:T(8,128)(2,1)S(1)}, u32[]{:S(2)}, u32[]{:S(2)}) %collective-permute-start.4) | collective-permute-done | bytes 98336 | tf_op jit(solution)/shard_map/ppermute | solution.py:40
  37.6 0.0 copy-done.2
  37.6 1.5 %shard_map.133 = (bf16[128,1024]{1,0:T(8,128)(2,1)S(1)}, f32[512,128]{1,0:T(8,128)S(1)}, f32[512,128]{1,0:T(8,128)S(1)}, f32[512,128]{1,0:T(8,128)S(1)}, bf16[51...) custom-call(bf16[192,512]{1,0:T(8,128)(2,1)S(1)} %get-tuple-element.55.query_ref, ...), custom_call_target="tpu_custom_call" | custom-call | flops 2147483648 | bytes 1048576 | tf_op jit(solution)/shard_map/pallas_call | solution.py:409
  39.1 0.0 collective-permute-done.3.far_ref
  39.1 0.8 %shard_map.134 = (bf16[192,512]{1,0:T(8,128)(2,1)S(1)}, bf16[192,512]{1,0:T(8,128)(2,1)S(1)}) custom-call(bf16[64,256]{1,0:T(8,128)(2,1)S(1)} %collective-permute-done.3.far_ref, bf16[80,256]{1,0:T(8,128)(2,1)S(1)} %collective-permute-done.far_ref.far_codes_ref, f32[2,2,256,256]{3,2,1,0:T(8,128)S(1)} %get-tuple-element.54.halo_bias, ...), custom_call_target="tpu_custom_call" | custom-call | flops 2147483648 | bytes 1048576 | tf_op jit(solution)/shard_map/pallas_call | solution.py:409
  39.9 2.1 %all-gather.1 = bf16[384,512]{1,0:T(8,128)(2,1)S(1)} all-gather(bf16[192,512]{1,0:T(8,128)(2,1)S(1)} %get-tuple-element.66), channel_id=3, replica_groups=mesh['sp'=256,'tp'=2] {'tp'}, dimensions={0}, use_global_device_ids=true | all-gather | bytes 589824 | tf_op jit(solution)/shard_map/all_gather | solution.py:529
  41.9 0.7 %shard_map.135 = bf16[192,512]{1,0:T(8,128)(2,1)} custom-call(bf16[2,192,512]{2,1,0:T(8,128)(2,1)S(1)} %bitcast.4, bf16[192,512]{1,0:T(8,128)(2,1)S(1)} %get-tuple-element.67.mine_ref, bf16[192,512]{1,0:T(8,128)(2,1)S(1)} %get-tuple-element.68.share_ref), custom_call_target="tpu_custom_call" | custom-call | flops 1048576 | bytes 1048576 | tf_op jit(solution)/shard_map/pallas_call | solution.py:409
  (3 shorter events, 0.0 us)
Async XLA Ops:
  0.0 7.9 %copy-start.4 = (f32[8,513]{1,0:T(8,128)S(1)}, f32[8,513]{1,0:T(8,128)}, u32[]{:S(2)}) copy-start(f32[8,513]{1,0:T(8,128)} %table_ref.2) | copy-start | bytes 49252
  0.9 17.2 %collective-permute-start = (bf16[80,256]{1,0:T(8,128)(2,1)S(1)}, bf16[80,256]{1,0:T(8,128)(2,1)S(1)}, u32[]{:S(2)}, u32[]{:S(2)}) collective-permute-start(bf16[80,256]{1,0:T(8,128)(2,1)S(1)} %get-tuple-element.37), channel_id=1, source_target_pairs={{0,4},{2,6},{4,8},{6,10},{8,12},{10,14},{12,16},{14,18},{16,20},{1... | collective-permute-start | bytes 122888 | tf_op jit(solution)/shard_map/ppermute | solution.py:43
  5.6 11.0 %copy-start = (bf16[512,1024]{1,0:T(8,128)(2,1)S(1)}, bf16[512,1024]{1,0:T(8,128)(2,1)}, u32[]{:S(2)}) copy-start(bf16[512,1024]{1,0:T(8,128)(2,1)} %weight_ref.6) | copy-start | bytes 3145732
  5.6 11.0 %copy-start.3 = (bf16[192,512]{1,0:T(8,128)(2,1)S(1)}, bf16[192,512]{1,0:T(8,128)(2,1)}, u32[]{:S(2)}) copy-start(bf16[192,512]{1,0:T(8,128)(2,1)} %residual_ref.3) | copy-start | bytes 589828
  5.6 11.0 %collective-permute-start.1 = (bf16[208,256]{1,0:T(8,128)(2,1)S(1)}, bf16[208,256]{1,0:T(8,128)(2,1)S(1)}, u32[]{:S(2)}, u32[]{:S(2)}) collective-permute-start(bf16[208,256]{1,0:T(8,128)(2,1)S(1)} %get-tuple-element.38.packed_ref), channel_id=1, source_target_pairs={{0,2},{2,4},{4,6},{6,8},{8,10},{10,12},{12,14},{14,16},{16,18},{18... | collective-permute-start | bytes 319496 | tf_op jit(solution)/shard_map/ppermute | solution.py:43
  10.1 12.9 %collective-permute-start.2 = (bf16[1024,256]{1,0:T(8,128)(2,1)S(1)}, bf16[1024,256]{1,0:T(8,128)(2,1)S(1)}, u32[]{:S(2)}, u32[]{:S(2)}) collective-permute-start(bf16[1024,256]{1,0:T(8,128)(2,1)S(1)} %get-tuple-element.50.weight_ref), channel_id=1, source_target_pairs={{0,1},{1,0},{2,3},{3,2},{4,5},{5,4},{6,7},{7,6},{8,9},{9,8},{10,11... | collective-permute-start | bytes 1572872 | tf_op jit(solution)/shard_map/ppermute | solution.py:477
  18.9 4.1 %copy-start.6 = (f32[1024]{0:T(1024)S(1)}, f32[1024]{0:T(1024)}, u32[]{:S(2)}) copy-start(f32[1024]{0:T(1024)} %param.20) | copy-start | bytes 12292
  23.0 4.4 %copy-start.1 = (bf16[1024,512]{1,0:T(8,128)(2,1)S(1)}, bf16[1024,512]{1,0:T(8,128)(2,1)}, u32[]{:S(2)}) copy-start(bf16[1024,512]{1,0:T(8,128)(2,1)} %weight_ref.7) | copy-start | bytes 3145732
  23.0 4.4 %copy-start.5 = (f32[8,513]{1,0:T(8,128)S(1)}, f32[8,513]{1,0:T(8,128)}, u32[]{:S(2)}) copy-start(f32[8,513]{1,0:T(8,128)} %table_ref.3) | copy-start | bytes 49252
  23.5 15.5 %collective-permute-start.3 = (bf16[64,256]{1,0:T(8,128)(2,1)S(1)}, bf16[64,256]{1,0:T(8,128)(2,1)S(1)}, u32[]{:S(2)}, u32[]{:S(2)}) collective-permute-start(bf16[64,256]{1,0:T(8,128)(2,1)S(1)} %get-tuple-element.51), channel_id=1, source_target_pairs={{0,5},{1,4},{2,7},{3,6},{4,9},{5,8},{6,11},{7,10},{8,13},{9,12},{1... | collective-permute-start | bytes 98312 | tf_op jit(solution)/shard_map/ppermute | solution.py:40
  25.5 12.1 %collective-permute-start.4 = (bf16[192,256]{1,0:T(8,128)(2,1)S(1)}, bf16[192,256]{1,0:T(8,128)(2,1)S(1)}, u32[]{:S(2)}, u32[]{:S(2)}) collective-permute-start(bf16[192,256]{1,0:T(8,128)(2,1)S(1)} %get-tuple-element.56), channel_id=1, source_target_pairs={{0,3},{1,2},{2,5},{3,4},{4,7},{5,6},{6,9},{7,8},{8,11},{9,10},{10,... | collective-permute-start | bytes 294920 | tf_op jit(solution)/shard_map/ppermute | solution.py:40
  27.4 10.2 %copy-start.2 = (bf16[512,1024]{1,0:T(8,128)(2,1)S(1)}, bf16[512,1024]{1,0:T(8,128)(2,1)}, u32[]{:S(2)}) copy-start(bf16[512,1024]{1,0:T(8,128)(2,1)} %weight_ref.9) | copy-start | bytes 3145732

commit v5 on v4

--- a/solution.py
+++ b/solution.py
@@ -66,8 +66,8 @@
     lanes = lax.broadcasted_iota(jnp.int32, flat.shape, 1)
     near = pltpu.roll(flat, SEG, 1)
     far = jnp.where(lanes < SEG, pltpu.roll(flat, 2 * TILE - (rows - SEG), 1), 0.0)
-    near_ref[rows : rows + 16, :] = jnp.concatenate([near, near], axis=0).astype(BF16)
-    far_ref[SEG : SEG + 16, :] = jnp.concatenate([far, far], axis=0).astype(BF16)
+    near_ref[rows : rows + 8, :] = near.astype(BF16)
+    far_ref[SEG : SEG + 8, :] = far.astype(BF16)
     for copy in copies[1:]:
         copy.wait()
 
@@ -269,7 +269,7 @@
 
 
 def codes_of(packed_ref, row, turn):
-    codes = packed_ref[row : row + 16, :].astype(F32)[0:8]
+    codes = packed_ref[row : row + 8, :].astype(F32)
     return pltpu.roll(codes, turn, 1) if turn else codes
 
 
@@ -297,15 +297,16 @@
 
 
 def before_two_kernel(
-    normed_ref, weight_ref, kv_ref, packed_ref, table_ref, query_ref, halo_bias, partial_ref, top_ref, total_ref,
+    normed_ref, weight_ref, kv_weight_ref, packed_ref, table_ref, query_ref, halo_bias, partial_ref, top_ref, total_ref,
     own_bias, band, swapped,
 ):
-    rows = kv_ref.shape[0]
+    rows = normed_ref.shape[0]
+    own = jnp.dot(normed_ref[...], kv_weight_ref[...], preferred_element_type=F32).astype(BF16)
     query = jnp.dot(normed_ref[...], weight_ref[...], preferred_element_type=F32).astype(BF16)
     query_ref[...] = query
     fill_bias(table_ref, halo_bias, own_bias)
     own_codes = codes_of(packed_ref, rows, 2 * TILE - SEG)
-    own_part(query, kv_ref[...], own_codes, own_bias, band, swapped, partial_ref, top_ref, total_ref)
+    own_part(query, own, own_codes, own_bias, band, swapped, partial_ref, top_ref, total_ref)
 
 
 def with_residual(partial, residual):
@@ -373,7 +374,7 @@
     theirs_ref[0:SEG, :] = jnp.where(first, partial[:, half:], partial[:, 0:half])
 
 
-def norm_kernel(both_ref, gain_ref, weight_ref, other_weight_ref, kv_ref, send_ref, tail_ref, normed_ref, share_ref):
+def norm_kernel(both_ref, gain_ref, other_weight_ref, send_ref, tail_ref, normed_ref, share_ref):
     layer = both_ref[0] + both_ref[1]
     wide = layer.astype(F32)
     rows, channels = wide.shape
@@ -382,7 +383,6 @@
     send = jnp.dot(normed, other_weight_ref[...], preferred_element_type=F32).astype(BF16)
     send_ref[...] = send
     tail_ref[...] = send[rows - SEG :]
-    kv_ref[...] = jnp.dot(normed, weight_ref[...], preferred_element_type=F32).astype(BF16)
     normed_ref[...] = normed
     half = channels // 2
     share_ref[...] = jnp.where(lax.axis_index("tp") == 0, layer[:, 0:half], layer[:, half:])
@@ -454,7 +454,7 @@
     own_shapes = (shape(2, 2, 4 * SEG, 2 * TILE, dtype=F32), stats, stats, stats)
     packed, far_send = call(
         pack_kernel,
-        (shape(rows + 16, 2 * TILE), shape(SEG + 16, 2 * TILE)),
+        (shape(rows + 8, 2 * TILE), shape(SEG + 8, 2 * TILE)),
         [pltpu.VMEM((8, 2 * TILE), F32), pltpu.VMEM((1, rows), jnp.int32), pltpu.SemaphoreType.DMA((7,))],
         tuple(pltpu.with_memory_space_constraint(x, pltpu.HBM) for x in (key_first, value_first, docs)),
         1 << 20,
@@ -490,17 +490,16 @@
         1 << 31,
     )
     both_one = lax.all_gather(sent_one, "tp", axis=0)
-    kv_two, send_two, tail_two, normed, share = call(
+    send_two, tail_two, normed, share = call(
         norm_kernel,
         (
-            shape(rows, 2 * TILE),
             shape(rows, 2 * TILE),
             shape(SEG, 2 * TILE),
             shape(rows, channels),
             shape(rows, half),
         ),
         [],
-        (both_one, gain, weights, other_weights),
+        (both_one, gain, other_weights),
         1 << 30,
     )
     near_two = from_behind(send_two, 1, across=True)
@@ -509,7 +508,7 @@
         before_two_kernel,
         (shape(rows, width), *own_shapes),
         before_scratch,
-        (normed, query_w, kv_two, packed, bias_second),
+        (normed, query_w, weights, packed, bias_second),
         1 << 31,
     )
     rest_two = call(

time: 43 us -> 42.9 us (level)
  the two profiles are of different devices: /device:TPU:257 before, /device:TPU:385 now
where the time goes in v5:
time: 42.9 us; the launch traced here: 42.6 us
  starting transfers between devices  14 us (33%)
  waiting for transfers between devices  11.6 us (27%)
  Pallas kernels  10.6 us (25%)
  blocking collectives  6.19 us (14%)
    pallas_call x9, Pallas kernels, call(): pl.pallas_call(kernel, out_shape=outs, in_specs=[whole()] * len(args) if...  10.6 us
    ppermute x2, waiting for transfers between devices, from_behind(): lax.ppermute(block, ('sp', 'tp'), [(2 * a + core, 2 * b + 1 - core) for a...  8.3 us
    ppermute x2, starting transfers between devices, from_behind(): return lax.ppermute(block, 'sp', route)  7 us
    all_gather x1, blocking collectives, body(): both_one = lax.all_gather(sent_one, 'tp', axis=0)  4.1 us
    ppermute x2, starting transfers between devices, from_behind(): lax.ppermute(block, ('sp', 'tp'), [(2 * a + core, 2 * b + 1 - core) for a...  3.84 us
    ppermute x2, waiting for transfers between devices, from_behind(): return lax.ppermute(block, 'sp', route)  3.34 us
    ppermute x1, starting transfers between devices, body(): other_weights = lax.ppermute(weights, 'tp', [(0, 1), (1, 0)])  3.14 us
    all_gather x1, blocking collectives, body(): both_two = lax.all_gather(sent_two, 'tp', axis=0)  2.09 us
  transfers between devices with their start and end apart: 5, of which 2 were waited for; matrix products, arithmetic and copies ran while one was open for 0% of the time, Pallas kernels for 18%

profile of v5, /device:TPU:385, one launch (start us, length us, event | category | flops | bytes accessed | tf_op | source)
XLA Modules:
  0.0 42.6 jit_solution(12781654141989110626)
XLA Ops:
  0.0 0.9 %shard_map.127 = (bf16[200,256]{1,0:T(8,128)(2,1)S(1)}, bf16[72,256]{1,0:T(8,128)(2,1)S(1)}) custom-call(bf16[192,128]{1,0:T(8,128)(2,1)} %key_hbm.1, bf16[192,128]{1,0:T(8,128)(2,1)} %value_hbm.1, s32[1,192]{1,0:T(1,128)} %bitcast.7), custom_call_target="tpu_custom_call" | custom-call | flops 1048576 | bytes 1048576 | tf_op jit(solution)/shard_map/pallas_call | solution.py:409
  0.9 4.7 %collective-permute-start = (bf16[72,256]{1,0:T(8,128)(2,1)S(1)}, bf16[72,256]{1,0:T(8,128)(2,1)S(1)}, u32[]{:S(2)}, u32[]{:S(2)}) collective-permute-start(bf16[72,256]{1,0:T(8,128)(2,1)S(1)} %get-tuple-element.36), channel_id=1, source_target_pairs={{0,4},{2,6},{4,8},{6,10},{8,12},{10,14},{12,16},{14,18},{16,20},{1... | collective-permute-start | bytes 110600 | tf_op jit(solution)/shard_map/ppermute | solution.py:43
  5.6 0.0 copy-start
  5.6 0.0 copy-start.3
  5.6 2.4 %collective-permute-start.1 = (bf16[200,256]{1,0:T(8,128)(2,1)S(1)}, bf16[200,256]{1,0:T(8,128)(2,1)S(1)}, u32[]{:S(2)}, u32[]{:S(2)}) collective-permute-start(bf16[200,256]{1,0:T(8,128)(2,1)S(1)} %get-tuple-element.37.packed_ref), channel_id=1, source_target_pairs={{0,2},{2,4},{4,6},{6,8},{8,10},{10,12},{12,14},{14,16},{16,18},{18... | collective-permute-start | bytes 307208 | tf_op jit(solution)/shard_map/ppermute | solution.py:43
  7.9 0.0 copy-done.4
  8.0 2.1 %shard_map.128 = (bf16[192,512]{1,0:T(8,128)(2,1)S(1)}, bf16[1024,256]{1,0:T(8,128)(2,1)S(1)}, f32[2,2,256,256]{3,2,1,0:T(8,128)S(1)}, f32[1536,128]{1,0:T(8,128...) custom-call(bf16[192,512]{1,0:T(8,128)(2,1)} %query_hbm.1, bf16[1024,128]{1,0:T(8,128)(2,1)} %key_w_hbm.1, ...), custom_call_target="tpu_custom_call" | custom-call | flops 2147483648 | bytes 1048576 | tf_op jit(solution)/shard_map/pallas_call | solution.py:409
  10.1 3.1 %collective-permute-start.2 = (bf16[1024,256]{1,0:T(8,128)(2,1)S(1)}, bf16[1024,256]{1,0:T(8,128)(2,1)S(1)}, u32[]{:S(2)}, u32[]{:S(2)}) collective-permute-start(bf16[1024,256]{1,0:T(8,128)(2,1)S(1)} %get-tuple-element.49.kv_weight_ref), channel_id=1, source_target_pairs={{0,1},{1,0},{2,3},{3,2},{4,5},{5,4},{6,7},{7,6},{8,9},{9,8},{10,11... | collective-permute-start | bytes 1572872 | tf_op jit(solution)/shard_map/ppermute | solution.py:477
  13.2 3.3 %collective-permute-done.1.near_ref.near_codes_ref = bf16[200,256]{1,0:T(8,128)(2,1)S(1)} collective-permute-done((bf16[200,256]{1,0:T(8,128)(2,1)S(1)}, bf16[200,256]{1,0:T(8,128)(2,1)S(1)}, u32[]{:S(2)}, u32[]{:S(2)}) %collective-permute-start.1) | collective-permute-done | bytes 102432 | tf_op jit(solution)/shard_map/ppermute | solution.py:43
  16.6 0.0 copy-done
  16.6 0.0 copy-done.3
  16.6 1.5 %shard_map.129 = (bf16[128,1024]{1,0:T(8,128)(2,1)S(1)}, f32[512,128]{1,0:T(8,128)S(1)}, f32[512,128]{1,0:T(8,128)S(1)}, f32[512,128]{1,0:T(8,128)S(1)}, bf16[51...) custom-call(bf16[192,512]{1,0:T(8,128)(2,1)S(1)} %get-tuple-element.39.query_ref, ...), custom_call_target="tpu_custom_call" | custom-call | flops 2147483648 | bytes 1048576 | tf_op jit(solution)/shard_map/pallas_call | solution.py:409
  18.1 0.0 collective-permute-done.far_ref.far_codes_ref
  18.1 0.8 %shard_map.130 = bf16[192,1024]{1,0:T(8,128)(2,1)S(1)} custom-call(bf16[72,256]{1,0:T(8,128)(2,1)S(1)} %collective-permute-done.far_ref.far_codes_ref, f32[2,2,256,256]{3,2,1,0:T(8,128)S(1)} %get-tuple-element.38.halo_bias, bf16[128,1024]{1,0:T(8,128)(2,1)S(1)} %get-tuple-element.43.rest_ref, f32[512,128]{1,0:T(8,128)S(1)} %get-tuple-element.44.partial_ref, ...), custom_call_target="tpu_custom_call" | custom-call | flops 2147483648 | bytes 1048576 | tf_op jit(solution)/shard_map/pallas_call | solution.py:409
  18.9 0.0 copy-start.6
  18.9 4.1 %all-gather = bf16[384,1024]{1,0:T(8,128)(2,1)S(1)} all-gather(bf16[192,1024]{1,0:T(8,128)(2,1)S(1)} %shard_map.130), channel_id=2, replica_groups=mesh['sp'=256,'tp'=2] {'tp'}, dimensions={0}, use_global_device_ids=true | all-gather | bytes 1179648 | tf_op jit(solution)/shard_map/all_gather | solution.py:492
  23.0 0.0 collective-permute-done.2.other_weight_ref
  23.0 0.0 copy-done.6
  23.0 0.4 shard_map.131
  23.4 1.9 %collective-permute-start.3 = (bf16[64,256]{1,0:T(8,128)(2,1)S(1)}, bf16[64,256]{1,0:T(8,128)(2,1)S(1)}, u32[]{:S(2)}, u32[]{:S(2)}) collective-permute-start(bf16[64,256]{1,0:T(8,128)(2,1)S(1)} %get-tuple-element.50), channel_id=1, source_target_pairs={{0,5},{1,4},{2,7},{3,6},{4,9},{5,8},{6,11},{7,10},{8,13},{9,12},{1... | collective-permute-start | bytes 98312 | tf_op jit(solution)/shard_map/ppermute | solution.py:40
  25.3 1.9 %collective-permute-start.4 = (bf16[192,256]{1,0:T(8,128)(2,1)S(1)}, bf16[192,256]{1,0:T(8,128)(2,1)S(1)}, u32[]{:S(2)}, u32[]{:S(2)}) collective-permute-start(bf16[192,256]{1,0:T(8,128)(2,1)S(1)} %get-tuple-element.54), channel_id=1, source_target_pairs={{0,3},{1,2},{2,5},{3,4},{4,7},{5,6},{6,9},{7,8},{8,11},{9,10},{10,... | collective-permute-start | bytes 294920 | tf_op jit(solution)/shard_map/ppermute | solution.py:40
  27.3 0.0 copy-done.1
  27.3 0.0 copy-done.5
  27.3 0.0 copy-start.2
  27.3 1.9 %shard_map.132 = (bf16[192,512]{1,0:T(8,128)(2,1)S(1)}, f32[2,2,256,256]{3,2,1,0:T(8,128)S(1)}, f32[1536,128]{1,0:T(8,128)S(1)}, f32[1536,128]{1,0:T(8,128)S(1)}, f32[1536,128]{1,0:T(8,128)S(1)}) custom-call(bf16[192,1024]{1,0:T(8,128)(2,1)S(1)} %get-tuple-element.51.normed_ref, bf16[1024,512]{1,0:T(8,128)(2,1)S(1)} %copy-done.1, ...), custom_call_target="tpu_custom_call" | custom-call | flops 2147483648 | bytes 1048576 | tf_op jit(solution)/shard_map/pallas_call | solution.py:409
  29.1 8.3 %collective-permute-done.4.near_ref = bf16[192,256]{1,0:T(8,128)(2,1)S(1)} collective-permute-done((bf16[192,256]{1,0:T(8,128)(2,1)S(1)}, bf16[192,256]{1,0:T(8,128)(2,1)S(1)}, u32[]{:S(2)}, u32[]{:S(2)}) %collective-permute-start.4) | collective-permute-done | bytes 98336 | tf_op jit(solution)/shard_map/ppermute | solution.py:40
  37.4 0.0 copy-done.2
  37.4 1.5 %shard_map.133 = (bf16[128,1024]{1,0:T(8,128)(2,1)S(1)}, f32[512,128]{1,0:T(8,128)S(1)}, f32[512,128]{1,0:T(8,128)S(1)}, f32[512,128]{1,0:T(8,128)S(1)}, bf16[51...) custom-call(bf16[192,512]{1,0:T(8,128)(2,1)S(1)} %get-tuple-element.53.query_ref, ...), custom_call_target="tpu_custom_call" | custom-call | flops 2147483648 | bytes 1048576 | tf_op jit(solution)/shard_map/pallas_call | solution.py:409
  39.0 0.0 collective-permute-done.3.far_ref
  39.0 0.8 %shard_map.134 = (bf16[192,512]{1,0:T(8,128)(2,1)S(1)}, bf16[192,512]{1,0:T(8,128)(2,1)S(1)}) custom-call(bf16[64,256]{1,0:T(8,128)(2,1)S(1)} %collective-permute-done.3.far_ref, bf16[72,256]{1,0:T(8,128)(2,1)S(1)} %collective-permute-done.far_ref.far_codes_ref, f32[2,2,256,256]{3,2,1,0:T(8,128)S(1)} %get-tuple-element.52.halo_bias, ...), custom_call_target="tpu_custom_call" | custom-call | flops 2147483648 | bytes 1048576 | tf_op jit(solution)/shard_map/pallas_call | solution.py:409
  39.8 2.1 %all-gather.1 = bf16[384,512]{1,0:T(8,128)(2,1)S(1)} all-gather(bf16[192,512]{1,0:T(8,128)(2,1)S(1)} %get-tuple-element.64), channel_id=3, replica_groups=mesh['sp'=256,'tp'=2] {'tp'}, dimensions={0}, use_global_device_ids=true | all-gather | bytes 589824 | tf_op jit(solution)/shard_map/all_gather | solution.py:528
  41.8 0.8 %shard_map.135 = bf16[192,512]{1,0:T(8,128)(2,1)} custom-call(bf16[2,192,512]{2,1,0:T(8,128)(2,1)S(1)} %bitcast.4, bf16[192,512]{1,0:T(8,128)(2,1)S(1)} %get-tuple-element.65.mine_ref, bf16[192,512]{1,0:T(8,128)(2,1)S(1)} %get-tuple-element.66.share_ref), custom_call_target="tpu_custom_call" | custom-call | flops 1048576 | bytes 1048576 | tf_op jit(solution)/shard_map/pallas_call | solution.py:409
  (3 shorter events, 0.0 us)
Async XLA Ops:
  0.0 7.9 %copy-start.4 = (f32[8,513]{1,0:T(8,128)S(1)}, f32[8,513]{1,0:T(8,128)}, u32[]{:S(2)}) copy-start(f32[8,513]{1,0:T(8,128)} %table_ref.2) | copy-start | bytes 49252
  0.9 17.2 %collective-permute-start = (bf16[72,256]{1,0:T(8,128)(2,1)S(1)}, bf16[72,256]{1,0:T(8,128)(2,1)S(1)}, u32[]{:S(2)}, u32[]{:S(2)}) collective-permute-start(bf16[72,256]{1,0:T(8,128)(2,1)S(1)} %get-tuple-element.36), channel_id=1, source_target_pairs={{0,4},{2,6},{4,8},{6,10},{8,12},{10,14},{12,16},{14,18},{16,20},{1... | collective-permute-start | bytes 110600 | tf_op jit(solution)/shard_map/ppermute | solution.py:43
  5.6 11.0 %copy-start = (bf16[512,1024]{1,0:T(8,128)(2,1)S(1)}, bf16[512,1024]{1,0:T(8,128)(2,1)}, u32[]{:S(2)}) copy-start(bf16[512,1024]{1,0:T(8,128)(2,1)} %weight_ref.6) | copy-start | bytes 3145732
  5.6 11.0 %copy-start.3 = (bf16[192,512]{1,0:T(8,128)(2,1)S(1)}, bf16[192,512]{1,0:T(8,128)(2,1)}, u32[]{:S(2)}) copy-start(bf16[192,512]{1,0:T(8,128)(2,1)} %residual_ref.3) | copy-start | bytes 589828
  5.6 11.0 %collective-permute-start.1 = (bf16[200,256]{1,0:T(8,128)(2,1)S(1)}, bf16[200,256]{1,0:T(8,128)(2,1)S(1)}, u32[]{:S(2)}, u32[]{:S(2)}) collective-permute-start(bf16[200,256]{1,0:T(8,128)(2,1)S(1)} %get-tuple-element.37.packed_ref), channel_id=1, source_target_pairs={{0,2},{2,4},{4,6},{6,8},{8,10},{10,12},{12,14},{14,16},{16,18},{18... | collective-permute-start | bytes 307208 | tf_op jit(solution)/shard_map/ppermute | solution.py:43
  10.1 12.9 %collective-permute-start.2 = (bf16[1024,256]{1,0:T(8,128)(2,1)S(1)}, bf16[1024,256]{1,0:T(8,128)(2,1)S(1)}, u32[]{:S(2)}, u32[]{:S(2)}) collective-permute-start(bf16[1024,256]{1,0:T(8,128)(2,1)S(1)} %get-tuple-element.49.kv_weight_ref), channel_id=1, source_target_pairs={{0,1},{1,0},{2,3},{3,2},{4,5},{5,4},{6,7},{7,6},{8,9},{9,8},{10,11... | collective-permute-start | bytes 1572872 | tf_op jit(solution)/shard_map/ppermute | solution.py:477
  18.9 4.1 %copy-start.6 = (f32[1024]{0:T(1024)S(1)}, f32[1024]{0:T(1024)}, u32[]{:S(2)}) copy-start(f32[1024]{0:T(1024)} %param.20) | copy-start | bytes 12292
  23.0 4.3 %copy-start.1 = (bf16[1024,512]{1,0:T(8,128)(2,1)S(1)}, bf16[1024,512]{1,0:T(8,128)(2,1)}, u32[]{:S(2)}) copy-start(bf16[1024,512]{1,0:T(8,128)(2,1)} %weight_ref.7) | copy-start | bytes 3145732
  23.0 4.3 %copy-start.5 = (f32[8,513]{1,0:T(8,128)S(1)}, f32[8,513]{1,0:T(8,128)}, u32[]{:S(2)}) copy-start(f32[8,513]{1,0:T(8,128)} %table_ref.3) | copy-start | bytes 49252
  23.4 15.6 %collective-permute-start.3 = (bf16[64,256]{1,0:T(8,128)(2,1)S(1)}, bf16[64,256]{1,0:T(8,128)(2,1)S(1)}, u32[]{:S(2)}, u32[]{:S(2)}) collective-permute-start(bf16[64,256]{1,0:T(8,128)(2,1)S(1)} %get-tuple-element.50), channel_id=1, source_target_pairs={{0,5},{1,4},{2,7},{3,6},{4,9},{5,8},{6,11},{7,10},{8,13},{9,12},{1... | collective-permute-start | bytes 98312 | tf_op jit(solution)/shard_map/ppermute | solution.py:40
  25.3 12.1 %collective-permute-start.4 = (bf16[192,256]{1,0:T(8,128)(2,1)S(1)}, bf16[192,256]{1,0:T(8,128)(2,1)S(1)}, u32[]{:S(2)}, u32[]{:S(2)}) collective-permute-start(bf16[192,256]{1,0:T(8,128)(2,1)S(1)} %get-tuple-element.54), channel_id=1, source_target_pairs={{0,3},{1,2},{2,5},{3,4},{4,7},{5,6},{6,9},{7,8},{8,11},{9,10},{10,... | collective-permute-start | bytes 294920 | tf_op jit(solution)/shard_map/ppermute | solution.py:40
  27.3 10.2 %copy-start.2 = (bf16[512,1024]{1,0:T(8,128)(2,1)S(1)}, bf16[512,1024]{1,0:T(8,128)(2,1)}, u32[]{:S(2)}) copy-start(bf16[512,1024]{1,0:T(8,128)(2,1)} %weight_ref.9) | copy-start | bytes 3145732

commit v6 on v5

--- a/solution.py
+++ b/solution.py
@@ -255,16 +255,15 @@
         top = jnp.maximum(jnp.max(s, axis=1, keepdims=True), old_top)
         e = jnp.exp(s - top[:, 0:SEG])
         old = jnp.exp(old_top - top)
-        share = 1.0 / (total_ref[place, :] * old + jnp.sum(e, axis=1, keepdims=True))
-        shares.append(share)
-        olds.append(old * share)
+        shares.append(1.0 / (total_ref[place, :] * old + jnp.sum(e, axis=1, keepdims=True)))
+        olds.append(old)
         weights.append(e.astype(BF16))
     blended = jnp.dot(jnp.concatenate(weights, axis=0), both, preferred_element_type=F32)
     results = []
     for block in range(8):
         place = slice(SEG * block, SEG * (block + 1))
         side = slice(TILE * (block // 4), TILE * (block // 4 + 1))
-        results.append(blended[place, side] * shares[block] + partial_ref[place, :] * olds[block])
+        results.append((blended[place, side] + partial_ref[place, :] * olds[block]) * shares[block])
     store_heads(mixed, 0, results, lanes)
 
 
@@ -333,7 +332,7 @@
 
 def near_two_kernel(
     query_ref, near_ref, near_codes_ref, packed_ref, halo_bias, partial_ref, top_ref, total_ref, weight_ref,
-    out_ref, head_partial, head_top, head_total, head_left, head_code, band, swapped, mixed,
+    mine_ref, theirs_ref, head_partial, head_top, head_total, head_left, head_code, band, swapped, mixed,
 ):
     rows = query_ref.shape[0]
     near_part(
@@ -341,7 +340,11 @@
         halo_bias, partial_ref, top_ref, total_ref, band, swapped, mixed,
         (head_partial, head_top, head_total, head_left, head_code),
     )
-    out_ref[...] = jnp.dot(mixed[...], weight_ref[...], preferred_element_type=F32).astype(BF16)
+    half = mine_ref.shape[1]
+    first = lax.axis_index("tp") == 0
+    partial = jnp.dot(mixed[...], weight_ref[...], preferred_element_type=F32).astype(BF16)
+    mine_ref[...] = jnp.where(first, partial[:, 0:half], partial[:, half:])
+    theirs_ref[...] = jnp.where(first, partial[:, half:], partial[:, 0:half])
 
 
 def far_one_kernel(
@@ -358,19 +361,17 @@
 
 
 def far_two_kernel(
-    far_ref, far_codes_ref, halo_bias, rest_ref, partial_ref, top_ref, total_ref, left_ref, code_ref, weight_ref,
+    far_ref, far_codes_ref, halo_bias, rest_theirs_ref, partial_ref, top_ref, total_ref, left_ref, code_ref, weight_ref,
     mine_ref, theirs_ref, mixed,
 ):
     half = mine_ref.shape[1]
     first = lax.axis_index("tp") == 0
-    rest = rest_ref[...]
-    mine_ref[SEG:, :] = jnp.where(first, rest[:, 0:half], rest[:, half:])
-    theirs_ref[SEG:, :] = jnp.where(first, rest[:, half:], rest[:, 0:half])
+    theirs_ref[SEG:, :] = rest_theirs_ref[...]
     far_part(
         far_ref[...], codes_of(far_codes_ref, SEG, 0), halo_bias, partial_ref, top_ref, total_ref, left_ref, code_ref, mixed
     )
     partial = jnp.dot(mixed[...], weight_ref[...], preferred_element_type=F32).astype(BF16)
-    mine_ref[0:SEG, :] = jnp.where(first, partial[:, 0:half], partial[:, half:])
+    mine_ref[...] = jnp.where(first, partial[:, 0:half], partial[:, half:])
     theirs_ref[0:SEG, :] = jnp.where(first, partial[:, half:], partial[:, 0:half])
 
 
@@ -388,16 +389,17 @@
     share_ref[...] = jnp.where(lax.axis_index("tp") == 0, layer[:, 0:half], layer[:, half:])
 
 
-def last_kernel(both_ref, mine_ref, share_ref, out_hbm, out, sems):
+def last_kernel(both_ref, head_ref, rest_ref, share_ref, out_hbm, out, sems):
     first = lax.axis_index("tp") == 0
     copies = []
     parts = sems.shape[0]
-    rows = out.shape[0] // parts
+    rows = SEG
     for part in range(parts):
         spot = slice(rows * part, rows * (part + 1))
         theirs = jnp.where(first, both_ref[1, spot, :], both_ref[0, spot, :])
+        mine = rest_ref[spot.start - SEG : spot.stop - SEG, :] if part else head_ref[...]
         out[spot, :] = (
-            share_ref[spot, :].astype(F32) + mine_ref[spot, :].astype(F32) + theirs.astype(F32)
+            share_ref[spot, :].astype(F32) + mine.astype(F32) + theirs.astype(F32)
         ).astype(BF16)
         copies.append(pltpu.make_async_copy(out.at[spot, :], out_hbm.at[spot, :], sems.at[part]))
         copies[-1].start()
@@ -511,16 +513,16 @@
         (normed, query_w, weights, packed, bias_second),
         1 << 31,
     )
-    rest_two = call(
+    rest_mine, *rest_two = call(
         near_two_kernel,
-        near_shapes,
+        (shape(rows - SEG, half), shape(rows - SEG, half), *near_shapes[1:]),
         near_scratch,
         (query_two, near_two, near_one, packed, *own_two, out_second),
         1 << 31,
     )
     mine_two, sent_two = call(
         far_two_kernel,
-        (shape(rows, half), shape(rows, half)),
+        (shape(SEG, half), shape(rows, half)),
         far_scratch,
         (far_two, far_one, own_two[0], *rest_two, out_second),
         1 << 31,
@@ -529,8 +531,8 @@
     return call(
         last_kernel,
         shape(rows, half),
-        [pltpu.VMEM((rows, half), BF16), pltpu.SemaphoreType.DMA((4,))],
-        (both_two, mine_two, share),
+        [pltpu.VMEM((rows, half), BF16), pltpu.SemaphoreType.DMA((3,))],
+        (both_two, mine_two, rest_mine, share),
         1 << 20,
         out_space=pltpu.HBM,
     )

time: 42.9 us -> 42.9 us (level)
  no operation moved by 1% of the time
where the time goes in v6:
time: 42.9 us; the launch traced here: 42.6 us
  starting transfers between devices  14 us (33%)
  waiting for transfers between devices  11.6 us (27%)
  Pallas kernels  10.6 us (25%)
  blocking collectives  6.19 us (14%)
    pallas_call x9, Pallas kernels, call(): pl.pallas_call(kernel, out_shape=outs, in_specs=[whole()] * len(args) if...  10.6 us
    ppermute x2, waiting for transfers between devices, from_behind(): lax.ppermute(block, ('sp', 'tp'), [(2 * a + core, 2 * b + 1 - core) for a...  8.3 us
    ppermute x2, starting transfers between devices, from_behind(): return lax.ppermute(block, 'sp', route)  7 us
    all_gather x1, blocking collectives, body(): both_one = lax.all_gather(sent_one, 'tp', axis=0)  4.1 us
    ppermute x2, starting transfers between devices, from_behind(): lax.ppermute(block, ('sp', 'tp'), [(2 * a + core, 2 * b + 1 - core) for a...  3.84 us
    ppermute x2, waiting for transfers between devices, from_behind(): return lax.ppermute(block, 'sp', route)  3.34 us
    ppermute x1, starting transfers between devices, body(): other_weights = lax.ppermute(weights, 'tp', [(0, 1), (1, 0)])  3.14 us
    all_gather x1, blocking collectives, body(): both_two = lax.all_gather(sent_two, 'tp', axis=0)  2.09 us
  transfers between devices with their start and end apart: 5, of which 2 were waited for; matrix products, arithmetic and copies ran while one was open for 0% of the time, Pallas kernels for 18%

profile of v6, /device:TPU:385, one launch (start us, length us, event | category | flops | bytes accessed | tf_op | source)
XLA Modules:
  0.0 42.6 jit_solution(18382375253734189553)
XLA Ops:
  0.0 0.9 %shard_map.127 = (bf16[200,256]{1,0:T(8,128)(2,1)S(1)}, bf16[72,256]{1,0:T(8,128)(2,1)S(1)}) custom-call(bf16[192,128]{1,0:T(8,128)(2,1)} %key_hbm.1, bf16[192,128]{1,0:T(8,128)(2,1)} %value_hbm.1, s32[1,192]{1,0:T(1,128)} %bitcast.7), custom_call_target="tpu_custom_call" | custom-call | flops 1048576 | bytes 1048576 | tf_op jit(solution)/shard_map/pallas_call | solution.py:411
  0.9 4.7 %collective-permute-start = (bf16[72,256]{1,0:T(8,128)(2,1)S(1)}, bf16[72,256]{1,0:T(8,128)(2,1)S(1)}, u32[]{:S(2)}, u32[]{:S(2)}) collective-permute-start(bf16[72,256]{1,0:T(8,128)(2,1)S(1)} %get-tuple-element.37), channel_id=1, source_target_pairs={{0,4},{2,6},{4,8},{6,10},{8,12},{10,14},{12,16},{14,18},{16,20},{1... | collective-permute-start | bytes 110600 | tf_op jit(solution)/shard_map/ppermute | solution.py:43
  5.6 0.0 copy-start
  5.6 0.0 copy-start.3
  5.6 2.4 %collective-permute-start.1 = (bf16[200,256]{1,0:T(8,128)(2,1)S(1)}, bf16[200,256]{1,0:T(8,128)(2,1)S(1)}, u32[]{:S(2)}, u32[]{:S(2)}) collective-permute-start(bf16[200,256]{1,0:T(8,128)(2,1)S(1)} %get-tuple-element.38.packed_ref), channel_id=1, source_target_pairs={{0,2},{2,4},{4,6},{6,8},{8,10},{10,12},{12,14},{14,16},{16,18},{18... | collective-permute-start | bytes 307208 | tf_op jit(solution)/shard_map/ppermute | solution.py:43
  7.9 0.0 copy-done.4
  8.0 2.1 %shard_map.128 = (bf16[192,512]{1,0:T(8,128)(2,1)S(1)}, bf16[1024,256]{1,0:T(8,128)(2,1)S(1)}, f32[2,2,256,256]{3,2,1,0:T(8,128)S(1)}, f32[1536,128]{1,0:T(8,128...) custom-call(bf16[192,512]{1,0:T(8,128)(2,1)} %query_hbm.1, bf16[1024,128]{1,0:T(8,128)(2,1)} %key_w_hbm.1, ...), custom_call_target="tpu_custom_call" | custom-call | flops 2147483648 | bytes 1048576 | tf_op jit(solution)/shard_map/pallas_call | solution.py:411
  10.1 3.1 %collective-permute-start.2 = (bf16[1024,256]{1,0:T(8,128)(2,1)S(1)}, bf16[1024,256]{1,0:T(8,128)(2,1)S(1)}, u32[]{:S(2)}, u32[]{:S(2)}) collective-permute-start(bf16[1024,256]{1,0:T(8,128)(2,1)S(1)} %get-tuple-element.50.kv_weight_ref), channel_id=1, source_target_pairs={{0,1},{1,0},{2,3},{3,2},{4,5},{5,4},{6,7},{7,6},{8,9},{9,8},{10,11... | collective-permute-start | bytes 1572872 | tf_op jit(solution)/shard_map/ppermute | solution.py:479
  13.2 3.3 %collective-permute-done.1.near_ref.near_codes_ref = bf16[200,256]{1,0:T(8,128)(2,1)S(1)} collective-permute-done((bf16[200,256]{1,0:T(8,128)(2,1)S(1)}, bf16[200,256]{1,0:T(8,128)(2,1)S(1)}, u32[]{:S(2)}, u32[]{:S(2)}) %collective-permute-start.1) | collective-permute-done | bytes 102432 | tf_op jit(solution)/shard_map/ppermute | solution.py:43
  16.6 0.0 copy-done
  16.6 0.0 copy-done.3
  16.6 1.5 %shard_map.129 = (bf16[128,1024]{1,0:T(8,128)(2,1)S(1)}, f32[512,128]{1,0:T(8,128)S(1)}, f32[512,128]{1,0:T(8,128)S(1)}, f32[512,128]{1,0:T(8,128)S(1)}, bf16[51...) custom-call(bf16[192,512]{1,0:T(8,128)(2,1)S(1)} %get-tuple-element.40.query_ref, ...), custom_call_target="tpu_custom_call" | custom-call | flops 2147483648 | bytes 1048576 | tf_op jit(solution)/shard_map/pallas_call | solution.py:411
  18.1 0.0 collective-permute-done.far_ref.far_codes_ref
  18.1 0.8 %shard_map.130 = bf16[192,1024]{1,0:T(8,128)(2,1)S(1)} custom-call(bf16[72,256]{1,0:T(8,128)(2,1)S(1)} %collective-permute-done.far_ref.far_codes_ref, f32[2,2,256,256]{3,2,1,0:T(8,128)S(1)} %get-tuple-element.39.halo_bias, bf16[128,1024]{1,0:T(8,128)(2,1)S(1)} %get-tuple-element.44.rest_ref, f32[512,128]{1,0:T(8,128)S(1)} %get-tuple-element.45.partial_ref, ...), custom_call_target="tpu_custom_call" | custom-call | flops 2147483648 | bytes 1048576 | tf_op jit(solution)/shard_map/pallas_call | solution.py:411
  18.9 0.0 copy-start.6
  18.9 4.1 %all-gather = bf16[384,1024]{1,0:T(8,128)(2,1)S(1)} all-gather(bf16[192,1024]{1,0:T(8,128)(2,1)S(1)} %shard_map.130), channel_id=2, replica_groups=mesh['sp'=256,'tp'=2] {'tp'}, dimensions={0}, use_global_device_ids=true | all-gather | bytes 1179648 | tf_op jit(solution)/shard_map/all_gather | solution.py:494
  23.0 0.0 collective-permute-done.2.other_weight_ref
  23.0 0.0 copy-done.6
  23.0 0.4 shard_map.131
  23.4 1.9 %collective-permute-start.3 = (bf16[64,256]{1,0:T(8,128)(2,1)S(1)}, bf16[64,256]{1,0:T(8,128)(2,1)S(1)}, u32[]{:S(2)}, u32[]{:S(2)}) collective-permute-start(bf16[64,256]{1,0:T(8,128)(2,1)S(1)} %get-tuple-element.51), channel_id=1, source_target_pairs={{0,5},{1,4},{2,7},{3,6},{4,9},{5,8},{6,11},{7,10},{8,13},{9,12},{1... | collective-permute-start | bytes 98312 | tf_op jit(solution)/shard_map/ppermute | solution.py:40
  25.3 1.9 %collective-permute-start.4 = (bf16[192,256]{1,0:T(8,128)(2,1)S(1)}, bf16[192,256]{1,0:T(8,128)(2,1)S(1)}, u32[]{:S(2)}, u32[]{:S(2)}) collective-permute-start(bf16[192,256]{1,0:T(8,128)(2,1)S(1)} %get-tuple-element.55), channel_id=1, source_target_pairs={{0,3},{1,2},{2,5},{3,4},{4,7},{5,6},{6,9},{7,8},{8,11},{9,10},{10,... | collective-permute-start | bytes 294920 | tf_op jit(solution)/shard_map/ppermute | solution.py:40
  27.3 0.0 copy-done.1
  27.3 0.0 copy-done.5
  27.3 0.0 copy-start.2
  27.3 1.9 %shard_map.132 = (bf16[192,512]{1,0:T(8,128)(2,1)S(1)}, f32[2,2,256,256]{3,2,1,0:T(8,128)S(1)}, f32[1536,128]{1,0:T(8,128)S(1)}, f32[1536,128]{1,0:T(8,128)S(1)}, f32[1536,128]{1,0:T(8,128)S(1)}) custom-call(bf16[192,1024]{1,0:T(8,128)(2,1)S(1)} %get-tuple-element.52.normed_ref, bf16[1024,512]{1,0:T(8,128)(2,1)S(1)} %copy-done.1, ...), custom_call_target="tpu_custom_call" | custom-call | flops 2147483648 | bytes 1048576 | tf_op jit(solution)/shard_map/pallas_call | solution.py:411
  29.1 8.3 %collective-permute-done.4.near_ref = bf16[192,256]{1,0:T(8,128)(2,1)S(1)} collective-permute-done((bf16[192,256]{1,0:T(8,128)(2,1)S(1)}, bf16[192,256]{1,0:T(8,128)(2,1)S(1)}, u32[]{:S(2)}, u32[]{:S(2)}) %collective-permute-start.4) | collective-permute-done | bytes 98336 | tf_op jit(solution)/shard_map/ppermute | solution.py:40
  37.4 0.0 copy-done.2
  37.4 1.5 %shard_map.133 = (bf16[128,512]{1,0:T(8,128)(2,1)S(1)}, bf16[128,512]{1,0:T(8,128)(2,1)S(1)}, f32[512,128]{1,0:T(8,128)S(1)}, f32[512,128]{1,0:T(8,128)S(1)}, f3...) custom-call(bf16[192,512]{1,0:T(8,128)(2,1)S(1)} %get-tuple-element.54.query_ref, ...), custom_call_target="tpu_custom_call" | custom-call | flops 2147483648 | bytes 1048576 | tf_op jit(solution)/shard_map/pallas_call | solution.py:411
  39.0 0.0 collective-permute-done.3.far_ref
  39.0 0.8 %shard_map.134 = (bf16[64,512]{1,0:T(8,128)(2,1)S(1)}, bf16[192,512]{1,0:T(8,128)(2,1)S(1)}) custom-call(bf16[64,256]{1,0:T(8,128)(2,1)S(1)} %collective-permute-done.3.far_ref, bf16[72,256]{1,0:T(8,128)(2,1)S(1)} %collective-permute-done.far_ref.far_codes_ref, f32[2,2,256,256]{3,2,1,0:T(8,128)S(1)} %get-tuple-element.53.halo_bias, ...), custom_call_target="tpu_custom_call" | custom-call | flops 2147483648 | bytes 1048576 | tf_op jit(solution)/shard_map/pallas_call | solution.py:411
  39.8 2.1 %all-gather.1 = bf16[384,512]{1,0:T(8,128)(2,1)S(1)} all-gather(bf16[192,512]{1,0:T(8,128)(2,1)S(1)} %get-tuple-element.65), channel_id=3, replica_groups=mesh['sp'=256,'tp'=2] {'tp'}, dimensions={0}, use_global_device_ids=true | all-gather | bytes 589824 | tf_op jit(solution)/shard_map/all_gather | solution.py:530
  41.8 0.7 %shard_map.135 = bf16[192,512]{1,0:T(8,128)(2,1)} custom-call(bf16[2,192,512]{2,1,0:T(8,128)(2,1)S(1)} %bitcast.4, bf16[64,512]{1,0:T(8,128)(2,1)S(1)} %get-tuple-element.66.head_ref, bf16[128,512]{1,0:T(8,128)(2,1)S(1)} %get-tuple-element.67.rest_ref, bf16[192,512]{1,0:T(8,128)(2,1)S(1)} %get-tuple-element.68.share_ref), custom_call_target="tpu_custom_call" | custom-call | flops 1048576 | bytes 1048576 | tf_op jit(solution)/shard_map/pallas_call | solution.py:411
  (3 shorter events, 0.0 us)
Async XLA Ops:
  0.0 7.9 %copy-start.4 = (f32[8,513]{1,0:T(8,128)S(1)}, f32[8,513]{1,0:T(8,128)}, u32[]{:S(2)}) copy-start(f32[8,513]{1,0:T(8,128)} %table_ref.2) | copy-start | bytes 49252
  0.9 17.2 %collective-permute-start = (bf16[72,256]{1,0:T(8,128)(2,1)S(1)}, bf16[72,256]{1,0:T(8,128)(2,1)S(1)}, u32[]{:S(2)}, u32[]{:S(2)}) collective-permute-start(bf16[72,256]{1,0:T(8,128)(2,1)S(1)} %get-tuple-element.37), channel_id=1, source_target_pairs={{0,4},{2,6},{4,8},{6,10},{8,12},{10,14},{12,16},{14,18},{16,20},{1... | collective-permute-start | bytes 110600 | tf_op jit(solution)/shard_map/ppermute | solution.py:43
  5.6 11.0 %copy-start = (bf16[512,1024]{1,0:T(8,128)(2,1)S(1)}, bf16[512,1024]{1,0:T(8,128)(2,1)}, u32[]{:S(2)}) copy-start(bf16[512,1024]{1,0:T(8,128)(2,1)} %weight_ref.6) | copy-start | bytes 3145732
  5.6 11.0 %copy-start.3 = (bf16[192,512]{1,0:T(8,128)(2,1)S(1)}, bf16[192,512]{1,0:T(8,128)(2,1)}, u32[]{:S(2)}) copy-start(bf16[192,512]{1,0:T(8,128)(2,1)} %residual_ref.3) | copy-start | bytes 589828
  5.6 11.0 %collective-permute-start.1 = (bf16[200,256]{1,0:T(8,128)(2,1)S(1)}, bf16[200,256]{1,0:T(8,128)(2,1)S(1)}, u32[]{:S(2)}, u32[]{:S(2)}) collective-permute-start(bf16[200,256]{1,0:T(8,128)(2,1)S(1)} %get-tuple-element.38.packed_ref), channel_id=1, source_target_pairs={{0,2},{2,4},{4,6},{6,8},{8,10},{10,12},{12,14},{14,16},{16,18},{18... | collective-permute-start | bytes 307208 | tf_op jit(solution)/shard_map/ppermute | solution.py:43
  10.1 12.9 %collective-permute-start.2 = (bf16[1024,256]{1,0:T(8,128)(2,1)S(1)}, bf16[1024,256]{1,0:T(8,128)(2,1)S(1)}, u32[]{:S(2)}, u32[]{:S(2)}) collective-permute-start(bf16[1024,256]{1,0:T(8,128)(2,1)S(1)} %get-tuple-element.50.kv_weight_ref), channel_id=1, source_target_pairs={{0,1},{1,0},{2,3},{3,2},{4,5},{5,4},{6,7},{7,6},{8,9},{9,8},{10,11... | collective-permute-start | bytes 1572872 | tf_op jit(solution)/shard_map/ppermute | solution.py:479
  18.9 4.1 %copy-start.6 = (f32[1024]{0:T(1024)S(1)}, f32[1024]{0:T(1024)}, u32[]{:S(2)}) copy-start(f32[1024]{0:T(1024)} %param.20) | copy-start | bytes 12292
  23.0 4.3 %copy-start.1 = (bf16[1024,512]{1,0:T(8,128)(2,1)S(1)}, bf16[1024,512]{1,0:T(8,128)(2,1)}, u32[]{:S(2)}) copy-start(bf16[1024,512]{1,0:T(8,128)(2,1)} %weight_ref.7) | copy-start | bytes 3145732
  23.0 4.3 %copy-start.5 = (f32[8,513]{1,0:T(8,128)S(1)}, f32[8,513]{1,0:T(8,128)}, u32[]{:S(2)}) copy-start(f32[8,513]{1,0:T(8,128)} %table_ref.3) | copy-start | bytes 49252
  23.4 15.6 %collective-permute-start.3 = (bf16[64,256]{1,0:T(8,128)(2,1)S(1)}, bf16[64,256]{1,0:T(8,128)(2,1)S(1)}, u32[]{:S(2)}, u32[]{:S(2)}) collective-permute-start(bf16[64,256]{1,0:T(8,128)(2,1)S(1)} %get-tuple-element.51), channel_id=1, source_target_pairs={{0,5},{1,4},{2,7},{3,6},{4,9},{5,8},{6,11},{7,10},{8,13},{9,12},{1... | collective-permute-start | bytes 98312 | tf_op jit(solution)/shard_map/ppermute | solution.py:40
  25.3 12.1 %collective-permute-start.4 = (bf16[192,256]{1,0:T(8,128)(2,1)S(1)}, bf16[192,256]{1,0:T(8,128)(2,1)S(1)}, u32[]{:S(2)}, u32[]{:S(2)}) collective-permute-start(bf16[192,256]{1,0:T(8,128)(2,1)S(1)} %get-tuple-element.55), channel_id=1, source_target_pairs={{0,3},{1,2},{2,5},{3,4},{4,7},{5,6},{6,9},{7,8},{8,11},{9,10},{10,... | collective-permute-start | bytes 294920 | tf_op jit(solution)/shard_map/ppermute | solution.py:40
  27.3 10.2 %copy-start.2 = (bf16[512,1024]{1,0:T(8,128)(2,1)S(1)}, bf16[512,1024]{1,0:T(8,128)(2,1)}, u32[]{:S(2)}) copy-start(bf16[512,1024]{1,0:T(8,128)(2,1)} %weight_ref.9) | copy-start | bytes 3145732
